TPU v7x, 128 devices: a whole 4x4x4 slice. The times are simulated.
128 devices in a mesh: ep: 32 (over z, y, core), tp: 4 (over x).
Axes of the slice: x: 4, y: 4, z: 4, core: 2. Of those that a mesh axis runs over, the one named last changes fastest.
Arguments:
- tokens: bfloat16 [10240, 2048], P('ep'), may hold values from -12 to 12, as said below
- cotangent: bfloat16 [10240, 2048], P('ep'), may hold values from -0.59765625 to 0.59765625
- route_ids: int32 [10240, 2], P('ep'), may hold values from 0 to 31, all different within a row; in each aligned block of 320 rows (0 to 319, 320 to 639, ...) at most 40 rows name the same one
- route_weights: bfloat16 [10240, 2], P('ep'), may hold values from 0.049804688 to 1
- w_gate: bfloat16 [32, 2048, 2048], P('ep', None, 'tp'), may hold values from -0.125 to 0.125
- w_up: bfloat16 [32, 2048, 2048], P('ep', None, 'tp'), may hold values from -0.125 to 0.125
- w_down: bfloat16 [32, 2048, 2048], P('ep', 'tp'), may hold values from -0.125 to 0.125
- dense_in: bfloat16 [2048, 256], P(('ep', 'tp')), may hold values from -0.125 to 0.125
- dense_out: bfloat16 [2048, 256], P(('ep', 'tp')), may hold values from -0.375 to 0.375
- dense_gate: bfloat16 [2048], replicated, may hold values from -0.125 to 0.125
Outputs:
- grad_tokens: bfloat16 [10240, 2048], P('ep', 'tp')
- grad_route_weights: bfloat16 [10240, 2], P('ep')
- grad_gate: float32 [32, 2048, 2048], P('ep', None, 'tp')
- grad_up: float32 [32, 2048, 2048], P('ep', None, 'tp')
- grad_down: float32 [32, 2048, 2048], P('ep', 'tp')
- grad_dense_in: float32 [2048, 256], P(('ep', 'tp'))
- grad_dense_out: float32 [2048, 256], P(('ep', 'tp'))
- grad_dense_gate: float32 [2048], P(('ep', 'tp'))
Inputs may be any that keep to these rules, and one draw needn't show every extreme that they name: `route_ids`: each row names 2 different experts; among the rows of one index of ep no expert is named more than 40 times, and that count is reached. `tokens`: rows carry scales between 0.5 and 2 that differ from row to row.
All inputs are finite; a program needn't handle non-finite values.
Results may differ from a plain program's by a relative error of at most 0.01.
Values may be sent and summed in bfloat16 or wider, within the bound.
No kernel may reach another device: no remote copies, remote signals or barrier semaphores. Data moves between devices by JAX's collectives and lax.ppermute only.
A program may use at most 128 MiB of HBM per device.

v0:
```python
import math

import jax
import jax.numpy as jnp
from jax import lax
from jax.sharding import PartitionSpec as P

CLAMP_LIMIT = 7.0
SIG_SLOPE = 1.702


def in_blocks(shard, dim, size):
    dims = shard.shape
    pieces = shard.reshape(*dims[:dim], size, dims[dim] // size, *dims[dim + 1 :])
    return jnp.moveaxis(pieces, dim, 0)


def summed_on_arrival(shard, axis, dim):
    pieces = in_blocks(shard, dim, lax.axis_size(axis))
    arrived = lax.all_to_all(pieces, axis, split_axis=0, concat_axis=0, tiled=True)
    return arrived.astype(jnp.float32).sum(axis=0)


def copy_for_each(shard, axis):
    copies = jnp.broadcast_to(shard, (lax.axis_size(axis), *shard.shape))
    return lax.all_to_all(copies, axis, split_axis=0, concat_axis=0, tiled=True)


def over_copies(shard, axis):
    return copy_for_each(shard, axis).sum(axis=0)


def in_one_piece(arrays, axis, split_dim, concat_dim, along):
    widths = [math.prod(a.shape[along:]) for a in arrays]
    both = jnp.concatenate(
        [a.reshape(*a.shape[:along], w) for a, w in zip(arrays, widths)], axis=along
    )
    result = lax.all_to_all(both, axis, split_axis=split_dim, concat_axis=concat_dim, tiled=True)
    pieces = jnp.split(result, [sum(widths[:k]) for k in range(1, len(widths))], axis=along)
    return tuple(
        (b.reshape(*result.shape[:along], *a.shape[along:]) for a, b in zip(arrays, pieces))
    )


def in_one_piece_2(arrays, axis, dim, along):
    ends, at = ([], 0)
    for a in arrays[:-1]:
        at += a.shape[along]
        ends.append(at)
    both = jnp.concatenate(arrays, axis=along)
    return tuple(jnp.split(lax.all_gather(both, axis, axis=dim, tiled=True), ends, axis=along))


def sent_together(arrays, axis, dim, along):
    widths = [math.prod(a.shape[along:]) for a in arrays]
    both = jnp.concatenate(
        [a.reshape(*a.shape[:along], w) for a, w in zip(arrays, widths)], axis=along
    )
    result = lax.psum_scatter(both, axis, scatter_dimension=dim, tiled=True)
    pieces = jnp.split(result, [sum(widths[:k]) for k in range(1, len(widths))], axis=along)
    return tuple(
        (b.reshape(*result.shape[:along], *a.shape[along:]) for a, b in zip(arrays, pieces))
    )


def shards(
    tokens,
    cotangent,
    route_ids,
    route_weights,
    w_gate,
    w_up,
    w_down,
    dense_in,
    dense_out,
    dense_gate,
):
    count_ep = lax.axis_size("ep")
    count_tp = lax.axis_size("tp")
    tp_index = lax.axis_index("tp")
    tok_dev, model_width = tokens.shape
    top_k = route_ids.shape[1]
    col_count = model_width // count_tp
    capacity = 2 * tok_dev * top_k // count_ep
    assigns = tok_dev * top_k
    slot_total = count_ep * capacity
    flat_ids = route_ids.reshape(-1)
    one_hot = (flat_ids[:, None] == jnp.arange(count_ep, dtype=jnp.int32)[None, :]).astype(
        jnp.int32
    )
    earlier = jnp.cumsum(one_hot, axis=0) - one_hot
    slot_index = jnp.sum(earlier * one_hot, axis=1)
    target = flat_ids * capacity + slot_index
    matches = target[None, :] == jnp.arange(slot_total, dtype=jnp.int32)[:, None]
    filled = jnp.any(matches, axis=1)
    source = jnp.sum(jnp.where(matches, jnp.arange(assigns, dtype=jnp.int32)[None, :], 0), axis=1)
    token_of = source // top_k
    x_rows = jnp.where(filled[:, None], tokens[token_of], jnp.zeros((), jnp.bfloat16)).reshape(
        count_ep, capacity, model_width
    )
    dy_rows = jnp.where(filled[:, None], cotangent[token_of], jnp.zeros((), jnp.bfloat16)).reshape(
        count_ep, capacity, model_width
    )
    weight_rows = jnp.where(
        filled, route_weights.reshape(-1)[source], jnp.zeros((), jnp.bfloat16)
    ).reshape(count_ep, capacity)
    x_in, dy_in, weight_in = (
        lax.all_to_all(x_rows, "ep", split_axis=0, concat_axis=0, tiled=True),
        lax.all_to_all(dy_rows, "ep", split_axis=0, concat_axis=0, tiled=True),
        lax.all_to_all(weight_rows, "ep", split_axis=0, concat_axis=0, tiled=True),
    )
    x_slots = x_in.reshape(slot_total, model_width)
    dy_slots = dy_in.reshape(slot_total, model_width)
    route_col = weight_in.reshape(slot_total, 1).astype(jnp.float32)
    gate_w = w_gate[0]
    up_w = w_up[0]
    down_w = w_down[0]
    gate_pre = jnp.dot(x_slots, gate_w, preferred_element_type=jnp.float32)
    up_pre = jnp.dot(x_slots, up_w, preferred_element_type=jnp.float32)
    gate_clamp = jnp.minimum(gate_pre, CLAMP_LIMIT)
    up_clamp = jnp.clip(up_pre, -CLAMP_LIMIT, CLAMP_LIMIT)
    sig = jax.nn.sigmoid(SIG_SLOPE * gate_clamp)
    act = (gate_clamp * sig * (up_clamp + 1.0)).astype(jnp.bfloat16)
    back = lax.dot_general(
        dy_slots, down_w, (((1,), (1,)), ((), ())), preferred_element_type=jnp.float32
    )
    d_act = route_col * back
    d_gate = jnp.where(
        gate_pre < CLAMP_LIMIT,
        d_act * (up_clamp + 1.0) * (sig + SIG_SLOPE * gate_clamp * sig * (1.0 - sig)),
        0.0,
    ).astype(jnp.bfloat16)
    d_up = jnp.where(jnp.abs(up_pre) < CLAMP_LIMIT, d_act * gate_clamp * sig, 0.0).astype(
        jnp.bfloat16
    )
    scaled_cot = (route_col * dy_slots.astype(jnp.float32)).astype(jnp.bfloat16)
    contract_rows = (((0,), (0,)), ((), ()))
    grad_gate = lax.dot_general(x_slots, d_gate, contract_rows, preferred_element_type=jnp.float32)
    grad_up = lax.dot_general(x_slots, d_up, contract_rows, preferred_element_type=jnp.float32)
    grad_down = lax.dot_general(act, scaled_cot, contract_rows, preferred_element_type=jnp.float32)
    contract_cols = (((1,), (1,)), ((), ()))
    row_partial = lax.dot_general(d_gate, gate_w, contract_cols, preferred_element_type=jnp.float32)
    row_partial = row_partial + lax.dot_general(
        d_up, up_w, contract_cols, preferred_element_type=jnp.float32
    )
    row_cols = summed_on_arrival(
        row_partial.reshape(count_ep, capacity, model_width).astype(jnp.bfloat16), "tp", 2
    ).astype(jnp.bfloat16)
    weight_grad = over_copies(jnp.sum(act.astype(jnp.float32) * back, axis=1), "tp").astype(
        jnp.bfloat16
    )
    back_rows, back_weights = in_one_piece(
        (row_cols, weight_grad.reshape(count_ep, capacity)), "ep", 0, 0, 2
    )
    expert_dx = (
        back_rows.reshape(slot_total, col_count)[target]
        .astype(jnp.float32)
        .reshape(tok_dev, top_k, col_count)
    )
    expert_dx = jnp.sum(expert_dx, axis=1)
    grad_route_weights = back_weights.reshape(-1)[target].reshape(tok_dev, top_k)
    in_whole, out_whole = in_one_piece_2((dense_in, dense_out), ("ep", "tp"), 0, 1)
    dense_pre = jnp.dot(tokens, in_whole, preferred_element_type=jnp.float32)
    dense_act = jax.nn.silu(dense_pre).astype(jnp.bfloat16)
    dense_val = lax.dot_general(
        dense_act, out_whole, contract_cols, preferred_element_type=jnp.float32
    )
    mix = jax.nn.sigmoid(jnp.dot(tokens, dense_gate, preferred_element_type=jnp.float32))
    cot_wide = cotangent.astype(jnp.float32)
    dense_scaled = (mix[:, None] * cot_wide).astype(jnp.bfloat16)
    dense_back = jnp.dot(dense_scaled, out_whole, preferred_element_type=jnp.float32)
    sig_pre = jax.nn.sigmoid(dense_pre)
    dense_dpre = (dense_back * sig_pre * (1.0 + dense_pre * (1.0 - sig_pre))).astype(jnp.bfloat16)
    dlogit = mix * (1.0 - mix) * jnp.sum(cot_wide * dense_val, axis=1)
    in_rows = lax.dynamic_slice_in_dim(in_whole, tp_index * col_count, col_count, 0)
    gate_cols = lax.dynamic_slice_in_dim(dense_gate, tp_index * col_count, col_count, 0)
    dense_dx = lax.dot_general(
        dense_dpre, in_rows, contract_cols, preferred_element_type=jnp.float32
    )
    dense_dx = dense_dx + dlogit[:, None] * gate_cols.astype(jnp.float32)[None, :]
    grad_tokens = (dense_dx + expert_dx).astype(jnp.bfloat16)
    block_cols = model_width // (count_ep * count_tp)
    tokens_own = lax.dynamic_index_in_dim(
        tokens.reshape(tok_dev, count_ep, count_tp, block_cols), tp_index, 2, keepdims=False
    ).reshape(tok_dev, count_ep * block_cols)
    scaled_own = lax.dynamic_index_in_dim(
        dense_scaled.reshape(tok_dev, count_ep, count_tp, block_cols), tp_index, 2, keepdims=False
    ).reshape(tok_dev, count_ep * block_cols)
    in_partial = lax.dot_general(
        tokens_own, dense_dpre, contract_rows, preferred_element_type=jnp.float32
    )
    out_partial = lax.dot_general(
        scaled_own, dense_act, contract_rows, preferred_element_type=jnp.float32
    )
    gate_partial = jnp.sum(tokens_own.astype(jnp.float32) * dlogit[:, None], axis=0)
    grad_dense_in, grad_dense_out, grad_dense_gate = sent_together(
        (in_partial, out_partial, gate_partial), "ep", 0, 1
    )
    return (
        grad_tokens,
        grad_route_weights,
        grad_gate[None],
        grad_up[None],
        grad_down[None],
        grad_dense_in,
        grad_dense_out,
        grad_dense_gate,
    )


def solution(mesh):
    placed = (
        P("ep", None),
        P("ep", None),
        P("ep", None),
        P("ep", None),
        P("ep", None, "tp"),
        P("ep", None, "tp"),
        P("ep", "tp", None),
        P(("ep", "tp"), None),
        P(("ep", "tp"), None),
        P(),
    )
    return jax.shard_map(
        shards,
        mesh=mesh,
        in_specs=placed,
        out_specs=(
            P("ep", "tp"),
            P("ep", None),
            P("ep", None, "tp"),
            P("ep", None, "tp"),
            P("ep", "tp", None),
            P(("ep", "tp"), None),
            P(("ep", "tp"), None),
            P(("ep", "tp")),
        ),
        check_vma=False,
    )
```

profile of v0, /device:TPU:0, one launch (start us, length us, event | category | flops | bytes accessed | tf_op | source)
XLA Modules:
  0.0 373.8 jit_solution(14015148685177293900)
XLA Ops:
  17.0 8.0 %gather_fusion.1 = bf16[1280]{0:T(1024)(128)(2,1)S(1)} fusion(bf16[640]{0:T(1024)(128)(2,1)S(1)} %reshape.261, s32[2048]{0:T(1024)S(1)} %get-tuple-element.64), kind=kCustom, calls=%fused_computation.1 | custom fusion | bytes 10240 | tf_op jit(solution)/shard_map/gather | solution.py:105
  25.7 8.4 %all-to-all-start.1 = ((bf16[32,1,40]{2,1,0:T(2,128)(2,1)}), bf16[32,1,40]{2,1,0:T(2,128)(2,1)S(1)}, u32[]{:S(2)}, u32[]{:S(2)}) async-start(bf16[32,1,40]{2,1,0:T(2,128)(2,1)} %select_n.101), calls=%async_computation.1 | async-start | bytes 32768 | tf_op jit(solution)/shard_map/all_to_all | solution.py:110
  34.3 6.1 %gather_fusion = bf16[1280,2048]{1,0:T(8,128)(2,1)} fusion(bf16[320,2048]{1,0:T(8,128)(2,1)S(1)} %copy-done.2, s32[2048]{0:T(1024)S(1)} %get-tuple-element.65), kind=kCustom, calls=%fused_computation | custom fusion | bytes 10490880 | tf_op jit(solution)/shard_map/gather | solution.py:98
  40.4 12.3 %gather_fusion.2 = bf16[1280,2048]{1,0:T(8,128)(2,1)} fusion(bf16[320,2048]{1,0:T(8,128)(2,1)} %param.11, s32[2048]{0:T(1024)S(1)} %get-tuple-element.65), kind=kCustom, calls=%fused_computation.2 | custom fusion | bytes 10490880 | tf_op jit(solution)/shard_map/gather | solution.py:101
  52.7 8.8 %broadcast_select_fusion.1 = (bf16[32,40,2048]{2,1,0:T(8,128)(2,1)}, bf16[32,40,2048]{2,1,0:T(8,128)(2,1)}) fusion(bf16[32,40,2048]{2,1,0:T(8,128)(2,1)} %bitcast.77, pred[32,40]{1,0:T(8,128)(4,1)S(1)} %broadcast_in_dim.66, bf16[32,40,2048]{2,1,0:T(8,128)(2,1)} %bitcast.78), kind=kLoop, calls=%fused_computation.11 | loop fusion | flops 5242880 | bytes 20972800 | tf_op jit(solution)/shard_map/jit(_where)/select_n | solution.py:98
  61.5 69.6 %all_to_all.32 = bf16[32,40,2048]{2,1,0:T(8,128)(2,1)} all-to-all(bf16[32,40,2048]{2,1,0:T(8,128)(2,1)} %get-tuple-element.60), channel_id=1, replica_groups=mesh['ep'=32,'tp'=4] {'ep'}, dimensions={0} | all-to-all | bytes 10485760 | tf_op jit(solution)/shard_map/all_to_all | solution.py:108
  131.1 5.0 %all-to-all-start.2 = ((bf16[32,40,2048]{2,1,0:T(8,128)(2,1)}), bf16[32,40,2048]{2,1,0:T(8,128)(2,1)}, u32[]{:S(2)}, u32[]{:S(2)}) async-start(bf16[32,40,2048]{2,1,0:T(8,128)(2,1)} %get-tuple-element.61), calls=%async_computation.2 | async-start | bytes 10485760 | tf_op jit(solution)/shard_map/all_to_all | solution.py:109
  137.5 7.6 %fusion.12 = f32[1280,512]{0,1:T(8,128)} fusion(bf16[1280,2048]{1,0:T(8,128)(2,1)} %bitcast.79, bf16[1,2048,512]{2,1,0:T(8,128)(2,1)} %param.14), kind=kOutput, calls=%fused_computation.35 | convolution fusion | flops 2684354560 | bytes 9961472 | tf_op jit(solution)/shard_map/dot_general | solution.py:118
  145.1 57.1 %all-to-all-done.2 = bf16[32,40,2048]{2,1,0:T(8,128)(2,1)} async-done(((bf16[32,40,2048]{2,1,0:T(8,128)(2,1)}), bf16[32,40,2048]{2,1,0:T(8,128)(2,1)}, u32[]{:S(2)}, u32[]{:S(2)}) %all-to-all-start.2) | async-done | bytes 5242912 | tf_op jit(solution)/shard_map/all_to_all | solution.py:109
  202.2 6.2 %fusion.8 = f32[1280,512]{0,1:T(8,128)S(1)} fusion(bf16[1280,2048]{1,0:T(8,128)(2,1)} %bitcast.6, bf16[1,512,2048]{2,1,0:T(8,128)(2,1)} %param.16), kind=kOutput, calls=%fused_computation.31 | convolution fusion | flops 2684354560 | bytes 9961472 | tf_op jit(solution)/shard_map/dot_general | solution.py:124
  208.5 6.8 %select_convert_fusion = (bf16[1280,512]{0,1:T(8,128)(2,1)}, bf16[1280,512]{0,1:T(8,128)(2,1)}, f32[1280]{0:T(1024)S(1)}, bf16[1280,512]{0,1:T(8,128)(2,1)}) fusion(f32[1280,512]{0,1:T(8,128)S(1)} %copy-done.19, f32[1280,512]{0,1:T(8,128)S(1)} %fusion.8, f32[1280]{0:T(1024)S(1)} %reshape.271, bf16[1280,2048]{1,0:T(8,128)(2,1)S(1)} %bitcast.82, ...), kind=kOutput, calls=%fused_computation.23 | convolution fusion | flops 2703358720 | bytes 16525312 | tf_op jit(solution)/shard_map/dot_general | solution.py:119
  215.9 4.5 %all-to-all-start.4 = ((f32[4,1,1280]{2,1,0:T(1,128)}), f32[4,1,1280]{2,1,0:T(1,128)S(1)}, u32[]{:S(2)}, u32[]{:S(2)}) async-start(f32[4,1,1280]{2,1,0:T(1,128)} %broadcast_in_dim.73), calls=%async_computation.4 | async-start | bytes 40960 | tf_op jit(solution)/shard_map/all_to_all | solution.py:26
  220.4 5.2 %fusion.10 = f32[1280,2048]{1,0:T(8,128)S(1)} fusion(bf16[1280,512]{0,1:T(8,128)(2,1)} %get-tuple-element.55, bf16[1,2048,512]{2,1,0:T(8,128)(2,1)} %param.14), kind=kOutput, calls=%fused_computation.33 | convolution fusion | flops 2684354560 | bytes 13893632 | tf_op jit(solution)/shard_map/dot_general | solution.py:142
  225.6 4.8 %add_convert_fusion = bf16[1280,2048]{1,0:T(8,128)(2,1)} fusion(f32[1280,2048]{1,0:T(8,128)S(1)} %fusion.10, bf16[1280,512]{0,1:T(8,128)(2,1)S(1)} %copy-done.17, bf16[1,2048,512]{2,1,0:T(8,128)(2,1)S(1)} %copy-done), kind=kOutput, calls=%fused_computation.6 | convolution fusion | flops 2689597440 | bytes 19136512 | tf_op jit(solution)/shard_map/dot_general | solution.py:143
  230.4 9.5 %convert_element_type.99 = bf16[32,40,4,512]{3,2,1,0:T(4,128)(2,1)} reshape(bf16[1280,2048]{1,0:T(8,128)(2,1)} %add_convert_fusion) | data formatting | bytes 10485760 | tf_op jit(solution)/shard_map/convert_element_type | solution.py:147
  239.9 5.9 %copy.84 = bf16[32,40,4,512]{3,1,0,2:T(8,128)(2,1)} copy(bf16[32,40,4,512]{3,2,1,0:T(4,128)(2,1)} %convert_element_type.99) | data formatting | bytes 10485760 | tf_op jit(solution)/shard_map/convert_element_type | solution.py:147
  245.8 5.2 %all-to-all-start.3 = ((bf16[4,32,40,512]{3,2,1,0:T(8,128)(2,1)}), bf16[4,32,40,512]{3,2,1,0:T(8,128)(2,1)}, u32[]{:S(2)}, u32[]{:S(2)}) async-start(bf16[4,32,40,512]{3,2,1,0:T(8,128)(2,1)} %bitcast.76), calls=%async_computation.3 | async-start | bytes 10485760 | tf_op jit(solution)/shard_map/all_to_all | solution.py:20
  267.0 7.0 %convolution_bitcast_fusion = f32[1,2048,512]{2,1,0:T(8,128)} fusion(bf16[1280,2048]{1,0:T(8,128)(2,1)} %bitcast.80, bf16[1280,512]{0,1:T(8,128)(2,1)S(1)} %copy-done.18), kind=kOutput, calls=%fused_computation.18 | convolution fusion | flops 2684354560 | bytes 10747904 | tf_op jit(solution)/shard_map/dot_general | solution.py:139
  274.7 32.6 %all-to-all-done.3 = bf16[4,32,40,512]{3,2,1,0:T(8,128)(2,1)} async-done(((bf16[4,32,40,512]{3,2,1,0:T(8,128)(2,1)}), bf16[4,32,40,512]{3,2,1,0:T(8,128)(2,1)}, u32[]{:S(2)}, u32[]{:S(2)}) %all-to-all-start.3) | async-done | bytes 5242912 | tf_op jit(solution)/shard_map/all_to_all | solution.py:20
  312.6 7.2 %all-to-all-start.5 = ((bf16[32,40,513]{2,1,0:T(8,128)(2,1)}), bf16[32,40,513]{2,1,0:T(8,128)(2,1)S(1)}, u32[]{:S(2)}, u32[]{:S(2)}) async-start(bf16[32,40,513]{2,1,0:T(8,128)(2,1)} %pad_maximum_fusion), calls=%async_computation.5 | async-start | bytes 3276800 | tf_op jit(solution)/shard_map/all_to_all | solution.py:38
  319.8 7.2 %convolution_bitcast_fusion.1 = f32[1,2048,512]{2,1,0:T(8,128)} fusion(bf16[1280,2048]{1,0:T(8,128)(2,1)} %bitcast.81, bf16[1280,512]{0,1:T(8,128)(2,1)S(1)} %copy-done.14), kind=kOutput, calls=%fused_computation.19 | convolution fusion | flops 2684354560 | bytes 10747904 | tf_op jit(solution)/shard_map/dot_general | solution.py:138
  327.0 7.1 %fusion.3 = f32[1,512,2048]{2,1,0:T(8,128)} fusion(bf16[1280,512]{0,1:T(8,128)(2,1)S(1)} %copy-done.20, bf16[1280,2048]{1,0:T(8,128)(2,1)} %bitcast.6, f32[1280]{0:T(1024)S(1)} %reshape.271), kind=kOutput, calls=%fused_computation.17 | convolution fusion | flops 2692218880 | bytes 10753024 | tf_op jit(solution)/shard_map/dot_general | solution.py:140
  334.1 12.2 %reduce-scatter.4.cloned.1.call-done = f32[16,513]{1,0:T(8,128)} async-done(((f32[512,513]{1,0:T(8,128)}), f32[16,513]{1,0:T(8,128)}) %reduce-scatter.4.cloned.1.call-update) | async-done | bytes 32848
  359.5 4.3 %gather_fusion.4 = bf16[640]{0:T(1024)(128)(2,1)S(1)} fusion(bf16[1280]{0:T(1024)(128)(2,1)S(1)} %reshape_reshape.4, s32[1024]{0:T(1024)S(1)} %pad_clamp_fusion.2), kind=kCustom, calls=%fused_computation.4 | custom fusion | bytes 5120 | tf_op jit(solution)/shard_map/gather | solution.py:161
  (111 shorter events, 50.4 us)
Async XLA Ops:
  7.2 201.3 %copy-start = (bf16[1,2048,512]{2,1,0:T(8,128)(2,1)S(1)}, bf16[1,2048,512]{2,1,0:T(8,128)(2,1)}, u32[]{:S(2)}) copy-start(bf16[1,2048,512]{2,1,0:T(8,128)(2,1)} %param.15) | copy-start | bytes 6291460
  8.8 25.4 %copy-start.2 = (bf16[320,2048]{1,0:T(8,128)(2,1)S(1)}, bf16[320,2048]{1,0:T(8,128)(2,1)}, u32[]{:S(2)}) copy-start(bf16[320,2048]{1,0:T(8,128)(2,1)} %param.10) | copy-start | bytes 3932164
  25.7 35.8 %all-to-all-start.1 = ((bf16[32,1,40]{2,1,0:T(2,128)(2,1)}), bf16[32,1,40]{2,1,0:T(2,128)(2,1)S(1)}, u32[]{:S(2)}, u32[]{:S(2)}) async-start(bf16[32,1,40]{2,1,0:T(2,128)(2,1)} %select_n.101), calls=%async_computation.1 | async-start | bytes 32768 | tf_op jit(solution)/shard_map/all_to_all | solution.py:110
  131.1 5.6 %copy-start.11 = (bf16[16,256]{1,0:T(8,128)(2,1)S(1)}, bf16[16,256]{1,0:T(8,128)(2,1)}, u32[]{:S(2)}) copy-start(bf16[16,256]{1,0:T(8,128)(2,1)} %param.18) | copy-start | bytes 24580
  131.1 5.6 %copy-start.12 = (bf16[16,256]{1,0:T(8,128)(2,1)S(1)}, bf16[16,256]{1,0:T(8,128)(2,1)}, u32[]{:S(2)}) copy-start(bf16[16,256]{1,0:T(8,128)(2,1)} %param.17) | copy-start | bytes 24580
  131.1 71.1 %all-to-all-start.2 = ((bf16[32,40,2048]{2,1,0:T(8,128)(2,1)}), bf16[32,40,2048]{2,1,0:T(8,128)(2,1)}, u32[]{:S(2)}, u32[]{:S(2)}) async-start(bf16[32,40,2048]{2,1,0:T(8,128)(2,1)} %get-tuple-element.61), calls=%async_computation.2 | async-start | bytes 10485760 | tf_op jit(solution)/shard_map/all_to_all | solution.py:109
  136.1 117.6 %all-gather.2.cloned.1.call-start = ((), (), s32[]{:S(2)}) async-start(), calls=%async_computation.7 | async-start | bytes 2113536 | tf_op jit(solution)/shard_map/all_gather | solution.py:51
  202.2 6.2 %copy-start.5 = (bf16[32,40,2048]{2,1,0:T(8,128)(2,1)S(1)}, bf16[32,40,2048]{2,1,0:T(8,128)(2,1)}, u32[]{:S(2)}) copy-start(bf16[32,40,2048]{2,1,0:T(8,128)(2,1)} %all_to_all.32) | copy-start | bytes 15728644
  202.2 6.2 %copy-start.19 = (f32[1280,512]{0,1:T(8,128)S(1)}, f32[1280,512]{0,1:T(8,128)}, u32[]{:S(2)}) copy-start(f32[1280,512]{0,1:T(8,128)} %fusion.12) | copy-start | bytes 7864324
  215.9 29.9 %all-to-all-start.4 = ((f32[4,1,1280]{2,1,0:T(1,128)}), f32[4,1,1280]{2,1,0:T(1,128)S(1)}, u32[]{:S(2)}, u32[]{:S(2)}) async-start(f32[4,1,1280]{2,1,0:T(1,128)} %broadcast_in_dim.73), calls=%async_computation.4 | async-start | bytes 40960 | tf_op jit(solution)/shard_map/all_to_all | solution.py:26
  220.3 5.2 %copy-start.17 = (bf16[1280,512]{0,1:T(8,128)(2,1)S(1)}, bf16[1280,512]{0,1:T(8,128)(2,1)}, u32[]{:S(2)}) copy-start(bf16[1280,512]{0,1:T(8,128)(2,1)} %get-tuple-element.54) | copy-start | bytes 3932164
  245.8 5.5 %copy-start.10 = (s32[320,2]{0,1:T(2,128)S(1)}, s32[320,2]{0,1:T(2,128)}, u32[]{:S(2)}) copy-start(s32[320,2]{0,1:T(2,128)} %param.12) | copy-start | bytes 7684
  245.8 61.4 %all-to-all-start.3 = ((bf16[4,32,40,512]{3,2,1,0:T(8,128)(2,1)}), bf16[4,32,40,512]{3,2,1,0:T(8,128)(2,1)}, u32[]{:S(2)}, u32[]{:S(2)}) async-start(bf16[4,32,40,512]{3,2,1,0:T(8,128)(2,1)} %bitcast.76), calls=%async_computation.3 | async-start | bytes 10485760 | tf_op jit(solution)/shard_map/all_to_all | solution.py:20
  251.0 95.3 %reduce-scatter.4.cloned.1.call-start = ((), (), s32[]{:S(2)}) async-start(), calls=%async_computation.8 | async-start | bytes 1351680
  253.3 2.4 copy-start.3
  256.8 3.9 %copy-start.16 = (f32[320,256]{1,0:T(8,128)S(1)}, f32[320,256]{1,0:T(8,128)}, u32[]{:S(2)}) copy-start(f32[320,256]{1,0:T(8,128)} %copy-done.15) | copy-start | bytes 983044
  262.4 2.3 copy-start.7
  263.2 3.8 %copy-start.18 = (bf16[1280,512]{0,1:T(8,128)(2,1)S(1)}, bf16[1280,512]{0,1:T(8,128)(2,1)}, u32[]{:S(2)}) copy-start(bf16[1280,512]{0,1:T(8,128)(2,1)} %get-tuple-element.54) | copy-start | bytes 3932164
  312.6 7.2 %copy-start.14 = (bf16[1280,512]{0,1:T(8,128)(2,1)S(1)}, bf16[1280,512]{0,1:T(8,128)(2,1)}, u32[]{:S(2)}) copy-start(bf16[1280,512]{0,1:T(8,128)(2,1)} %get-tuple-element.55) | copy-start | bytes 3932164
  312.6 36.3 %all-to-all-start.5 = ((bf16[32,40,513]{2,1,0:T(8,128)(2,1)}), bf16[32,40,513]{2,1,0:T(8,128)(2,1)S(1)}, u32[]{:S(2)}, u32[]{:S(2)}) async-start(bf16[32,40,513]{2,1,0:T(8,128)(2,1)} %pad_maximum_fusion), calls=%async_computation.5 | async-start | bytes 3276800 | tf_op jit(solution)/shard_map/all_to_all | solution.py:38
  319.8 7.2 %copy-start.20 = (bf16[1280,512]{0,1:T(8,128)(2,1)S(1)}, bf16[1280,512]{0,1:T(8,128)(2,1)}, u32[]{:S(2)}) copy-start(bf16[1280,512]{0,1:T(8,128)(2,1)} %get-tuple-element.57) | copy-start | bytes 3932164
  353.4 13.2 %copy-start.1 = (bf16[1,2048,512]{2,1,0:T(8,128)(2,1)S(1)}, bf16[1,2048,512]{2,1,0:T(8,128)(2,1)}, u32[]{:S(2)}) copy-start(bf16[1,2048,512]{2,1,0:T(8,128)(2,1)} %param.15) | copy-start | bytes 6291460
  358.1 6.6 %copy-start.6 = (f32[320,512]{1,0:T(8,128)S(1)}, f32[320,512]{1,0:T(8,128)}, u32[]{:S(2)}) copy-start(f32[320,512]{1,0:T(8,128)} %reduce_sum.87) | copy-start | bytes 1966084
  358.1 6.6 %copy-start.8 = (bf16[320,256]{1,0:T(8,128)(2,1)S(1)}, bf16[320,256]{1,0:T(8,128)(2,1)}, u32[]{:S(2)}) copy-start(bf16[320,256]{1,0:T(8,128)(2,1)} %copy-done.7) | copy-start | bytes 491524
  (4 other events, 6.1 us)
Sparse Core Ops, SparseCore 0:
  140.5 91.2 all-gather.1
  264.9 81.3 reduce-scatter.3
where the time goes:
time: 381 us; the launch traced here: 374 us
  waiting for transfers between devices  102 us (27%)
  local copies, waits for them, and re-layouts  73.4 us (19%)
  blocking collectives  69.6 us (18%)
  matrix products  59.3 us (16%)
  starting transfers between devices  31.1 us (8%)
  other arithmetic  23.6 us (6%)
  between operations  14.8 us (4%)
    all_to_all x1, blocking collectives, shards(): lax.all_to_all(x_rows, 'ep', split_axis=0, concat_axis=0, tiled=True)  69.6 us
    all_to_all x1, waiting for transfers between devices, shards(): lax.all_to_all(dy_rows, 'ep', split_axis=0, concat_axis=0, tiled=True)  57.1 us
    all_to_all x1, waiting for transfers between devices, summed_on_arrival(): lax.all_to_all(pieces, axis, split_axis=0, concat_axis=0, tiled=True)  32.6 us
    convert_element_type x2, local copies, waits for them, and re-layouts, shards(): row_partial.reshape(count_ep, capacity, model_width).astype(jnp.bfloat16)  15.4 us
    gather x1, local copies, waits for them, and re-layouts, shards(): cotangent[token_of]  12.3 us
    unnamed x3, waiting for transfers between devices  12.2 us
    select_n x1, other arithmetic, shards(): jnp.where(filled[:, None], tokens[token_of], jnp.zeros((), jnp.bfloat16))  8.76 us
    all_to_all x1, starting transfers between devices, shards(): lax.all_to_all(weight_rows, 'ep', split_axis=0, concat_axis=0, tiled=True)  8.44 us
  transfers between devices with their start and end apart: 7, of which 3 were waited for; matrix products, arithmetic and copies ran while one was open for 32% of the time, Pallas kernels for 0%

commit v1 on v0

v1 whole, which is shorter than its diff:
```python
import jax
import jax.numpy as jnp
from jax import lax
from jax.sharding import PartitionSpec as P

CLAMP_LIMIT = 7.0
SIG_SLOPE = 1.702
F32 = jnp.float32
BF16 = jnp.bfloat16
COLS = (((1,), (1,)), ((), ()))
ROWS = (((0,), (0,)), ((), ()))


def mm(a, b, dims=(((1,), (0,)), ((), ()))):
    return lax.dot_general(a, b, dims, preferred_element_type=F32)


def shards(
    tokens,
    cotangent,
    route_ids,
    route_weights,
    w_gate,
    w_up,
    w_down,
    dense_in,
    dense_out,
    dense_gate,
):
    n_ep = lax.axis_size("ep")
    n_tp = lax.axis_size("tp")
    tp = lax.axis_index("tp")
    tok, width = tokens.shape
    top = route_ids.shape[1]
    cap = 2 * tok * top // n_ep
    slots = n_ep * cap
    quarter = width // n_tp
    up = [(k, (k + 1) % n_tp) for k in range(n_tp)]
    down = [(k, (k - 1) % n_tp) for k in range(n_tp)]
    own, nxt, prv, far = tp, (tp + 1) % n_tp, (tp + 3) % n_tp, (tp + 2) % n_tp

    def cols(a, q):
        return lax.dynamic_slice_in_dim(a, q * quarter, quarter, 1)

    def rows(a, q):
        return lax.dynamic_slice_in_dim(a, q * quarter, quarter, 0)

    def exchange(a):
        return lax.all_to_all(a, "ep", split_axis=0, concat_axis=0, tiled=True)

    ids = route_ids.T
    wts = route_weights.T
    experts = lax.broadcasted_iota(jnp.int32, (n_ep, tok), 0)
    picks = [ids[k][None, :] == experts for k in range(top)]
    named = picks[0] | picks[1]
    earlier = (
        lax.broadcasted_iota(jnp.int32, (tok, tok), 0)
        < lax.broadcasted_iota(jnp.int32, (tok, tok), 1)
    ).astype(BF16)
    rank = mm(named.astype(BF16), earlier).astype(jnp.int32)
    key = jnp.where(named, rank, -1)
    hit = key[:, None, :] == lax.broadcasted_iota(jnp.int32, (n_ep, cap, tok), 1)
    place = hit.astype(BF16).reshape(slots, tok)
    share = jnp.where(picks[0], wts[0][None, :], 0) + jnp.where(picks[1], wts[1][None, :], 0)
    place_w = jnp.where(hit, share.astype(BF16)[:, None, :], 0).astype(BF16).reshape(slots, tok)

    def pair(a):
        return jnp.concatenate([cols(a, own), cols(a, nxt)], axis=1)

    x_send = mm(place, pair(tokens)).astype(BF16).reshape(n_ep, cap, 2 * quarter)
    y_send = mm(place_w, pair(cotangent)).astype(BF16).reshape(n_ep, cap, 2 * quarter)
    x_got = exchange(x_send).reshape(slots, 2 * quarter)
    y_got = exchange(y_send).reshape(slots, 2 * quarter)

    def whole(got):
        a, b = got[:, :quarter], got[:, quarter:]
        c = lax.ppermute(a, "tp", up)
        d = lax.ppermute(b, "tp", down)
        full = jnp.zeros((slots, width), BF16)
        for piece, q in ((a, own), (b, nxt), (c, prv), (d, far)):
            full = lax.dynamic_update_slice_in_dim(full, piece, q * quarter, 1)
        return full

    x_slots = whole(x_got)
    y_slots = whole(y_got)
    gate_w, up_w, down_w = w_gate[0], w_up[0], w_down[0]
    gate_pre = mm(x_slots, gate_w)
    up_pre = mm(x_slots, up_w)
    gate_clamp = jnp.minimum(gate_pre, CLAMP_LIMIT)
    up_clamp = jnp.clip(up_pre, -CLAMP_LIMIT, CLAMP_LIMIT)
    sig = jax.nn.sigmoid(SIG_SLOPE * gate_clamp)
    glu = gate_clamp * sig
    act = (glu * (up_clamp + 1.0)).astype(BF16)
    to_gate = jnp.where(
        gate_pre < CLAMP_LIMIT,
        (up_clamp + 1.0) * (sig + SIG_SLOPE * gate_clamp * sig * (1.0 - sig)),
        0.0,
    )
    to_up = jnp.where(jnp.abs(up_pre) < CLAMP_LIMIT, glu, 0.0)
    back = mm(y_slots, down_w, COLS)
    d_gate = (back * to_gate).astype(BF16)
    d_up = (back * to_up).astype(BF16)
    w_part = jnp.sum(act.astype(F32) * back, axis=1)

    def partial(q):
        return mm(d_gate, rows(gate_w, q), COLS) + mm(d_up, rows(up_w, q), COLS)

    sent_prv = lax.ppermute(partial(prv).astype(BF16), "tp", down)
    sent_far = lax.ppermute(partial(far).astype(BF16), "tp", up)
    keep_own = (partial(own) + sent_prv.astype(F32)).astype(BF16)
    keep_nxt = (partial(nxt) + sent_far.astype(F32)).astype(BF16)
    back_rows = exchange(
        jnp.concatenate([keep_own, keep_nxt], axis=1).reshape(n_ep, cap, 2 * quarter)
    ).reshape(slots, 2 * quarter)

    w_back = exchange(w_part.reshape(n_ep, 1, cap)).reshape(n_ep, cap)
    w_back = w_back + lax.ppermute(w_back, "tp", [(k, k ^ 1) for k in range(n_tp)])
    w_back = w_back + lax.ppermute(w_back, "tp", [(k, k ^ 2) for k in range(n_tp)])
    per_expert = jnp.sum(jnp.where(hit, w_back[:, :, None], 0.0), axis=1)
    grad_route_weights = jnp.stack(
        [
            jnp.sum(jnp.where(picks[k], per_expert, 0.0), axis=0) / wts[k].astype(F32)
            for k in range(top)
        ],
        axis=1,
    ).astype(BF16)

    grad_gate = mm(x_slots, d_gate, ROWS)
    grad_up = mm(x_slots, d_up, ROWS)
    grad_down = mm(act, y_slots, ROWS)

    both = lax.all_gather(
        jnp.concatenate([dense_in, dense_out], axis=1), ("ep", "tp"), axis=0, tiled=True
    )
    hidden = dense_in.shape[1]
    in_whole, out_whole = both[:, :hidden], both[:, hidden:]
    dense_pre = mm(tokens, in_whole)
    dense_act = jax.nn.silu(dense_pre).astype(BF16)
    dense_val = mm(dense_act, out_whole, COLS)
    mix = jax.nn.sigmoid(jnp.dot(tokens, dense_gate, preferred_element_type=F32))
    cot_wide = cotangent.astype(F32)
    dense_scaled = (mix[:, None] * cot_wide).astype(BF16)
    dense_back = mm(dense_scaled, out_whole)
    sig_pre = jax.nn.sigmoid(dense_pre)
    dense_dpre = (dense_back * sig_pre * (1.0 + dense_pre * (1.0 - sig_pre))).astype(BF16)
    dlogit = mix * (1.0 - mix) * jnp.sum(cot_wide * dense_val, axis=1)
    dense_dx = mm(dense_dpre, rows(in_whole, own), COLS)
    gate_cols = lax.dynamic_slice_in_dim(dense_gate, own * quarter, quarter, 0)
    dense_dx = dense_dx + dlogit[:, None] * gate_cols.astype(F32)[None, :]

    block = width // (n_ep * n_tp)

    def mine(a):
        return lax.dynamic_index_in_dim(
            a.reshape(tok, n_ep, n_tp, block), own, 2, keepdims=False
        ).reshape(tok, n_ep * block)

    tokens_own = mine(tokens)
    in_part = mm(tokens_own, dense_dpre, ROWS)
    out_part = mm(mine(dense_scaled), dense_act, ROWS)
    gate_part = jnp.sum(tokens_own.astype(F32) * dlogit[:, None], axis=0)
    summed = lax.psum_scatter(
        jnp.concatenate([in_part, out_part, gate_part[:, None]], axis=1),
        "ep",
        scatter_dimension=0,
        tiled=True,
    )

    got = mm(place, back_rows, ROWS)
    others = lax.ppermute(got[:, quarter:].astype(BF16), "tp", up)
    grad_tokens = (dense_dx + got[:, :quarter] + others.astype(F32)).astype(BF16)
    return (
        grad_tokens,
        grad_route_weights,
        grad_gate[None],
        grad_up[None],
        grad_down[None],
        summed[:, :hidden],
        summed[:, hidden : 2 * hidden],
        summed[:, 2 * hidden],
    )


def solution(mesh):
    both = ("ep", "tp")
    return jax.shard_map(
        shards,
        mesh=mesh,
        in_specs=(
            P("ep", None),
            P("ep", None),
            P("ep", None),
            P("ep", None),
            P("ep", None, "tp"),
            P("ep", None, "tp"),
            P("ep", "tp", None),
            P(both, None),
            P(both, None),
            P(),
        ),
        out_specs=(
            P("ep", "tp"),
            P("ep", None),
            P("ep", None, "tp"),
            P("ep", None, "tp"),
            P("ep", "tp", None),
            P(both, None),
            P(both, None),
            P(both),
        ),
        check_vma=False,
    )
```

time: 381 us -> 365 us (0.958)
  waiting for transfers between devices: 102 us -> 192 us
  blocking collectives: 69.6 us -> 0 us
  local copies, waits for them, and re-layouts: 73.4 us -> 37.4 us
  other arithmetic: 23.6 us -> 7.83 us
  starting transfers between devices: 31.1 us -> 39.8 us
  matrix products: 59.3 us -> 66.9 us
    all_to_all x1 -> x0, blocking collectives: 69.6 us -> none  [shards(): lax.all_to_all(x_rows, 'ep', split_axis=0, concat_axis=0, tiled=True)]
    ppermute x0 -> x9, waiting for transfers between devices: none -> 68.8 us  [the longest x1 24.9 us: shards(): lax.ppermute(w_back, 'tp', [(k, k ^ 1) for k in range(n_tp)])]
    unnamed x3, waiting for transfers between devices: 12.2 us -> 48.3 us
    gather x5 -> x0, local copies, waits for them, and re-layouts: 34 us -> none  [the longest x1 12.3 us: shards(): cotangent[token_of]]
    convert_element_type x6 -> x1, local copies, waits for them, and re-layouts: 19.7 us -> 1.55 us  [shards(): dense_scaled = (mix[:, None] * cot_wide).astype(BF16)]
    all_to_all x5 -> x4, waiting for transfers between devices: 89.7 us -> 74.5 us  [exchange(): return lax.all_to_all(a, 'ep', split_axis=0, concat_axis=0, tiled=True)]
    ppermute x0 -> x9, starting transfers between devices: none -> 13.7 us  [the longest x2 3.65 us: whole(): d = lax.ppermute(b, 'tp', down)]
    slice x1 -> x9, local copies, waits for them, and re-layouts: 0.25 us -> 10.3 us  [the longest x2 5.86 us: whole(): a, b = (got[:, :quarter], got[:, quarter:])]
  transfers between devices with their start and end apart: 7 -> 15, of which waited for: 3 -> 8; matrix products, arithmetic and copies ran while one was open for 32% -> 28% of each run, Pallas kernels for 0% -> 0%
where the time goes in v1:
time: 365 us; the launch traced here: 358 us
  waiting for transfers between devices  192 us (53%)
  matrix products  66.9 us (18%)
  starting transfers between devices  39.8 us (11%)
  local copies, waits for them, and re-layouts  37.4 us (10%)
  between operations  14.8 us (4%)
  other arithmetic  7.83 us (2%)
    all_to_all x4, waiting for transfers between devices, exchange(): return lax.all_to_all(a, 'ep', split_axis=0, concat_axis=0, tiled=True)  74.5 us
    dot_general x24, matrix products, mm(): return lax.dot_general(a, b, dims, preferred_element_type=F32)  66.4 us
    unnamed x3, waiting for transfers between devices  48.3 us
    all_to_all x4, starting transfers between devices, exchange(): return lax.all_to_all(a, 'ep', split_axis=0, concat_axis=0, tiled=True)  25.8 us
    ppermute x1, waiting for transfers between devices, shards(): lax.ppermute(w_back, 'tp', [(k, k ^ 1) for k in range(n_tp)])  24.9 us
    ppermute x2, waiting for transfers between devices, whole(): c = lax.ppermute(a, 'tp', up)  23.3 us
    ppermute x2, waiting for transfers between devices, whole(): d = lax.ppermute(b, 'tp', down)  20.6 us
    unnamed x54, local copies, waits for them, and re-layouts  7.34 us
  transfers between devices with their start and end apart: 15, of which 8 were waited for; matrix products, arithmetic and copies ran while one was open for 28% of the time, Pallas kernels for 0%

profile of v1, /device:TPU:0, one launch (start us, length us, event | category | flops | bytes accessed | tf_op | source)
XLA Modules:
  0.0 358.3 jit_solution(14650623838948668973)
XLA Ops:
  10.6 3.0 convolution_convert_fusion.1
  13.7 8.7 %all-to-all-start = ((bf16[32,40,1024]{2,1,0:T(8,128)(2,1)}), bf16[32,40,1024]{2,1,0:T(8,128)(2,1)}, u32[]{:S(2)}, u32[]{:S(2)}) async-start(bf16[32,40,1024]{2,1,0:T(8,128)(2,1)} %bitcast.111), calls=%async_computation | async-start | bytes 5242880 | tf_op jit(solution)/shard_map/all_to_all | solution.py:49
  22.8 3.0 convolution_convert_fusion
  25.8 32.7 %all-to-all-done = bf16[32,40,1024]{2,1,0:T(8,128)(2,1)} async-done(((bf16[32,40,1024]{2,1,0:T(8,128)(2,1)}), bf16[32,40,1024]{2,1,0:T(8,128)(2,1)}, u32[]{:S(2)}, u32[]{:S(2)}) %all-to-all-start) | async-done | bytes 2621472 | tf_op jit(solution)/shard_map/all_to_all | solution.py:49
  58.5 4.9 %all-to-all-start.1 = ((bf16[32,40,1024]{2,1,0:T(8,128)(2,1)}), bf16[32,40,1024]{2,1,0:T(8,128)(2,1)}, u32[]{:S(2)}, u32[]{:S(2)}) async-start(bf16[32,40,1024]{2,1,0:T(8,128)(2,1)} %bitcast.110), calls=%async_computation.1 | async-start | bytes 5242880 | tf_op jit(solution)/shard_map/all_to_all | solution.py:49
  66.4 3.0 broadcast.81.clone.1
  69.4 3.8 %fusion.74 = (bf16[1280,512]{1,0:T(8,128)(2,1)}, bf16[1280,2048]{1,0:T(8,128)(2,1)}, bf16[1280,512]{1,0:T(8,128)(2,1)}) fusion(bf16[1280,1024]{1,0:T(8,128)(2,1)} %bitcast.6, bf16[1280,2048]{1,0:T(8,128)(2,1)} %broadcast.81.clone.1, s32[]{:T(128)S(6)} %select_n.92), kind=kLoop, calls=%fused_computation.136 | loop fusion | bytes 6553604 | tf_op jit(solution)/shard_map/slice | solution.py:76
  74.8 25.0 %all-to-all-done.1 = bf16[32,40,1024]{2,1,0:T(8,128)(2,1)} async-done(((bf16[32,40,1024]{2,1,0:T(8,128)(2,1)}), bf16[32,40,1024]{2,1,0:T(8,128)(2,1)}, u32[]{:S(2)}, u32[]{:S(2)}) %all-to-all-start.1) | async-done | bytes 2621472 | tf_op jit(solution)/shard_map/all_to_all | solution.py:49
  113.0 23.3 %collective-permute-done.2 = bf16[1280,512]{1,0:T(8,128)(2,1)S(1)} collective-permute-done((bf16[1280,512]{1,0:T(8,128)(2,1)S(1)}, bf16[1280,512]{1,0:T(8,128)(2,1)S(1)}, u32[]{:S(2)}, u32[]{:S(2)}) %collective-permute-start.2) | collective-permute-done | bytes 1310752 | tf_op jit(solution)/shard_map/ppermute | solution.py:77
  139.0 3.2 fusion.3
  142.3 3.3 fusion.5
  145.6 18.3 %collective-permute-done.1 = bf16[1280,512]{1,0:T(8,128)(2,1)S(1)} collective-permute-done((bf16[1280,512]{1,0:T(8,128)(2,1)S(1)}, bf16[1280,512]{1,0:T(8,128)(2,1)S(1)}, u32[]{:S(2)}, u32[]{:S(2)}) %collective-permute-start.1) | collective-permute-done | bytes 1310752 | tf_op jit(solution)/shard_map/ppermute | solution.py:78
  165.1 8.6 %multiply_reduce_fusion = (f32[1280]{0:T(1024)S(1)}, bf16[1280,512]{0,1:T(8,128)(2,1)}, bf16[1280,512]{0,1:T(8,128)(2,1)S(1)}, bf16[1280,512]{0,1:T(8,128)(2,1)}) fusion(f32[1280,512]{0,1:T(8,128)S(1)} %fusion.3, f32[1280,512]{0,1:T(8,128)S(1)} %fusion.5, bf16[1280,2048]{1,0:T(8,128)(2,1)} %constant_dynamic-update-slice_fusion.4, ...), kind=kOutput, calls=%fused_computation.15 | convolution fusion | flops 2702048000 | bytes 16520192 | tf_op jit(solution)/shard_map/dot_general | solution.py:15
  174.4 4.9 %all-to-all-start.3 = ((f32[32,1,40]{2,1,0:T(1,128)}), f32[32,1,40]{2,1,0:T(1,128)S(1)}, u32[]{:S(2)}, u32[]{:S(2)}) async-start(f32[32,1,40]{2,1,0:T(1,128)} %reshape.180), calls=%async_computation.3 | async-start | bytes 32768 | tf_op jit(solution)/shard_map/all_to_all | solution.py:49
  183.5 3.1 collective-permute-start.4
  189.4 4.7 %convolution_bitcast_fusion.1 = f32[1,2048,512]{2,1,0:T(8,128)} fusion(bf16[1280,2048]{1,0:T(8,128)(2,1)S(1)} %bitcast.109, bf16[1280,512]{0,1:T(8,128)(2,1)S(1)} %get-tuple-element.42), kind=kOutput, calls=%fused_computation.9 | convolution fusion | flops 2684354560 | bytes 10747904 | tf_op jit(solution)/shard_map/dot_general | solution.py:15
  194.1 4.7 %convolution_bitcast_fusion.2 = f32[1,2048,512]{2,1,0:T(8,128)} fusion(bf16[1280,2048]{1,0:T(8,128)(2,1)S(1)} %bitcast.109, bf16[1280,512]{0,1:T(8,128)(2,1)S(1)} %copy-done.1), kind=kOutput, calls=%fused_computation.10 | convolution fusion | flops 2684354560 | bytes 10747904 | tf_op jit(solution)/shard_map/dot_general | solution.py:15
  201.7 3.7 %fusion.31 = f32[1280,512]{0,1:T(8,128)} fusion(bf16[1280,512]{0,1:T(8,128)(2,1)} %get-tuple-element.43, bf16[1,2048,512]{2,1,0:T(8,128)(2,1)S(1)} %copy-done, s32[]{:T(128)S(6)} %select_n.98), kind=kOutput, calls=%fused_computation.64 | convolution fusion | flops 671088640 | bytes 4456452 | tf_op jit(solution)/shard_map/dot_general | solution.py:15
  205.3 24.9 %collective-permute-done.7 = f32[32,40]{1,0:T(8,128)S(1)} collective-permute-done((f32[32,40]{1,0:T(8,128)S(1)}, f32[32,40]{1,0:T(8,128)S(1)}, u32[]{:S(2)}, u32[]{:S(2)}) %collective-permute-start.7) | collective-permute-done | bytes 5152 | tf_op jit(solution)/shard_map/ppermute | solution.py:117
  243.0 4.5 %copy.38 = bf16[1280,1024]{1,0:T(8,128)(2,1)} copy(bf16[1280,1024]{0,1:T(8,128)(2,1)} %pad_maximum_fusion) | data formatting | bytes 5242880 | tf_op jit(solution)/shard_map/concatenate | solution.py:113
  247.5 7.3 %all-to-all-start.2 = ((bf16[32,40,1024]{2,1,0:T(8,128)(2,1)}), bf16[32,40,1024]{2,1,0:T(8,128)(2,1)}, u32[]{:S(2)}, u32[]{:S(2)}) async-start(bf16[32,40,1024]{2,1,0:T(8,128)(2,1)} %bitcast.107), calls=%async_computation.2 | async-start | bytes 5242880 | tf_op jit(solution)/shard_map/all_to_all | solution.py:49
  265.7 7.8 %convolution_bitcast_fusion = f32[1,512,2048]{2,1,0:T(8,128)} fusion(bf16[1280,512]{0,1:T(8,128)(2,1)} %get-tuple-element.41, bf16[1280,2048]{1,0:T(8,128)(2,1)} %constant_dynamic-update-slice_fusion.4), kind=kOutput, calls=%fused_computation.8 | convolution fusion | flops 2684354560 | bytes 10747904 | tf_op jit(solution)/shard_map/dot_general | solution.py:15
  274.3 16.8 %all-to-all-done.2 = bf16[32,40,1024]{2,1,0:T(8,128)(2,1)} async-done(((bf16[32,40,1024]{2,1,0:T(8,128)(2,1)}), bf16[32,40,1024]{2,1,0:T(8,128)(2,1)}, u32[]{:S(2)}, u32[]{:S(2)}) %all-to-all-start.2) | async-done | bytes 2621472 | tf_op jit(solution)/shard_map/all_to_all | solution.py:49
  298.2 48.2 %reduce-scatter.4.cloned.1.call-done = f32[16,513]{1,0:T(8,128)} async-done(((f32[512,513]{1,0:T(8,128)}), f32[16,513]{1,0:T(8,128)}) %reduce-scatter.4.cloned.1.call-update) | async-done | bytes 32848
  (130 shorter events, 72.1 us)
Async XLA Ops:
  7.2 135.1 %copy-start = (bf16[1,2048,512]{2,1,0:T(8,128)(2,1)S(1)}, bf16[1,2048,512]{2,1,0:T(8,128)(2,1)}, u32[]{:S(2)}) copy-start(bf16[1,2048,512]{2,1,0:T(8,128)(2,1)} %param.14) | copy-start | bytes 6291460
  13.7 9.0 %copy-start.4 = (bf16[320,2048]{1,0:T(8,128)(2,1)S(1)}, bf16[320,2048]{1,0:T(8,128)(2,1)}, u32[]{:S(2)}) copy-start(bf16[320,2048]{1,0:T(8,128)(2,1)} %param.10) | copy-start | bytes 3932164
  13.7 44.9 %all-to-all-start = ((bf16[32,40,1024]{2,1,0:T(8,128)(2,1)}), bf16[32,40,1024]{2,1,0:T(8,128)(2,1)}, u32[]{:S(2)}, u32[]{:S(2)}) async-start(bf16[32,40,1024]{2,1,0:T(8,128)(2,1)} %bitcast.111), calls=%async_computation | async-start | bytes 5242880 | tf_op jit(solution)/shard_map/all_to_all | solution.py:49
  58.5 41.2 %all-to-all-start.1 = ((bf16[32,40,1024]{2,1,0:T(8,128)(2,1)}), bf16[32,40,1024]{2,1,0:T(8,128)(2,1)}, u32[]{:S(2)}, u32[]{:S(2)}) async-start(bf16[32,40,1024]{2,1,0:T(8,128)(2,1)} %bitcast.110), calls=%async_computation.1 | async-start | bytes 5242880 | tf_op jit(solution)/shard_map/all_to_all | solution.py:49
  63.5 168.2 %all-gather.2.cloned.1.call-start = ((), (), s32[]{:S(2)}) async-start(), calls=%async_computation.5 | async-start | bytes 2113536 | tf_op jit(solution)/shard_map/all_gather | solution.py:132
  73.3 38.5 %collective-permute-start = (bf16[1280,512]{1,0:T(8,128)(2,1)}, bf16[1280,512]{1,0:T(8,128)(2,1)S(1)}, u32[]{:S(2)}, u32[]{:S(2)}) collective-permute-start(bf16[1280,512]{1,0:T(8,128)(2,1)} %get-tuple-element.49), channel_id=1, source_target_pairs={{0,1},{1,2},{2,3},{3,0},{4,5},{5,6},{6,7},{7,4},{8,9},{9,10},{10,1... | collective-permute-start | bytes 3932168 | tf_op jit(solution)/shard_map/ppermute | solution.py:77
  102.5 5.9 %copy-start.12 = (bf16[1280,512]{1,0:T(8,128)(2,1)S(1)}, bf16[1280,512]{1,0:T(8,128)(2,1)}, u32[]{:S(2)}) copy-start(bf16[1280,512]{1,0:T(8,128)(2,1)} %get-tuple-element.47) | copy-start | bytes 3932164
  102.5 33.9 %collective-permute-start.2 = (bf16[1280,512]{1,0:T(8,128)(2,1)S(1)}, bf16[1280,512]{1,0:T(8,128)(2,1)S(1)}, u32[]{:S(2)}, u32[]{:S(2)}) collective-permute-start(bf16[1280,512]{1,0:T(8,128)(2,1)S(1)} %get-tuple-element.46), channel_id=1, source_target_pairs={{0,1},{1,2},{2,3},{3,0},{4,5},{5,6},{6,7},{7,4},{8,9},{9,10},{10,1... | collective-permute-start | bytes 3932168 | tf_op jit(solution)/shard_map/ppermute | solution.py:77
  104.0 34.8 %collective-permute-start.3 = (bf16[1280,512]{1,0:T(8,128)(2,1)S(1)}, bf16[1280,512]{1,0:T(8,128)(2,1)S(1)}, u32[]{:S(2)}, u32[]{:S(2)}) collective-permute-start(bf16[1280,512]{1,0:T(8,128)(2,1)S(1)} %get-tuple-element.44), channel_id=1, source_target_pairs={{0,3},{1,0},{2,1},{3,2},{4,7},{5,4},{6,5},{7,6},{8,11},{9,8},{10,9... | collective-permute-start | bytes 3932168 | tf_op jit(solution)/shard_map/ppermute | solution.py:78
  108.4 55.5 %collective-permute-start.1 = (bf16[1280,512]{1,0:T(8,128)(2,1)S(1)}, bf16[1280,512]{1,0:T(8,128)(2,1)S(1)}, u32[]{:S(2)}, u32[]{:S(2)}) collective-permute-start(bf16[1280,512]{1,0:T(8,128)(2,1)S(1)} %copy-done.12), channel_id=1, source_target_pairs={{0,3},{1,0},{2,1},{3,2},{4,7},{5,4},{6,5},{7,6},{8,11},{9,8},{10,9... | collective-permute-start | bytes 3932168 | tf_op jit(solution)/shard_map/ppermute | solution.py:78
  113.0 26.0 %copy-start.7 = (bf16[1,2048,512]{2,1,0:T(8,128)(2,1)S(1)}, bf16[1,2048,512]{2,1,0:T(8,128)(2,1)}, u32[]{:S(2)}) copy-start(bf16[1,2048,512]{2,1,0:T(8,128)(2,1)} %param.15) | copy-start | bytes 6291460
  145.5 19.5 %copy-start.20 = (bf16[1,512,2048]{2,1,0:T(8,128)(2,1)S(1)}, bf16[1,512,2048]{2,1,0:T(8,128)(2,1)}, u32[]{:S(2)}) copy-start(bf16[1,512,2048]{2,1,0:T(8,128)(2,1)} %param.16) | copy-start | bytes 6291460
  174.4 26.8 %all-to-all-start.3 = ((f32[32,1,40]{2,1,0:T(1,128)}), f32[32,1,40]{2,1,0:T(1,128)S(1)}, u32[]{:S(2)}, u32[]{:S(2)}) async-start(f32[32,1,40]{2,1,0:T(1,128)} %reshape.180), calls=%async_computation.3 | async-start | bytes 32768 | tf_op jit(solution)/shard_map/all_to_all | solution.py:49
  181.6 7.9 %slice-start = ((s8[5242880]{0:T(1024)(128)(4,1)}), s8[4194304]{0:T(1024)(128)(4,1)S(1)}, s32[]{:S(2)}) async-start(s8[5242880]{0:T(1024)(128)(4,1)} %bitcast.108), calls=%async_computation.7 | async-start | bytes 8388608
  183.5 51.6 %collective-permute-start.4 = (bf16[1280,512]{0,1:T(8,128)(2,1)}, bf16[1280,512]{0,1:T(8,128)(2,1)}, u32[]{:S(2)}, u32[]{:S(2)}) collective-permute-start(bf16[1280,512]{0,1:T(8,128)(2,1)} %fusion), channel_id=1, source_target_pairs={{0,3},{1,0},{2,1},{3,2},{4,7},{5,4},{6,5},{7,6},{8,11},{9,8},{10,9... | collective-permute-start | bytes 3932168 | tf_op jit(solution)/shard_map/ppermute | solution.py:108
  201.2 38.0 %collective-permute-start.5 = (bf16[1280,512]{0,1:T(8,128)(2,1)}, bf16[1280,512]{0,1:T(8,128)(2,1)}, u32[]{:S(2)}, u32[]{:S(2)}) collective-permute-start(bf16[1280,512]{0,1:T(8,128)(2,1)} %fusion.1), channel_id=1, source_target_pairs={{0,1},{1,2},{2,3},{3,0},{4,5},{5,6},{6,7},{7,4},{8,9},{9,10},{10,1... | collective-permute-start | bytes 3932168 | tf_op jit(solution)/shard_map/ppermute | solution.py:109
  201.2 29.0 %collective-permute-start.7 = (f32[32,40]{1,0:T(8,128)S(1)}, f32[32,40]{1,0:T(8,128)S(1)}, u32[]{:S(2)}, u32[]{:S(2)}) collective-permute-start(f32[32,40]{1,0:T(8,128)S(1)} %bitcast.116), channel_id=1, source_target_pairs={{0,1},{1,0},{2,3},{3,2},{4,5},{5,4},{6,7},{7,6},{8,9},{9,8},{10,11... | collective-permute-start | bytes 15368 | tf_op jit(solution)/shard_map/ppermute | solution.py:117
  230.2 43.3 %collective-permute-start.8 = (f32[32,40]{1,0:T(8,128)S(1)}, f32[32,40]{1,0:T(8,128)S(1)}, u32[]{:S(2)}, u32[]{:S(2)}) collective-permute-start(f32[32,40]{1,0:T(8,128)S(1)} %add.143), channel_id=1, source_target_pairs={{0,2},{1,3},{2,0},{3,1},{4,6},{5,7},{6,4},{7,5},{8,10},{9,11},{10,... | collective-permute-start | bytes 15368 | tf_op jit(solution)/shard_map/ppermute | solution.py:118
  247.5 43.5 %all-to-all-start.2 = ((bf16[32,40,1024]{2,1,0:T(8,128)(2,1)}), bf16[32,40,1024]{2,1,0:T(8,128)(2,1)}, u32[]{:S(2)}, u32[]{:S(2)}) async-start(bf16[32,40,1024]{2,1,0:T(8,128)(2,1)} %bitcast.107), calls=%async_computation.2 | async-start | bytes 5242880 | tf_op jit(solution)/shard_map/all_to_all | solution.py:49
  254.8 91.5 %reduce-scatter.4.cloned.1.call-start = ((), (), s32[]{:S(2)}) async-start(), calls=%async_computation.6 | async-start | bytes 1351680
  265.7 8.5 %copy-start.16 = (bf16[320,2]{0,1:T(2,128)(2,1)S(1)}, bf16[320,2]{0,1:T(2,128)(2,1)}, u32[]{:S(2)}) copy-start(bf16[320,2]{0,1:T(2,128)(2,1)} %param.13) | copy-start | bytes 3844
  294.9 54.1 %slice-start.2 = ((bf16[2048,512]{1,0:T(8,128)(2,1)}), bf16[2048,256]{1,0:T(8,128)(2,1)S(1)}, s32[]{:S(2)}) async-start(bf16[2048,512]{1,0:T(8,128)(2,1)} %all-gather.2.cloned.1.call-done), calls=%async_computation.9 | async-start | bytes 2097152 | tf_op jit(solution)/shard_map/slice | solution.py:136
  294.9 54.1 %copy-start.15 = (bf16[320,256]{1,0:T(8,128)(2,1)S(1)}, bf16[320,256]{1,0:T(8,128)(2,1)}, u32[]{:S(2)}) copy-start(bf16[320,256]{1,0:T(8,128)(2,1)} %copy-done.14) | copy-start | bytes 491524
  295.7 53.3 %collective-permute-start.6 = (bf16[320,512]{1,0:T(8,128)(2,1)}, bf16[320,512]{1,0:T(8,128)(2,1)}, u32[]{:S(2)}, u32[]{:S(2)}) collective-permute-start(bf16[320,512]{1,0:T(8,128)(2,1)} %slice.98), channel_id=1, source_target_pairs={{0,1},{1,2},{2,3},{3,0},{4,5},{5,6},{6,7},{7,4},{8,9},{9,10},{10,1... | collective-permute-start | bytes 983048 | tf_op jit(solution)/shard_map/ppermute | solution.py:170
  (17 other events, 49.2 us)
Sparse Core Ops, SparseCore 0:
  67.9 74.2 all-gather.1
  265.8 80.4 reduce-scatter.3

commit v2 on v1

--- a/solution.py
+++ b/solution.py
@@ -2,6 +2,7 @@
 import jax.numpy as jnp
 from jax import lax
 from jax.sharding import PartitionSpec as P
+
 
 CLAMP_LIMIT = 7.0
 SIG_SLOPE = 1.702
@@ -64,25 +65,32 @@
     share = jnp.where(picks[0], wts[0][None, :], 0) + jnp.where(picks[1], wts[1][None, :], 0)
     place_w = jnp.where(hit, share.astype(BF16)[:, None, :], 0).astype(BF16).reshape(slots, tok)
 
-    def pair(a):
-        return jnp.concatenate([cols(a, own), cols(a, nxt)], axis=1)
-
-    x_send = mm(place, pair(tokens)).astype(BF16).reshape(n_ep, cap, 2 * quarter)
-    y_send = mm(place_w, pair(cotangent)).astype(BF16).reshape(n_ep, cap, 2 * quarter)
-    x_got = exchange(x_send).reshape(slots, 2 * quarter)
+    x_send = mm(place, cols(tokens, own)).astype(BF16).reshape(n_ep, cap, quarter)
+    y_pair = jnp.concatenate([cols(cotangent, own), cols(cotangent, nxt)], axis=1)
+    y_send = mm(place_w, y_pair).astype(BF16).reshape(n_ep, cap, 2 * quarter)
+    x_got = exchange(x_send).reshape(slots, quarter)
     y_got = exchange(y_send).reshape(slots, 2 * quarter)
 
-    def whole(got):
-        a, b = got[:, :quarter], got[:, quarter:]
-        c = lax.ppermute(a, "tp", up)
-        d = lax.ppermute(b, "tp", down)
-        full = jnp.zeros((slots, width), BF16)
-        for piece, q in ((a, own), (b, nxt), (c, prv), (d, far)):
-            full = lax.dynamic_update_slice_in_dim(full, piece, q * quarter, 1)
-        return full
-
-    x_slots = whole(x_got)
-    y_slots = whole(y_got)
+    def put(full, piece, q):
+        return lax.dynamic_update_slice_in_dim(full, piece, q * quarter, 1)
+
+    half = slots // 2
+    x_up = lax.ppermute(x_got, "tp", up)
+    x_dn = lax.ppermute(x_got, "tp", down)
+    x_far_a = lax.ppermute(x_dn[:half], "tp", down)
+    x_far_b = lax.ppermute(x_up[half:], "tp", up)
+    x_slots = jnp.zeros((slots, width), BF16)
+    for piece, q in ((x_got, own), (x_up, prv), (x_dn, nxt)):
+        x_slots = put(x_slots, piece, q)
+    x_slots = lax.dynamic_update_slice(x_slots, x_far_a, (0, far * quarter))
+    x_slots = lax.dynamic_update_slice(x_slots, x_far_b, (half, far * quarter))
+    y_a, y_b = y_got[:, :quarter], y_got[:, quarter:]
+    y_up = lax.ppermute(y_a, "tp", up)
+    y_dn = lax.ppermute(y_b, "tp", down)
+    y_slots = jnp.zeros((slots, width), BF16)
+    for piece, q in ((y_a, own), (y_b, nxt), (y_up, prv), (y_dn, far)):
+        y_slots = put(y_slots, piece, q)
+
     gate_w, up_w, down_w = w_gate[0], w_up[0], w_down[0]
     gate_pre = mm(x_slots, gate_w)
     up_pre = mm(x_slots, up_w)
@@ -97,6 +105,8 @@
         0.0,
     )
     to_up = jnp.where(jnp.abs(up_pre) < CLAMP_LIMIT, glu, 0.0)
+    act, to_gate, to_up = lax.optimization_barrier((act, to_gate, to_up))
+    tokens, cotangent, act = lax.optimization_barrier((tokens, cotangent, act))
     back = mm(y_slots, down_w, COLS)
     d_gate = (back * to_gate).astype(BF16)
     d_up = (back * to_up).astype(BF16)
@@ -105,13 +115,19 @@
     def partial(q):
         return mm(d_gate, rows(gate_w, q), COLS) + mm(d_up, rows(up_w, q), COLS)
 
-    sent_prv = lax.ppermute(partial(prv).astype(BF16), "tp", down)
-    sent_far = lax.ppermute(partial(far).astype(BF16), "tp", up)
-    keep_own = (partial(own) + sent_prv.astype(F32)).astype(BF16)
-    keep_nxt = (partial(nxt) + sent_far.astype(F32)).astype(BF16)
-    back_rows = exchange(
-        jnp.concatenate([keep_own, keep_nxt], axis=1).reshape(n_ep, cap, 2 * quarter)
-    ).reshape(slots, 2 * quarter)
+    away = partial(far).astype(BF16)
+    top_in = lax.ppermute(away[:half], "tp", up)
+    low_in = lax.ppermute(away[half:], "tp", down)
+    ahead = partial(nxt)
+    ahead = jnp.concatenate([ahead[:half] + top_in.astype(F32), ahead[half:]], axis=0).astype(BF16)
+    behind = partial(prv)
+    behind = jnp.concatenate([behind[:half], behind[half:] + low_in.astype(F32)], axis=0)
+    behind = behind.astype(BF16)
+    ahead = lax.ppermute(ahead, "tp", up)
+    behind = lax.ppermute(behind, "tp", down)
+    total = partial(own) + ahead.astype(F32) + behind.astype(F32)
+    back_rows = exchange(total.astype(BF16).reshape(n_ep, cap, quarter))
+    back_rows = back_rows.reshape(slots, quarter)
 
     w_back = exchange(w_part.reshape(n_ep, 1, cap)).reshape(n_ep, cap)
     w_back = w_back + lax.ppermute(w_back, "tp", [(k, k ^ 1) for k in range(n_tp)])
@@ -136,14 +152,13 @@
     in_whole, out_whole = both[:, :hidden], both[:, hidden:]
     dense_pre = mm(tokens, in_whole)
     dense_act = jax.nn.silu(dense_pre).astype(BF16)
-    dense_val = mm(dense_act, out_whole, COLS)
+    cot_out = mm(cotangent, out_whole)
     mix = jax.nn.sigmoid(jnp.dot(tokens, dense_gate, preferred_element_type=F32))
-    cot_wide = cotangent.astype(F32)
-    dense_scaled = (mix[:, None] * cot_wide).astype(BF16)
+    dense_scaled = (mix[:, None] * cotangent.astype(F32)).astype(BF16)
     dense_back = mm(dense_scaled, out_whole)
     sig_pre = jax.nn.sigmoid(dense_pre)
     dense_dpre = (dense_back * sig_pre * (1.0 + dense_pre * (1.0 - sig_pre))).astype(BF16)
-    dlogit = mix * (1.0 - mix) * jnp.sum(cot_wide * dense_val, axis=1)
+    dlogit = mix * (1.0 - mix) * jnp.sum(dense_act.astype(F32) * cot_out, axis=1)
     dense_dx = mm(dense_dpre, rows(in_whole, own), COLS)
     gate_cols = lax.dynamic_slice_in_dim(dense_gate, own * quarter, quarter, 0)
     dense_dx = dense_dx + dlogit[:, None] * gate_cols.astype(F32)[None, :]
@@ -166,9 +181,7 @@
         tiled=True,
     )
 
-    got = mm(place, back_rows, ROWS)
-    others = lax.ppermute(got[:, quarter:].astype(BF16), "tp", up)
-    grad_tokens = (dense_dx + got[:, :quarter] + others.astype(F32)).astype(BF16)
+    grad_tokens = (dense_dx + mm(place, back_rows, ROWS)).astype(BF16)
     return (
         grad_tokens,
         grad_route_weights,
@@ -183,6 +196,7 @@
 
 def solution(mesh):
     both = ("ep", "tp")
+
     return jax.shard_map(
         shards,
         mesh=mesh,

time: 365 us -> 330 us (0.904); the launches traced: 358 us -> 329 us
  waiting for transfers between devices: 192 us -> 135 us
  other arithmetic: 7.83 us -> 17.4 us
  local copies, waits for them, and re-layouts: 37.4 us -> 46.1 us
  matrix products: 66.9 us -> 72.8 us
    all_to_all x4, waiting for transfers between devices: 74.5 us -> 42.2 us  [exchange(): return lax.all_to_all(a, 'ep', split_axis=0, concat_axis=0, tiled=True)]
    ppermute x1, waiting for transfers between devices: 24.9 us -> 0.01 us  [shards(): lax.ppermute(w_back, 'tp', [(k, k ^ 1) for k in range(n_tp)])]
    ppermute x7 -> x10, waiting for transfers between devices: 43.9 us -> 53.8 us  [the longest x1 30.6 us: shards(): x_far_a = lax.ppermute(x_dn[:half], 'tp', down)]
    unnamed x3, waiting for transfers between devices: 48.3 us -> 39.3 us
    dynamic_update_slice x6 -> x8, local copies, waits for them, and re-layouts: 6.93 us -> 15.2 us  [the longest x6 13.3 us: put(): return lax.dynamic_update_slice_in_dim(full, piece, q * quarter, 1)]
    dot_general x24, matrix products: 66.4 us -> 72.4 us  [mm(): return lax.dot_general(a, b, dims, preferred_element_type=F32)]
    slice x3 -> x6, local copies, waits for them, and re-layouts: 6.62 us -> 12 us  [the longest x1 3.59 us: shards(): y_a, y_b = (y_got[:, :quarter], y_got[:, quarter:])]
    concatenate x1 -> x0, local copies, waits for them, and re-layouts: 4.47 us -> none  [shards(): jnp.concatenate([keep_own, keep_nxt], axis=1)]
  transfers between devices with their start and end apart: 15 -> 18, of which waited for: 8 -> 7; matrix products, arithmetic and copies ran while one was open for 28% -> 39% of each run, Pallas kernels for 0% -> 0%
where the time goes in v2:
time: 330 us; the launch traced here: 329 us
  waiting for transfers between devices  135 us (41%)
  matrix products  72.8 us (22%)
  local copies, waits for them, and re-layouts  46.1 us (14%)
  starting transfers between devices  42.8 us (13%)
  other arithmetic  17.4 us (5%)
  between operations  14.6 us (4%)
    dot_general x24, matrix products, mm(): return lax.dot_general(a, b, dims, preferred_element_type=F32)  72.4 us
    all_to_all x4, waiting for transfers between devices, exchange(): return lax.all_to_all(a, 'ep', split_axis=0, concat_axis=0, tiled=True)  42.2 us
    unnamed x3, waiting for transfers between devices  39.3 us
    ppermute x1, waiting for transfers between devices, shards(): x_far_a = lax.ppermute(x_dn[:half], 'tp', down)  30.6 us
    all_to_all x4, starting transfers between devices, exchange(): return lax.all_to_all(a, 'ep', split_axis=0, concat_axis=0, tiled=True)  25.6 us
    ppermute x1, waiting for transfers between devices, shards(): behind = lax.ppermute(behind, 'tp', down)  14.8 us
    dynamic_update_slice x6, local copies, waits for them, and re-layouts, put(): return lax.dynamic_update_slice_in_dim(full, piece, q * quarter, 1)  13.3 us
  transfers between devices with their start and end apart: 18, of which 7 were waited for; matrix products, arithmetic and copies ran while one was open for 39% of the time, Pallas kernels for 0%

profile of v2, /device:TPU:0, one launch (start us, length us, event | category | flops | bytes accessed | tf_op | source)
XLA Modules:
  0.0 329.1 jit_solution(2620849602066052313)
XLA Ops:
  11.6 8.4 %all-to-all-start = ((bf16[32,40,512]{2,1,0:T(8,128)(2,1)}), bf16[32,40,512]{2,1,0:T(8,128)(2,1)S(1)}, u32[]{:S(2)}, u32[]{:S(2)}) async-start(bf16[32,40,512]{2,1,0:T(8,128)(2,1)} %bitcast.118), calls=%async_computation | async-start | bytes 2621440 | tf_op jit(solution)/shard_map/all_to_all | solution.py:50
  22.5 4.2 %convolution_convert_fusion = bf16[1280,1024]{1,0:T(8,128)(2,1)} fusion(bf16[1280,320]{1,0:T(8,128)(2,1)} %bitcast_select_fusion, bf16[320,512]{1,0:T(8,128)(2,1)S(1)} %get-tuple-element.64, bf16[320,512]{1,0:T(8,128)(2,1)S(1)} %get-tuple-element.63), kind=kOutput, calls=%fused_computation | convolution fusion | flops 841482240 | bytes 4096000 | tf_op jit(solution)/shard_map/dot_general | solution.py:16
  26.7 13.8 %all-to-all-done = bf16[32,40,512]{2,1,0:T(8,128)(2,1)S(1)} async-done(((bf16[32,40,512]{2,1,0:T(8,128)(2,1)}), bf16[32,40,512]{2,1,0:T(8,128)(2,1)S(1)}, u32[]{:S(2)}, u32[]{:S(2)}) %all-to-all-start) | async-done | bytes 1310752 | tf_op jit(solution)/shard_map/all_to_all | solution.py:50
  40.6 4.9 %all-to-all-start.1 = ((bf16[32,40,1024]{2,1,0:T(8,128)(2,1)}), bf16[32,40,1024]{2,1,0:T(8,128)(2,1)}, u32[]{:S(2)}, u32[]{:S(2)}) async-start(bf16[32,40,1024]{2,1,0:T(8,128)(2,1)} %bitcast.114), calls=%async_computation.1 | async-start | bytes 5242880 | tf_op jit(solution)/shard_map/all_to_all | solution.py:50
  49.2 3.0 broadcast.80.clone
  53.4 28.4 %all-to-all-done.1 = bf16[32,40,1024]{2,1,0:T(8,128)(2,1)} async-done(((bf16[32,40,1024]{2,1,0:T(8,128)(2,1)}), bf16[32,40,1024]{2,1,0:T(8,128)(2,1)}, u32[]{:S(2)}, u32[]{:S(2)}) %all-to-all-start.1) | async-done | bytes 2621472 | tf_op jit(solution)/shard_map/all_to_all | solution.py:50
  82.5 3.6 %fusion.70 = (bf16[1280,512]{1,0:T(8,128)(2,1)}, bf16[1280,2048]{1,0:T(8,128)(2,1)S(1)}, bf16[1280,512]{1,0:T(8,128)(2,1)}) fusion(bf16[1280,1024]{1,0:T(8,128)(2,1)} %bitcast.9, bf16[1280,2048]{1,0:T(8,128)(2,1)S(1)} %broadcast.80.clone.1, s32[]{:T(128)S(6)} %select_n.93), kind=kLoop, calls=%fused_computation.137 | loop fusion | bytes 6553604 | tf_op jit(solution)/shard_map/slice | solution.py:87
  90.0 3.3 %collective-permute-start.2 = (bf16[640,512]{1,0:T(8,128)(2,1)S(1)}, bf16[640,512]{1,0:T(8,128)(2,1)S(1)}, u32[]{:S(2)}, u32[]{:S(2)}) collective-permute-start(bf16[640,512]{1,0:T(8,128)(2,1)S(1)} %slice.82), channel_id=1, source_target_pairs={{0,3},{1,0},{2,1},{3,2},{4,7},{5,4},{6,5},{7,6},{8,11},{9,8},{10,9... | collective-permute-start | bytes 1966088 | tf_op jit(solution)/shard_map/ppermute | solution.py:80
  102.0 30.6 %collective-permute-done.2 = bf16[640,512]{1,0:T(8,128)(2,1)S(1)} collective-permute-done((bf16[640,512]{1,0:T(8,128)(2,1)S(1)}, bf16[640,512]{1,0:T(8,128)(2,1)S(1)}, u32[]{:S(2)}, u32[]{:S(2)}) %collective-permute-start.2) | collective-permute-done | bytes 655392 | tf_op jit(solution)/shard_map/ppermute | solution.py:80
  136.9 4.8 %fusion.6 = f32[1280,512]{1,0:T(8,128)S(1)} fusion(bf16[1280,2048]{1,0:T(8,128)(2,1)} %constant_dynamic-update-slice_fusion.8, bf16[1,2048,512]{2,1,0:T(8,128)(2,1)S(1)} %copy-done.10), kind=kOutput, calls=%fused_computation.26 | convolution fusion | flops 2684354560 | bytes 9961472 | tf_op jit(solution)/shard_map/dot_general | solution.py:16
  141.8 8.7 %fusion.1 = (f32[1280,512]{1,0:T(8,128)}, f32[1280,512]{1,0:T(8,128)}, bf16[1280,512]{1,0:T(8,128)(2,1)}) fusion(f32[1280,512]{1,0:T(8,128)S(1)} %fusion.6, bf16[1280,2048]{1,0:T(8,128)(2,1)} %constant_dynamic-update-slice_fusion.8, bf16[1,2048,512]{2,1,0:T(8,128)(2,1)S(1)} %copy-done), kind=kOutput, calls=%fused_computation.20 | convolution fusion | flops 2697461760 | bytes 16515072 | tf_op jit(solution)/shard_map/dot_general | solution.py:16
  160.5 7.3 %multiply_reduce_fusion = (f32[1280]{0:T(1024)S(1)}, bf16[1280,512]{1,0:T(8,128)(2,1)}, bf16[1280,512]{1,0:T(8,128)(2,1)S(1)}) fusion(bf16[1280,512]{1,0:T(8,128)(2,1)S(1)} %copy-done.12, f32[1280,512]{1,0:T(8,128)S(1)} %copy-done.25, f32[1280,512]{1,0:T(8,128)} %get-tuple-element.17, bf16[1280,2048]{1,0:T(8,128)(2,1)} %constant_dynamic-update-slice_fusion, ...), kind=kOutput, calls=%fused_computation.11 | convolution fusion | flops 2688940800 | bytes 16520192 | tf_op jit(solution)/shard_map/dot_general | solution.py:16
  168.5 4.9 %all-to-all-start.3 = ((f32[32,1,40]{2,1,0:T(1,128)}), f32[32,1,40]{2,1,0:T(1,128)S(1)}, u32[]{:S(2)}, u32[]{:S(2)}) async-start(f32[32,1,40]{2,1,0:T(1,128)} %reshape.180), calls=%async_computation.3 | async-start | bytes 32768 | tf_op jit(solution)/shard_map/all_to_all | solution.py:50
  177.6 3.2 collective-permute-start.8
  187.6 4.4 %convolution_bitcast_fusion = f32[1,512,2048]{2,1,0:T(8,128)} fusion(bf16[1280,512]{1,0:T(8,128)(2,1)S(1)} %copy-done.13, bf16[1280,2048]{1,0:T(8,128)(2,1)S(1)} %bitcast.109), kind=kOutput, calls=%fused_computation.5 | convolution fusion | flops 2684354560 | bytes 10747904 | tf_op jit(solution)/shard_map/dot_general | solution.py:16
  192.0 7.0 %convolution_bitcast_fusion.1 = f32[1,2048,512]{2,1,0:T(8,128)} fusion(bf16[1280,2048]{1,0:T(8,128)(2,1)} %constant_dynamic-update-slice_fusion.8, bf16[1280,512]{1,0:T(8,128)(2,1)S(1)} %copy-done.2), kind=kOutput, calls=%fused_computation.6 | convolution fusion | flops 2684354560 | bytes 10747904 | tf_op jit(solution)/shard_map/dot_general | solution.py:16
  201.4 4.6 %convolution_add_fusion.3 = f32[1280,512]{1,0:T(8,128)} fusion(f32[1280,512]{1,0:T(8,128)} %fusion.34, bf16[1280,512]{1,0:T(8,128)(2,1)} %get-tuple-element.56, bf16[1,2048,512]{2,1,0:T(8,128)(2,1)S(1)} %copy-done, s32[]{:T(128)S(6)} %select_n.93), kind=kOutput, calls=%fused_computation.4 | convolution fusion | flops 671744000 | bytes 7077892 | tf_op jit(solution)/shard_map/dot_general | solution.py:16
  220.4 3.2 collective-permute-start.9
  236.5 14.8 %collective-permute-done.9 = bf16[1280,512]{1,0:T(8,128)(2,1)} collective-permute-done((bf16[1280,512]{1,0:T(8,128)(2,1)}, bf16[1280,512]{1,0:T(8,128)(2,1)}, u32[]{:S(2)}, u32[]{:S(2)}) %collective-permute-start.9) | collective-permute-done | bytes 1310752 | tf_op jit(solution)/shard_map/ppermute | solution.py:127
  251.3 5.9 %collective-permute-done.7 = bf16[1280,512]{1,0:T(8,128)(2,1)} collective-permute-done((bf16[1280,512]{1,0:T(8,128)(2,1)}, bf16[1280,512]{1,0:T(8,128)(2,1)}, u32[]{:S(2)}, u32[]{:S(2)}) %collective-permute-start.7) | collective-permute-done | bytes 1310752 | tf_op jit(solution)/shard_map/ppermute | solution.py:126
  257.3 4.2 %add_convert_fusion = bf16[1280,512]{1,0:T(8,128)(2,1)} fusion(bf16[1280,512]{1,0:T(8,128)(2,1)} %collective-permute-done.9, f32[1280,512]{1,0:T(8,128)} %convolution_add_fusion.3, bf16[1280,512]{1,0:T(8,128)(2,1)} %collective-permute-done.7), kind=kLoop, calls=%fused_computation.12 | loop fusion | flops 3276800 | bytes 6553600 | tf_op jit(solution)/shard_map/convert_element_type | solution.py:129
  261.5 7.3 %all-to-all-start.2 = ((bf16[32,40,512]{2,1,0:T(8,128)(2,1)}), bf16[32,40,512]{2,1,0:T(8,128)(2,1)}, u32[]{:S(2)}, u32[]{:S(2)}) async-start(bf16[32,40,512]{2,1,0:T(8,128)(2,1)} %bitcast.113), calls=%async_computation.2 | async-start | bytes 2621440 | tf_op jit(solution)/shard_map/all_to_all | solution.py:50
  268.8 7.1 %convolution_bitcast_fusion.2 = f32[1,2048,512]{2,1,0:T(8,128)} fusion(bf16[1280,2048]{1,0:T(8,128)(2,1)} %constant_dynamic-update-slice_fusion.8, bf16[1280,512]{1,0:T(8,128)(2,1)S(1)} %get-tuple-element.57), kind=kOutput, calls=%fused_computation.7 | convolution fusion | flops 2684354560 | bytes 10747904 | tf_op jit(solution)/shard_map/dot_general | solution.py:16
  277.5 39.3 %reduce-scatter.4.cloned.1.call-done = f32[16,513]{1,0:T(8,128)} async-done(((f32[512,513]{1,0:T(8,128)}), f32[16,513]{1,0:T(8,128)}) %reduce-scatter.4.cloned.1.call-update) | async-done | bytes 32848
  (149 shorter events, 87.4 us)
Async XLA Ops:
  7.2 134.6 %copy-start = (bf16[1,2048,512]{2,1,0:T(8,128)(2,1)S(1)}, bf16[1,2048,512]{2,1,0:T(8,128)(2,1)}, u32[]{:S(2)}) copy-start(bf16[1,2048,512]{2,1,0:T(8,128)(2,1)} %param.15) | copy-start | bytes 6291460
  8.7 11.4 %copy-start.18 = (bf16[320,2]{0,1:T(2,128)(2,1)S(1)}, bf16[320,2]{0,1:T(2,128)(2,1)}, u32[]{:S(2)}) copy-start(bf16[320,2]{0,1:T(2,128)(2,1)} %param.13) | copy-start | bytes 3844
  11.6 29.0 %all-to-all-start = ((bf16[32,40,512]{2,1,0:T(8,128)(2,1)}), bf16[32,40,512]{2,1,0:T(8,128)(2,1)S(1)}, u32[]{:S(2)}, u32[]{:S(2)}) async-start(bf16[32,40,512]{2,1,0:T(8,128)(2,1)} %bitcast.118), calls=%async_computation | async-start | bytes 2621440 | tf_op jit(solution)/shard_map/all_to_all | solution.py:50
  40.6 7.8 %copy-start.19 = (bf16[16,256]{1,0:T(8,128)(2,1)S(1)}, bf16[16,256]{1,0:T(8,128)(2,1)}, u32[]{:S(2)}) copy-start(bf16[16,256]{1,0:T(8,128)(2,1)} %param.18) | copy-start | bytes 24580
  40.6 7.8 %copy-start.20 = (bf16[16,256]{1,0:T(8,128)(2,1)S(1)}, bf16[16,256]{1,0:T(8,128)(2,1)}, u32[]{:S(2)}) copy-start(bf16[16,256]{1,0:T(8,128)(2,1)} %param.17) | copy-start | bytes 24580
  40.6 8.5 %copy-start.21 = (bf16[2048]{0:T(1024)(128)(2,1)S(1)}, bf16[2048]{0:T(1024)(128)(2,1)}, u32[]{:S(2)}) copy-start(bf16[2048]{0:T(1024)(128)(2,1)} %param.19) | copy-start | bytes 12292
  40.6 41.2 %all-to-all-start.1 = ((bf16[32,40,1024]{2,1,0:T(8,128)(2,1)}), bf16[32,40,1024]{2,1,0:T(8,128)(2,1)}, u32[]{:S(2)}, u32[]{:S(2)}) async-start(bf16[32,40,1024]{2,1,0:T(8,128)(2,1)} %bitcast.114), calls=%async_computation.1 | async-start | bytes 5242880 | tf_op jit(solution)/shard_map/all_to_all | solution.py:50
  45.5 166.5 %all-gather.2.cloned.1.call-start = ((), (), s32[]{:S(2)}) async-start(), calls=%async_computation.5 | async-start | bytes 2113536 | tf_op jit(solution)/shard_map/all_gather | solution.py:148
  45.6 43.3 %collective-permute-start.1 = (bf16[1280,512]{1,0:T(8,128)(2,1)S(1)}, bf16[1280,512]{1,0:T(8,128)(2,1)}, u32[]{:S(2)}, u32[]{:S(2)}) collective-permute-start(bf16[1280,512]{1,0:T(8,128)(2,1)S(1)} %bitcast.110), channel_id=1, source_target_pairs={{0,3},{1,0},{2,1},{3,2},{4,7},{5,4},{6,5},{7,6},{8,11},{9,8},{10,9... | collective-permute-start | bytes 3932168 | tf_op jit(solution)/shard_map/ppermute | solution.py:79
  49.2 45.6 %collective-permute-start = (bf16[1280,512]{1,0:T(8,128)(2,1)S(1)}, bf16[1280,512]{1,0:T(8,128)(2,1)}, u32[]{:S(2)}, u32[]{:S(2)}) collective-permute-start(bf16[1280,512]{1,0:T(8,128)(2,1)S(1)} %bitcast.111), channel_id=1, source_target_pairs={{0,1},{1,2},{2,3},{3,0},{4,5},{5,6},{6,7},{7,4},{8,9},{9,10},{10,1... | collective-permute-start | bytes 3932168 | tf_op jit(solution)/shard_map/ppermute | solution.py:78
  86.1 71.9 %collective-permute-start.5 = (bf16[1280,512]{1,0:T(8,128)(2,1)}, bf16[1280,512]{1,0:T(8,128)(2,1)}, u32[]{:S(2)}, u32[]{:S(2)}) collective-permute-start(bf16[1280,512]{1,0:T(8,128)(2,1)} %get-tuple-element.58), channel_id=1, source_target_pairs={{0,3},{1,0},{2,1},{3,2},{4,7},{5,4},{6,5},{7,6},{8,11},{9,8},{10,9... | collective-permute-start | bytes 3932168 | tf_op jit(solution)/shard_map/ppermute | solution.py:89
  88.8 66.4 %collective-permute-start.4 = (bf16[1280,512]{1,0:T(8,128)(2,1)}, bf16[1280,512]{1,0:T(8,128)(2,1)}, u32[]{:S(2)}, u32[]{:S(2)}) collective-permute-start(bf16[1280,512]{1,0:T(8,128)(2,1)} %get-tuple-element.60), channel_id=1, source_target_pairs={{0,1},{1,2},{2,3},{3,0},{4,5},{5,6},{6,7},{7,4},{8,9},{9,10},{10,1... | collective-permute-start | bytes 3932168 | tf_op jit(solution)/shard_map/ppermute | solution.py:88
  90.0 42.6 %collective-permute-start.2 = (bf16[640,512]{1,0:T(8,128)(2,1)S(1)}, bf16[640,512]{1,0:T(8,128)(2,1)S(1)}, u32[]{:S(2)}, u32[]{:S(2)}) collective-permute-start(bf16[640,512]{1,0:T(8,128)(2,1)S(1)} %slice.82), channel_id=1, source_target_pairs={{0,3},{1,0},{2,1},{3,2},{4,7},{5,4},{6,5},{7,6},{8,11},{9,8},{10,9... | collective-permute-start | bytes 1966088 | tf_op jit(solution)/shard_map/ppermute | solution.py:80
  96.4 39.6 %collective-permute-start.3 = (bf16[640,512]{1,0:T(8,128)(2,1)S(1)}, bf16[640,512]{1,0:T(8,128)(2,1)S(1)}, u32[]{:S(2)}, u32[]{:S(2)}) collective-permute-start(bf16[640,512]{1,0:T(8,128)(2,1)S(1)} %slice.83), channel_id=1, source_target_pairs={{0,1},{1,2},{2,3},{3,0},{4,5},{5,6},{6,7},{7,4},{8,9},{9,10},{10,1... | collective-permute-start | bytes 1966088 | tf_op jit(solution)/shard_map/ppermute | solution.py:81
  99.3 37.7 %copy-start.10 = (bf16[1,2048,512]{2,1,0:T(8,128)(2,1)S(1)}, bf16[1,2048,512]{2,1,0:T(8,128)(2,1)}, u32[]{:S(2)}) copy-start(bf16[1,2048,512]{2,1,0:T(8,128)(2,1)} %param.14) | copy-start | bytes 6291460
  168.5 32.8 %all-to-all-start.3 = ((f32[32,1,40]{2,1,0:T(1,128)}), f32[32,1,40]{2,1,0:T(1,128)S(1)}, u32[]{:S(2)}, u32[]{:S(2)}) async-start(f32[32,1,40]{2,1,0:T(1,128)} %reshape.180), calls=%async_computation.3 | async-start | bytes 32768 | tf_op jit(solution)/shard_map/all_to_all | solution.py:50
  173.4 143.4 %reduce-scatter.4.cloned.1.call-start = ((), (), s32[]{:S(2)}) async-start(), calls=%async_computation.6 | async-start | bytes 1351680
  177.6 46.0 %collective-permute-start.6 = (bf16[640,512]{1,0:T(8,128)(2,1)}, bf16[640,512]{1,0:T(8,128)(2,1)}, u32[]{:S(2)}, u32[]{:S(2)}) collective-permute-start(bf16[640,512]{1,0:T(8,128)(2,1)} %get-tuple-element.61), channel_id=1, source_target_pairs={{0,1},{1,2},{2,3},{3,0},{4,5},{5,6},{6,7},{7,4},{8,9},{9,10},{10,1... | collective-permute-start | bytes 1966088 | tf_op jit(solution)/shard_map/ppermute | solution.py:119
  177.6 40.1 %collective-permute-start.8 = (bf16[640,512]{1,0:T(8,128)(2,1)}, bf16[640,512]{1,0:T(8,128)(2,1)}, u32[]{:S(2)}, u32[]{:S(2)}) collective-permute-start(bf16[640,512]{1,0:T(8,128)(2,1)} %get-tuple-element.62), channel_id=1, source_target_pairs={{0,3},{1,0},{2,1},{3,2},{4,7},{5,4},{6,5},{7,6},{8,11},{9,8},{10,9... | collective-permute-start | bytes 1966088 | tf_op jit(solution)/shard_map/ppermute | solution.py:120
  201.4 9.1 %collective-permute-start.10 = (f32[32,40]{1,0:T(8,128)S(1)}, f32[32,40]{1,0:T(8,128)S(1)}, u32[]{:S(2)}, u32[]{:S(2)}) collective-permute-start(f32[32,40]{1,0:T(8,128)S(1)} %bitcast.120), channel_id=1, source_target_pairs={{0,1},{1,0},{2,3},{3,2},{4,5},{5,4},{6,7},{7,6},{8,9},{9,8},{10,11... | collective-permute-start | bytes 15368 | tf_op jit(solution)/shard_map/ppermute | solution.py:133
  210.5 65.4 %collective-permute-start.11 = (f32[32,40]{1,0:T(8,128)S(1)}, f32[32,40]{1,0:T(8,128)S(1)}, u32[]{:S(2)}, u32[]{:S(2)}) collective-permute-start(f32[32,40]{1,0:T(8,128)S(1)} %add.147), channel_id=1, source_target_pairs={{0,2},{1,3},{2,0},{3,1},{4,6},{5,7},{6,4},{7,5},{8,10},{9,11},{10,... | collective-permute-start | bytes 15368 | tf_op jit(solution)/shard_map/ppermute | solution.py:134
  220.4 30.9 %collective-permute-start.9 = (bf16[1280,512]{1,0:T(8,128)(2,1)}, bf16[1280,512]{1,0:T(8,128)(2,1)}, u32[]{:S(2)}, u32[]{:S(2)}) collective-permute-start(bf16[1280,512]{1,0:T(8,128)(2,1)} %pad_maximum_fusion.1), channel_id=1, source_target_pairs={{0,3},{1,0},{2,1},{3,2},{4,7},{5,4},{6,5},{7,6},{8,11},{9,8},{10,9... | collective-permute-start | bytes 3932168 | tf_op jit(solution)/shard_map/ppermute | solution.py:127
  226.2 31.1 %collective-permute-start.7 = (bf16[1280,512]{1,0:T(8,128)(2,1)}, bf16[1280,512]{1,0:T(8,128)(2,1)}, u32[]{:S(2)}, u32[]{:S(2)}) collective-permute-start(bf16[1280,512]{1,0:T(8,128)(2,1)} %pad_maximum_fusion), channel_id=1, source_target_pairs={{0,1},{1,2},{2,3},{3,0},{4,5},{5,6},{6,7},{7,4},{8,9},{9,10},{10,1... | collective-permute-start | bytes 3932168 | tf_op jit(solution)/shard_map/ppermute | solution.py:126
  261.5 58.0 %all-to-all-start.2 = ((bf16[32,40,512]{2,1,0:T(8,128)(2,1)}), bf16[32,40,512]{2,1,0:T(8,128)(2,1)}, u32[]{:S(2)}, u32[]{:S(2)}) async-start(bf16[32,40,512]{2,1,0:T(8,128)(2,1)} %bitcast.113), calls=%async_computation.2 | async-start | bytes 2621440 | tf_op jit(solution)/shard_map/all_to_all | solution.py:50
  (23 other events, 79.3 us)
Sparse Core Ops, SparseCore 0:
  49.9 74.5 all-gather.1
  236.6 80.0 reduce-scatter.3

commit v3 on v2

v3 whole, which is shorter than its diff:
```python
import jax
import jax.numpy as jnp
from jax import lax
from jax.experimental import pallas as pl
from jax.experimental.pallas import tpu as pltpu
from jax.sharding import PartitionSpec as P


CLAMP_LIMIT = 7.0
SIG_SLOPE = 1.702
F32 = jnp.float32
BF16 = jnp.bfloat16
PLAIN = (((1,), (0,)), ((), ()))
COLS = (((1,), (1,)), ((), ()))
ROWS = (((0,), (0,)), ((), ()))
TILES = 4


def mm(a, b, dims=PLAIN):
    return lax.dot_general(a, b, dims, preferred_element_type=F32)


def call(body, grid, q, ins, outs, flops):
    nbytes = sum(a.size * a.dtype.itemsize for a, _ in ins)
    nbytes += sum(a.size * a.dtype.itemsize for a, _ in outs)
    return pl.pallas_call(
        body,
        grid_spec=pltpu.PrefetchScalarGridSpec(
            num_scalar_prefetch=1,
            grid=(grid,),
            in_specs=[spec for _, spec in ins],
            out_specs=[spec for _, spec in outs],
        ),
        out_shape=[a for a, _ in outs],
        cost_estimate=pl.CostEstimate(flops=flops, bytes_accessed=nbytes, transcendentals=0),
    )(q, *[a for a, _ in ins])


def first_parts(q, xa, xn, xp, ya, yb, ga, gn, gp, ua, un, up, da, dn, gate_o, up_o, back_o):
    gate_o[...] = mm(xa[...], ga[...]) + mm(xn[...], gn[...]) + mm(xp[...], gp[...])
    up_o[...] = mm(xa[...], ua[...]) + mm(xn[...], un[...]) + mm(xp[...], up[...])
    back_o[...] = mm(ya[...], da[...]) + mm(yb[...], dn[...])


def last_parts(
    q, gate_in, up_in, back_in, xf, yp, yf, gf, uf, dp, df, gt, ut, act_o, dgate_o, dup_o, w_o, away_o
):
    gate_pre = gate_in[...] + mm(xf[...], gf[...])
    up_pre = up_in[...] + mm(xf[...], uf[...])
    gate_clamp = jnp.minimum(gate_pre, CLAMP_LIMIT)
    up_clamp = jnp.clip(up_pre, -CLAMP_LIMIT, CLAMP_LIMIT)
    sig = jax.nn.sigmoid(SIG_SLOPE * gate_clamp)
    glu = gate_clamp * sig
    act = (glu * (up_clamp + 1.0)).astype(BF16)
    act_o[...] = act
    back = back_in[...] + mm(yp[...], dp[...]) + mm(yf[...], df[...])
    w_o[...] = jnp.sum(act.astype(F32) * back, axis=1, keepdims=True)
    slope = (up_clamp + 1.0) * (sig + SIG_SLOPE * gate_clamp * sig * (1.0 - sig))
    d_gate = jnp.where(gate_pre < CLAMP_LIMIT, back * slope, 0.0).astype(BF16)
    d_up = jnp.where(jnp.abs(up_pre) < CLAMP_LIMIT, back * glu, 0.0).astype(BF16)
    dgate_o[...] = d_gate
    dup_o[...] = d_up
    away_o[...] = (mm(d_gate, gt[...]) + mm(d_up, ut[...])).astype(BF16)


def next_parts(q, dg, du, gn, un, gp, up, top, low, ahead_o, behind_o):
    first = pl.program_id(0) < TILES // 2
    ahead = mm(dg[...], gn[...]) + mm(du[...], un[...])
    behind = mm(dg[...], gp[...]) + mm(du[...], up[...])
    ahead_o[...] = (ahead + jnp.where(first, top[...].astype(F32), 0.0)).astype(BF16)
    behind_o[...] = (behind + jnp.where(first, 0.0, low[...].astype(F32))).astype(BF16)


def own_part(q, dg, du, ga, ua, out):
    out[...] = (mm(dg[...], ga[...]) + mm(du[...], ua[...])).astype(BF16)


def weight_grads(q, xa, xn, xp, xf, ya, yn, yp, yf, dg, du, act, gate_o, up_o, down_o):
    for k, (x, y) in enumerate(((xa, ya), (xn, yn), (xp, yp), (xf, yf))):

        @pl.when(pl.program_id(0) == k)
        def _():
            gate_o[...] = mm(x[...], dg[...], ROWS)
            up_o[...] = mm(x[...], du[...], ROWS)
            down_o[...] = mm(act[...], y[...], ROWS)


def shards(
    tokens,
    cotangent,
    route_ids,
    route_weights,
    w_gate,
    w_up,
    w_down,
    dense_in,
    dense_out,
    dense_gate,
):
    n_ep = lax.axis_size("ep")
    n_tp = lax.axis_size("tp")
    tp = lax.axis_index("tp")
    tok, width = tokens.shape
    top = route_ids.shape[1]
    cap = 2 * tok * top // n_ep
    slots = n_ep * cap
    quarter = width // n_tp
    hid = w_gate.shape[2]
    thin, hidden = dense_in.shape
    up = [(k, (k + 1) % n_tp) for k in range(n_tp)]
    down = [(k, (k - 1) % n_tp) for k in range(n_tp)]
    own, nxt, prv, far = tp, (tp + 1) % n_tp, (tp + 3) % n_tp, (tp + 2) % n_tp
    q = jnp.stack([own, nxt, prv, far]).astype(jnp.int32)

    def cols(a, k):
        return lax.dynamic_slice_in_dim(a, k * quarter, quarter, 1)

    def exchange(a):
        return lax.all_to_all(a, "ep", split_axis=0, concat_axis=0, tiled=True)

    ids = route_ids.T
    wts = route_weights.T
    experts = lax.broadcasted_iota(jnp.int32, (n_ep, tok), 0)
    picks = [ids[k][None, :] == experts for k in range(top)]
    named = picks[0] | picks[1]
    earlier = (
        lax.broadcasted_iota(jnp.int32, (tok, tok), 0)
        < lax.broadcasted_iota(jnp.int32, (tok, tok), 1)
    ).astype(BF16)
    rank = mm(named.astype(BF16), earlier).astype(jnp.int32)
    key = jnp.where(named, rank, -1)
    hit = key[:, None, :] == lax.broadcasted_iota(jnp.int32, (n_ep, cap, tok), 1)
    place = hit.astype(BF16).reshape(slots, tok)
    share = jnp.where(picks[0], wts[0][None, :], 0) + jnp.where(picks[1], wts[1][None, :], 0)
    place_w = jnp.where(hit, share.astype(BF16)[:, None, :], 0).astype(BF16).reshape(slots, tok)

    full = cap + thin
    key_more = jnp.concatenate(
        [key, lax.broadcasted_iota(jnp.int32, (n_ep, thin), 1) + cap], axis=1
    )
    hit_more = key_more[:, None, :] == lax.broadcasted_iota(
        jnp.int32, (n_ep, full, tok + thin), 1
    )
    mine = jnp.concatenate([dense_in, dense_out], axis=1)
    rows = jnp.concatenate([cols(tokens, own), mine], axis=0)
    x_send = mm(hit_more.astype(BF16).reshape(n_ep * full, tok + thin), rows)
    x_send = x_send.astype(BF16).reshape(n_ep, full, quarter)
    x_all = exchange(x_send)
    gate_w, up_w, down_w = w_gate[0], w_up[0], w_down[0]
    x_all, gate_t, up_t, down_t = lax.optimization_barrier(
        (x_all, gate_w.T, up_w.T, down_w.T)
    )
    y_pair = jnp.concatenate([cols(cotangent, own), cols(cotangent, nxt)], axis=1)
    y_send = mm(place_w, y_pair).astype(BF16).reshape(n_ep, cap, 2 * quarter)
    f_send = mm(place, cols(tokens, far)).astype(BF16).reshape(n_ep, cap, quarter)

    def owned(a):
        return lax.dynamic_index_in_dim(
            a.reshape(tok, n_ep, n_tp, thin), own, 2, keepdims=False
        ).reshape(tok, n_ep * thin)

    tokens_own, cot_own = owned(tokens), owned(cotangent)
    f_send, tokens_own, cot_own = lax.optimization_barrier((f_send, tokens_own, cot_own))
    y_got = exchange(y_send).reshape(slots, 2 * quarter)
    x_far = exchange(f_send).reshape(slots, quarter)
    x_all_up = lax.ppermute(x_all, "tp", up)
    x_all_dn = lax.ppermute(x_all, "tp", down)
    x_own = x_all[:, :cap].reshape(slots, quarter)
    x_prv, x_nxt = [a[:, :cap].reshape(slots, quarter) for a in (x_all_up, x_all_dn)]
    d_own, d_prv, d_nxt = [a[:, cap:] for a in (x_all, x_all_up, x_all_dn)]
    d_far_low = lax.ppermute(d_prv[n_ep // 2 :], "tp", up)
    d_far_top = lax.ppermute(d_nxt[: n_ep // 2], "tp", down)
    y_own, y_nxt = y_got[:, :quarter], y_got[:, quarter:]
    y_prv = lax.ppermute(y_own, "tp", up)
    y_far = lax.ppermute(y_nxt, "tp", down)

    tile = slots // TILES

    def by_tile(a):
        return a, pl.BlockSpec((tile, a.shape[1]), lambda t, q: (t, 0))

    def by_row(a, k):
        return a, pl.BlockSpec((quarter, hid), lambda t, q: (q[k], 0))

    def by_col(a, k):
        return a, pl.BlockSpec((hid, quarter), lambda t, q: (0, q[k]))

    def whole(a):
        return a, pl.BlockSpec(a.shape, lambda t, q: (0, 0))

    def wide(width_, dtype):
        return by_tile(jax.ShapeDtypeStruct((slots, width_), dtype))

    unit = 2 * slots * quarter * hid
    parts = call(
        first_parts,
        TILES,
        q,
        [by_tile(a) for a in (x_own, x_nxt, x_prv, y_own, y_nxt)]
        + [by_row(gate_w, k) for k in range(3)]
        + [by_row(up_w, k) for k in range(3)]
        + [by_row(down_t, k) for k in range(2)],
        [wide(hid, F32)] * 3,
        8 * unit,
    )
    act, d_gate, d_up, w_part, away = call(
        last_parts,
        TILES,
        q,
        [by_tile(a) for a in (*parts, x_far, y_prv, y_far)]
        + [by_row(gate_w, 3), by_row(up_w, 3), by_row(down_t, 2), by_row(down_t, 3)]
        + [by_col(gate_t, 3), by_col(up_t, 3)],
        [wide(hid, BF16)] * 3 + [wide(1, F32), wide(quarter, BF16)],
        6 * unit,
    )
    half = slots // 2
    top_in = lax.ppermute(away[:half], "tp", up)
    low_in = lax.ppermute(away[half:], "tp", down)
    ahead, behind = call(
        next_parts,
        TILES,
        q,
        [by_tile(d_gate), by_tile(d_up), by_col(gate_t, 1), by_col(up_t, 1)]
        + [by_col(gate_t, 2), by_col(up_t, 2)]
        + [
            (top_in, pl.BlockSpec((tile, quarter), lambda t, q: (lax.min(t, TILES // 2 - 1), 0))),
            (low_in, pl.BlockSpec((tile, quarter), lambda t, q: (lax.max(t - TILES // 2, 0), 0))),
        ],
        [wide(quarter, BF16)] * 2,
        4 * unit,
    )
    ahead = lax.ppermute(ahead, "tp", up)
    behind = lax.ppermute(behind, "tp", down)
    (mid,) = call(
        own_part,
        TILES,
        q,
        [by_tile(d_gate), by_tile(d_up), by_col(gate_t, 0), by_col(up_t, 0)],
        [wide(quarter, BF16)],
        2 * unit,
    )
    total = (mid.astype(F32) + ahead.astype(F32) + behind.astype(F32)).astype(BF16)
    back_rows = exchange(total.reshape(n_ep, cap, quarter)).reshape(slots, quarter)

    grad_gate, grad_up, grad_down = call(
        weight_grads,
        n_tp,
        q,
        [whole(a) for a in (x_own, x_nxt, x_prv, x_far, y_own, y_nxt, y_prv, y_far)]
        + [whole(d_gate), whole(d_up), whole(act)],
        [
            (jax.ShapeDtypeStruct((width, hid), F32), pl.BlockSpec((quarter, hid), lambda t, q: (q[t], 0))),
            (jax.ShapeDtypeStruct((width, hid), F32), pl.BlockSpec((quarter, hid), lambda t, q: (q[t], 0))),
            (jax.ShapeDtypeStruct((hid, width), F32), pl.BlockSpec((hid, quarter), lambda t, q: (0, q[t]))),
        ],
        12 * unit,
    )

    d_far = jnp.concatenate([d_far_top, d_far_low], axis=0)
    both = jnp.zeros((n_ep, n_tp, thin, 2 * hidden), BF16)
    for piece, k in ((d_own, own), (d_nxt, nxt), (d_prv, prv), (d_far, far)):
        both = lax.dynamic_update_index_in_dim(both, piece, k, 1)
    both = both.reshape(width, 2 * hidden)
    in_whole, out_whole = both[:, :hidden], both[:, hidden:]
    dense_pre = mm(tokens, in_whole)
    dense_act = jax.nn.silu(dense_pre).astype(BF16)
    mix = jax.nn.sigmoid(jnp.dot(tokens, dense_gate, preferred_element_type=F32))
    dense_scaled = (mix[:, None] * cotangent.astype(F32)).astype(BF16)
    cot_out = mm(cotangent, out_whole)
    dense_back = mm(dense_scaled, out_whole)
    sig_pre = jax.nn.sigmoid(dense_pre)
    dense_dpre = (dense_back * sig_pre * (1.0 + dense_pre * (1.0 - sig_pre))).astype(BF16)
    dlogit = mix * (1.0 - mix) * jnp.sum(dense_act.astype(F32) * cot_out, axis=1)
    in_rows = lax.dynamic_slice_in_dim(in_whole, own * quarter, quarter, 0)
    dense_dx = mm(dense_dpre, in_rows, COLS)
    gate_cols = lax.dynamic_slice_in_dim(dense_gate, own * quarter, quarter, 0)
    dense_dx = dense_dx + dlogit[:, None] * gate_cols.astype(F32)[None, :]

    in_part = mm(tokens_own, dense_dpre, ROWS)
    scaled_own = (mix[:, None] * cot_own.astype(F32)).astype(BF16)
    out_part = mm(scaled_own, dense_act, ROWS)
    gate_part = jnp.sum(tokens_own.astype(F32) * dlogit[:, None], axis=0)
    sent = jnp.concatenate([in_part, out_part], axis=1).reshape(n_ep, thin, 2 * hidden)
    w_rows = w_part.reshape(n_ep, 1, cap)
    w_high = w_rows.astype(BF16)
    w_low = (w_rows - w_high.astype(F32)).astype(BF16)

    def line(a):
        return jnp.pad(a.astype(BF16), ((0, 0), (0, 0), (0, 2 * hidden - a.shape[2])))

    tail = jnp.concatenate([line(gate_part.reshape(n_ep, 1, thin)), line(w_high), line(w_low)], axis=1)
    tail = jnp.pad(tail, ((0, 0), (0, 5), (0, 0)))
    sent = jnp.concatenate([sent.astype(BF16), tail], axis=1)
    came = exchange(sent)
    summed = jnp.sum(came[:, : thin + 1].astype(F32), axis=0)
    w_back = came[:, thin + 1, :cap].astype(F32) + came[:, thin + 2, :cap].astype(F32)
    w_back = w_back + lax.ppermute(w_back, "tp", [(k, k ^ 1) for k in range(n_tp)])
    w_back = w_back + lax.ppermute(w_back, "tp", [(k, k ^ 2) for k in range(n_tp)])
    per_expert = jnp.sum(jnp.where(hit, w_back[:, :, None], 0.0), axis=1)
    grad_route_weights = jnp.stack(
        [
            jnp.sum(jnp.where(picks[k], per_expert, 0.0), axis=0) / wts[k].astype(F32)
            for k in range(top)
        ],
        axis=1,
    ).astype(BF16)
    grad_tokens = (dense_dx + mm(place, back_rows, ROWS)).astype(BF16)
    return (
        grad_tokens,
        grad_route_weights,
        grad_gate[None],
        grad_up[None],
        grad_down[None],
        summed[:thin, :hidden],
        summed[:thin, hidden:],
        summed[thin, :thin],
    )


def solution(mesh):
    both = ("ep", "tp")

    return jax.shard_map(
        shards,
        mesh=mesh,
        in_specs=(
            P("ep", None),
            P("ep", None),
            P("ep", None),
            P("ep", None),
            P("ep", None, "tp"),
            P("ep", None, "tp"),
            P("ep", "tp", None),
            P(both, None),
            P(both, None),
            P(),
        ),
        out_specs=(
            P("ep", "tp"),
            P("ep", None),
            P("ep", None, "tp"),
            P("ep", None, "tp"),
            P("ep", "tp", None),
            P(both, None),
            P(both, None),
            P(both),
        ),
        check_vma=False,
    )
```

time: 330 us -> 258 us (0.78)
  waiting for transfers between devices: 135 us -> 74.2 us
  matrix products: 72.8 us -> 18.5 us
  Pallas kernels: 0 us -> 52.3 us
  between operations: 14.6 us -> 1.14 us
  starting transfers between devices: 42.8 us -> 51.2 us
  other arithmetic: 17.4 us -> 12 us
    dot_general x24 -> x11, matrix products: 72.4 us -> 17.4 us  [mm(): return lax.dot_general(a, b, dims, preferred_element_type=F32)]
    pallas_call x0 -> x5, Pallas kernels: none -> 52.3 us  [call(): pl.pallas_call(body, grid_spec=pltpu.PrefetchScalarGridSpec(num_scalar_pr...]
    unnamed x3 -> x0, waiting for transfers between devices: 39.3 us -> none
    ppermute x6, waiting for transfers between devices: 33.1 us -> 5.36 us  [the longest x1 2.7 us: shards(): y_far = lax.ppermute(y_nxt, 'tp', down)]
    ppermute x1, waiting for transfers between devices: 14.8 us -> 0.01 us  [shards(): behind = lax.ppermute(behind, 'tp', down)]
    unnamed x59 -> x46, local copies, waits for them, and re-layouts: 5.03 us -> 16.4 us
    dynamic_update_slice x8 -> x3, local copies, waits for them, and re-layouts: 15.2 us -> 4.73 us  [shards(): both = lax.dynamic_update_index_in_dim(both, piece, k, 1)]
    all_to_all x4 -> x5, starting transfers between devices: 25.6 us -> 33 us  [exchange(): return lax.all_to_all(a, 'ep', split_axis=0, concat_axis=0, tiled=True)]
  transfers between devices with their start and end apart: 18 -> 17, of which waited for: 7 -> 10; matrix products, arithmetic and copies ran while one was open for 39% -> 27% of each run, Pallas kernels for 0% -> 18%
where the time goes in v3:
time: 258 us; the launch traced here: 256 us
  waiting for transfers between devices  74.2 us (29%)
  Pallas kernels  52.3 us (20%)
  starting transfers between devices  51.2 us (20%)
  local copies, waits for them, and re-layouts  46.4 us (18%)
  matrix products  18.5 us (7%)
  other arithmetic  12 us (5%)
    pallas_call x5, Pallas kernels, call(): pl.pallas_call(body, grid_spec=pltpu.PrefetchScalarGridSpec(num_scalar_pr...  52.3 us
    all_to_all x5, waiting for transfers between devices, exchange(): return lax.all_to_all(a, 'ep', split_axis=0, concat_axis=0, tiled=True)  43.3 us
    all_to_all x5, starting transfers between devices, exchange(): return lax.all_to_all(a, 'ep', split_axis=0, concat_axis=0, tiled=True)  33 us
    dot_general x11, matrix products, mm(): return lax.dot_general(a, b, dims, preferred_element_type=F32)  17.4 us
    unnamed x46, local copies, waits for them, and re-layouts  16.4 us
    ppermute x1, waiting for transfers between devices, shards(): ahead = lax.ppermute(ahead, 'tp', up)  10.2 us
    ppermute x1, waiting for transfers between devices, shards(): low_in = lax.ppermute(away[half:], 'tp', down)  6.69 us
  transfers between devices with their start and end apart: 17, of which 10 were waited for; matrix products, arithmetic and copies ran while one was open for 27% of the time, Pallas kernels for 18%

profile of v3, /device:TPU:0, one launch (start us, length us, event | category | flops | bytes accessed | tf_op | source)
XLA Modules:
  0.0 255.9 jit_solution(9174749964098570105)
XLA Ops:
  5.9 8.6 %all-to-all-start = ((bf16[32,56,512]{2,1,0:T(8,128)(2,1)}), bf16[32,56,512]{2,1,0:T(8,128)(2,1)S(1)}, u32[]{:S(2)}, u32[]{:S(2)}) async-start(bf16[32,56,512]{2,1,0:T(8,128)(2,1)} %bitcast.141), calls=%async_computation | async-start | bytes 3670016 | tf_op jit(solution)/shard_map/all_to_all | solution.py:119
  15.0 3.0 %convolution_convert_fusion = bf16[1280,1024]{1,0:T(8,128)(2,1)} fusion(bf16[1280,320]{1,0:T(8,128)(2,1)S(1)} %bitcast_select_fusion, bf16[320,512]{1,0:T(8,128)(2,1)S(1)} %get-tuple-element.59, bf16[320,512]{1,0:T(8,128)(2,1)S(1)} %get-tuple-element.58), kind=kOutput, calls=%fused_computation | convolution fusion | flops 841482240 | bytes 4096000 | tf_op jit(solution)/shard_map/dot_general | solution.py:20
  18.1 23.4 %all-to-all-done = bf16[32,56,512]{2,1,0:T(8,128)(2,1)S(1)} async-done(((bf16[32,56,512]{2,1,0:T(8,128)(2,1)}), bf16[32,56,512]{2,1,0:T(8,128)(2,1)S(1)}, u32[]{:S(2)}, u32[]{:S(2)}) %all-to-all-start) | async-done | bytes 1835040 | tf_op jit(solution)/shard_map/all_to_all | solution.py:119
  42.7 4.8 %all-to-all-start.1 = ((bf16[32,40,1024]{2,1,0:T(8,128)(2,1)}), bf16[32,40,1024]{2,1,0:T(8,128)(2,1)}, u32[]{:S(2)}, u32[]{:S(2)}) async-start(bf16[32,40,1024]{2,1,0:T(8,128)(2,1)} %bitcast.137), calls=%async_computation.1 | async-start | bytes 5242880 | tf_op jit(solution)/shard_map/all_to_all | solution.py:119
  47.6 4.1 %copy.34 = bf16[1,512,2048]{1,2,0:T(8,128)(2,1)} copy(bf16[1,512,2048]{2,1,0:T(8,128)(2,1)} %param.16) | data formatting | bytes 4194304 | tf_op args[6]
  54.2 4.1 %copy.33 = bf16[1,2048,512]{1,2,0:T(8,128)(2,1)} copy(bf16[1,2048,512]{2,1,0:T(8,128)(2,1)} %param.15) | data formatting | bytes 4194304 | tf_op args[5]
  74.1 9.7 %all-to-all-done.1 = bf16[32,40,1024]{2,1,0:T(8,128)(2,1)} async-done(((bf16[32,40,1024]{2,1,0:T(8,128)(2,1)}), bf16[32,40,1024]{2,1,0:T(8,128)(2,1)}, u32[]{:S(2)}, u32[]{:S(2)}) %all-to-all-start.1) | async-done | bytes 2621472 | tf_op jit(solution)/shard_map/all_to_all | solution.py:119
  83.7 4.7 %all-to-all-start.2 = ((bf16[32,40,512]{2,1,0:T(8,128)(2,1)}), bf16[32,40,512]{2,1,0:T(8,128)(2,1)}, u32[]{:S(2)}, u32[]{:S(2)}) async-start(bf16[32,40,512]{2,1,0:T(8,128)(2,1)} %bitcast.142), calls=%async_computation.2 | async-start | bytes 2621440 | tf_op jit(solution)/shard_map/all_to_all | solution.py:119
  88.4 3.5 %fusion.53 = (bf16[1280,512]{1,0:T(8,128)(2,1)}, bf16[1280,512]{1,0:T(8,128)(2,1)}) fusion(bf16[1280,1024]{1,0:T(8,128)(2,1)} %bitcast.30), kind=kLoop, calls=%fused_computation.111 | loop fusion | bytes 5242880 | tf_op jit(solution)/shard_map/slice | solution.py:173
  105.4 3.2 %collective-permute-start.2 = (bf16[16,16,512]{2,1,0:T(8,128)(2,1)S(1)}, bf16[16,16,512]{2,1,0:T(8,128)(2,1)S(1)}, u32[]{:S(2)}, u32[]{:S(2)}) collective-permute-start(bf16[16,16,512]{2,1,0:T(8,128)(2,1)S(1)} %slice.104), channel_id=1, source_target_pairs={{0,3},{1,0},{2,1},{3,2},{4,7},{5,4},{6,5},{7,6},{8,11},{9,8},{10,9... | collective-permute-start | bytes 786440 | tf_op jit(solution)/shard_map/ppermute | solution.py:172
  117.5 10.7 %shard_map.161 = (f32[1280,512]{1,0:T(8,128)}, f32[1280,512]{1,0:T(8,128)}, f32[1280,512]{1,0:T(8,128)}) custom-call(s32[4]{0:T(128)} %pad_add_fusion.1.q, bf16[1280,512]{1,0:T(8,128)(2,1)} %bitcast.129, bf16[1280,512]{1,0:T(8,128)(2,1)} %bitcast.133, bf16[1280,512]{1,0:T(8,128)(2,1)} %bitcast.131, bf16[1280,512]{1,0:T(8,128)(2,1)} %get-tuple-element.55.ya, ...), custom_call_target="tpu_custom_call" | custom-call | flops 5368709120 | bytes 31195136 | tf_op jit(solution)/shard_map/pallas_call | solution.py:26
  130.9 11.7 %shard_map.162 = (bf16[1280,512]{1,0:T(8,128)(2,1)}, bf16[1280,512]{1,0:T(8,128)(2,1)}, bf16[1280,512]{1,0:T(8,128)(2,1)}, f32[1280,1]{1,0:T(8,128)}, bf16[1280,512]{1,0:T(8,128)(2,1)}) custom-call(s32[4]{0:T(128)} %pad_add_fusion.1.q, f32[1280,512]{1,0:T(8,128)} %get-tuple-element.30.gate_in, f32[1280,512]{1,0:T(8,128)} %get-tuple-element.31.up_in, ...), custom_call_target="tpu_custom_call" | custom-call | flops 4026531840 | bytes 29627392 | tf_op jit(solution)/shard_map/pallas_call | solution.py:26
  145.0 16.7 %shard_map.165 = (f32[2048,512]{1,0:T(8,128)}, f32[2048,512]{1,0:T(8,128)}, f32[512,2048]{1,0:T(8,128)}) custom-call(s32[4]{0:T(128)} %pad_add_fusion.1.q, bf16[1280,512]{1,0:T(8,128)(2,1)} %bitcast.130, bf16[1280,512]{1,0:T(8,128)(2,1)} %bitcast.134, bf16[1280,512]{1,0:T(8,128)(2,1)} %bitcast.132, bf16[1280,512]{1,0:T(8,128)(2,1)} %bitcast.42.xf, ...), custom_call_target="tpu_custom_call" | custom-call | flops 8053063680 | bytes 27000832 | tf_op jit(solution)/shard_map/pallas_call | solution.py:26
  161.7 5.8 %shard_map.163 = bf16[1280,512]{1,0:T(8,128)(2,1)} custom-call(s32[4]{0:T(128)} %pad_add_fusion.1.q, bf16[1280,512]{1,0:T(8,128)(2,1)} %get-tuple-element.36.dg, bf16[1280,512]{1,0:T(8,128)(2,1)} %get-tuple-element.37.du, bf16[512,2048]{1,0:T(8,128)(2,1)} %bitcast.122, bf16[512,2048]{1,0:T(8,128)(2,1)} %bitcast.126), custom_call_target="tpu_custom_call" | custom-call | flops 1342177280 | bytes 8126464 | tf_op jit(solution)/shard_map/pallas_call | solution.py:26
  167.9 3.0 %collective-permute-start.7 = (bf16[640,512]{1,0:T(8,128)(2,1)}, bf16[640,512]{1,0:T(8,128)(2,1)}, u32[]{:S(2)}, u32[]{:S(2)}) collective-permute-start(bf16[640,512]{1,0:T(8,128)(2,1)} %get-tuple-element.56), channel_id=1, source_target_pairs={{0,3},{1,0},{2,1},{3,2},{4,7},{5,4},{6,5},{7,6},{8,11},{9,8},{10,9... | collective-permute-start | bytes 1966088 | tf_op jit(solution)/shard_map/ppermute | solution.py:218
  176.5 6.7 %collective-permute-done.7.low = bf16[640,512]{1,0:T(8,128)(2,1)} collective-permute-done((bf16[640,512]{1,0:T(8,128)(2,1)}, bf16[640,512]{1,0:T(8,128)(2,1)}, u32[]{:S(2)}, u32[]{:S(2)}) %collective-permute-start.7) | collective-permute-done | bytes 655392 | tf_op jit(solution)/shard_map/ppermute | solution.py:218
  183.2 3.4 %collective-permute-done.6.top = bf16[640,512]{1,0:T(8,128)(2,1)} collective-permute-done((bf16[640,512]{1,0:T(8,128)(2,1)}, bf16[640,512]{1,0:T(8,128)(2,1)}, u32[]{:S(2)}, u32[]{:S(2)}) %collective-permute-start.6) | collective-permute-done | bytes 655392 | tf_op jit(solution)/shard_map/ppermute | solution.py:217
  186.6 7.4 %shard_map.164 = (bf16[1280,512]{1,0:T(8,128)(2,1)}, bf16[1280,512]{1,0:T(8,128)(2,1)}) custom-call(s32[4]{0:T(128)} %pad_add_fusion.1.q, bf16[1280,512]{1,0:T(8,128)(2,1)} %get-tuple-element.36.dg, bf16[1280,512]{1,0:T(8,128)(2,1)} %get-tuple-element.37.du, bf16[512,2048]{1,0:T(8,128)(2,1)} %bitcast.123, bf16[512,2048]{1,0:T(8,128)(2,1)} %bitcast.127, ...), custom_call_target="tpu_custom_call" | custom-call | flops 2684354560 | bytes 14942208 | tf_op jit(solution)/shard_map/pallas_call | solution.py:26
  194.0 3.2 %collective-permute-start.9 = (bf16[1280,512]{1,0:T(8,128)(2,1)}, bf16[1280,512]{1,0:T(8,128)(2,1)}, u32[]{:S(2)}, u32[]{:S(2)}) collective-permute-start(bf16[1280,512]{1,0:T(8,128)(2,1)} %get-tuple-element.40), channel_id=1, source_target_pairs={{0,3},{1,0},{2,1},{3,2},{4,7},{5,4},{6,5},{7,6},{8,11},{9,8},{10,9... | collective-permute-start | bytes 3932168 | tf_op jit(solution)/shard_map/ppermute | solution.py:233
  204.1 7.4 %all-to-all-start.4 = ((bf16[32,24,512]{2,1,0:T(8,128)(2,1)}), bf16[32,24,512]{2,1,0:T(8,128)(2,1)S(1)}, u32[]{:S(2)}, u32[]{:S(2)}) async-start(bf16[32,24,512]{2,1,0:T(8,128)(2,1)} %fusion.16), calls=%async_computation.4 | async-start | bytes 1572864 | tf_op jit(solution)/shard_map/all_to_all | solution.py:119
  212.7 10.2 %collective-permute-done.8 = bf16[1280,512]{1,0:T(8,128)(2,1)} collective-permute-done((bf16[1280,512]{1,0:T(8,128)(2,1)}, bf16[1280,512]{1,0:T(8,128)(2,1)}, u32[]{:S(2)}, u32[]{:S(2)}) %collective-permute-start.8) | collective-permute-done | bytes 1310752 | tf_op jit(solution)/shard_map/ppermute | solution.py:232
  222.9 3.3 %add_convert_fusion = bf16[1280,512]{1,0:T(8,128)(2,1)} fusion(bf16[1280,512]{1,0:T(8,128)(2,1)} %collective-permute-done.9, bf16[1280,512]{1,0:T(8,128)(2,1)} %collective-permute-done.8, bf16[1280,512]{1,0:T(8,128)(2,1)S(1)} %copy-done.4), kind=kLoop, calls=%fused_computation.4 | loop fusion | flops 3932160 | bytes 5242880 | tf_op jit(solution)/shard_map/convert_element_type | solution.py:242
  226.2 7.6 %all-to-all-start.3 = ((bf16[32,40,512]{2,1,0:T(8,128)(2,1)}), bf16[32,40,512]{2,1,0:T(8,128)(2,1)S(1)}, u32[]{:S(2)}, u32[]{:S(2)}) async-start(bf16[32,40,512]{2,1,0:T(8,128)(2,1)} %bitcast.45), calls=%async_computation.3 | async-start | bytes 2621440 | tf_op jit(solution)/shard_map/all_to_all | solution.py:119
  244.2 10.1 %all-to-all-done.3 = bf16[32,40,512]{2,1,0:T(8,128)(2,1)S(1)} async-done(((bf16[32,40,512]{2,1,0:T(8,128)(2,1)}), bf16[32,40,512]{2,1,0:T(8,128)(2,1)S(1)}, u32[]{:S(2)}, u32[]{:S(2)}) %all-to-all-start.3) | async-done | bytes 1310752 | tf_op jit(solution)/shard_map/all_to_all | solution.py:119
  (126 shorter events, 78.4 us)
Async XLA Ops:
  1.5 13.1 %copy-start.13 = (s32[320]{0:T(512)}, s32[320]{0:T(512)S(1)}, u32[]{:S(2)}) copy-start(s32[320]{0:T(512)S(1)} %get-tuple-element.51) | copy-start | bytes 3844
  1.8 12.8 %copy-start.7 = (s32[32,320]{1,0:T(8,128)}, s32[32,320]{1,0:T(8,128)S(1)}, u32[]{:S(2)}) copy-start(s32[32,320]{1,0:T(8,128)S(1)} %fusion.12) | copy-start | bytes 122884
  5.9 8.7 %copy-start.12 = (bf16[320,2]{0,1:T(2,128)(2,1)S(1)}, bf16[320,2]{0,1:T(2,128)(2,1)}, u32[]{:S(2)}) copy-start(bf16[320,2]{0,1:T(2,128)(2,1)} %param.13) | copy-start | bytes 3844
  5.9 35.6 %all-to-all-start = ((bf16[32,56,512]{2,1,0:T(8,128)(2,1)}), bf16[32,56,512]{2,1,0:T(8,128)(2,1)S(1)}, u32[]{:S(2)}, u32[]{:S(2)}) async-start(bf16[32,56,512]{2,1,0:T(8,128)(2,1)} %bitcast.141), calls=%async_computation | async-start | bytes 3670016 | tf_op jit(solution)/shard_map/all_to_all | solution.py:119
  42.7 41.0 %all-to-all-start.1 = ((bf16[32,40,1024]{2,1,0:T(8,128)(2,1)}), bf16[32,40,1024]{2,1,0:T(8,128)(2,1)}, u32[]{:S(2)}, u32[]{:S(2)}) async-start(bf16[32,40,1024]{2,1,0:T(8,128)(2,1)} %bitcast.137), calls=%async_computation.1 | async-start | bytes 5242880 | tf_op jit(solution)/shard_map/all_to_all | solution.py:119
  58.3 44.2 %collective-permute-start.1 = (bf16[32,56,512]{2,1,0:T(8,128)(2,1)S(1)}, bf16[32,56,512]{2,1,0:T(8,128)(2,1)}, u32[]{:S(2)}, u32[]{:S(2)}) collective-permute-start(bf16[32,56,512]{2,1,0:T(8,128)(2,1)S(1)} %copy-done.2), channel_id=1, source_target_pairs={{0,1},{1,2},{2,3},{3,0},{4,5},{5,6},{6,7},{7,4},{8,9},{9,10},{10,1... | collective-permute-start | bytes 5505032 | tf_op jit(solution)/shard_map/ppermute | solution.py:166
  59.8 44.7 %collective-permute-start = (bf16[32,56,512]{2,1,0:T(8,128)(2,1)S(1)}, bf16[32,56,512]{2,1,0:T(8,128)(2,1)}, u32[]{:S(2)}, u32[]{:S(2)}) collective-permute-start(bf16[32,56,512]{2,1,0:T(8,128)(2,1)S(1)} %copy-done.2), channel_id=1, source_target_pairs={{0,3},{1,0},{2,1},{3,2},{4,7},{5,4},{6,5},{7,6},{8,11},{9,8},{10,9... | collective-permute-start | bytes 5505032 | tf_op jit(solution)/shard_map/ppermute | solution.py:167
  83.7 44.4 %all-to-all-start.2 = ((bf16[32,40,512]{2,1,0:T(8,128)(2,1)}), bf16[32,40,512]{2,1,0:T(8,128)(2,1)}, u32[]{:S(2)}, u32[]{:S(2)}) async-start(bf16[32,40,512]{2,1,0:T(8,128)(2,1)} %bitcast.142), calls=%async_computation.2 | async-start | bytes 2621440 | tf_op jit(solution)/shard_map/all_to_all | solution.py:119
  91.9 39.0 %collective-permute-start.5 = (bf16[1280,512]{1,0:T(8,128)(2,1)}, bf16[1280,512]{1,0:T(8,128)(2,1)}, u32[]{:S(2)}, u32[]{:S(2)}) collective-permute-start(bf16[1280,512]{1,0:T(8,128)(2,1)} %get-tuple-element.54.yb.yn), channel_id=1, source_target_pairs={{0,3},{1,0},{2,1},{3,2},{4,7},{5,4},{6,5},{7,6},{8,11},{9,8},{10,9... | collective-permute-start | bytes 3932168 | tf_op jit(solution)/shard_map/ppermute | solution.py:175
  94.7 36.2 %collective-permute-start.4 = (bf16[1280,512]{1,0:T(8,128)(2,1)}, bf16[1280,512]{1,0:T(8,128)(2,1)}, u32[]{:S(2)}, u32[]{:S(2)}) collective-permute-start(bf16[1280,512]{1,0:T(8,128)(2,1)} %get-tuple-element.55.ya), channel_id=1, source_target_pairs={{0,1},{1,2},{2,3},{3,0},{4,5},{5,6},{6,7},{7,4},{8,9},{9,10},{10,1... | collective-permute-start | bytes 3932168 | tf_op jit(solution)/shard_map/ppermute | solution.py:174
  104.2 66.7 %collective-permute-start.3 = (bf16[16,16,512]{2,1,0:T(8,128)(2,1)}, bf16[16,16,512]{2,1,0:T(8,128)(2,1)}, u32[]{:S(2)}, u32[]{:S(2)}) collective-permute-start(bf16[16,16,512]{2,1,0:T(8,128)(2,1)} %slice.105), channel_id=1, source_target_pairs={{0,1},{1,2},{2,3},{3,0},{4,5},{5,6},{6,7},{7,4},{8,9},{9,10},{10,1... | collective-permute-start | bytes 786440 | tf_op jit(solution)/shard_map/ppermute | solution.py:171
  105.4 65.5 %collective-permute-start.2 = (bf16[16,16,512]{2,1,0:T(8,128)(2,1)S(1)}, bf16[16,16,512]{2,1,0:T(8,128)(2,1)S(1)}, u32[]{:S(2)}, u32[]{:S(2)}) collective-permute-start(bf16[16,16,512]{2,1,0:T(8,128)(2,1)S(1)} %slice.104), channel_id=1, source_target_pairs={{0,3},{1,0},{2,1},{3,2},{4,7},{5,4},{6,5},{7,6},{8,11},{9,8},{10,9... | collective-permute-start | bytes 786440 | tf_op jit(solution)/shard_map/ppermute | solution.py:172
  167.9 15.3 %collective-permute-start.7 = (bf16[640,512]{1,0:T(8,128)(2,1)}, bf16[640,512]{1,0:T(8,128)(2,1)}, u32[]{:S(2)}, u32[]{:S(2)}) collective-permute-start(bf16[640,512]{1,0:T(8,128)(2,1)} %get-tuple-element.56), channel_id=1, source_target_pairs={{0,3},{1,0},{2,1},{3,2},{4,7},{5,4},{6,5},{7,6},{8,11},{9,8},{10,9... | collective-permute-start | bytes 1966088 | tf_op jit(solution)/shard_map/ppermute | solution.py:218
  170.9 15.7 %collective-permute-start.6 = (bf16[640,512]{1,0:T(8,128)(2,1)}, bf16[640,512]{1,0:T(8,128)(2,1)}, u32[]{:S(2)}, u32[]{:S(2)}) collective-permute-start(bf16[640,512]{1,0:T(8,128)(2,1)} %get-tuple-element.57), channel_id=1, source_target_pairs={{0,1},{1,2},{2,3},{3,0},{4,5},{5,6},{6,7},{7,4},{8,9},{9,10},{10,1... | collective-permute-start | bytes 1966088 | tf_op jit(solution)/shard_map/ppermute | solution.py:217
  194.0 28.9 %collective-permute-start.8 = (bf16[1280,512]{1,0:T(8,128)(2,1)}, bf16[1280,512]{1,0:T(8,128)(2,1)}, u32[]{:S(2)}, u32[]{:S(2)}) collective-permute-start(bf16[1280,512]{1,0:T(8,128)(2,1)} %get-tuple-element.39), channel_id=1, source_target_pairs={{0,1},{1,2},{2,3},{3,0},{4,5},{5,6},{6,7},{7,4},{8,9},{9,10},{10,1... | collective-permute-start | bytes 3932168 | tf_op jit(solution)/shard_map/ppermute | solution.py:232
  194.0 28.9 %collective-permute-start.9 = (bf16[1280,512]{1,0:T(8,128)(2,1)}, bf16[1280,512]{1,0:T(8,128)(2,1)}, u32[]{:S(2)}, u32[]{:S(2)}) collective-permute-start(bf16[1280,512]{1,0:T(8,128)(2,1)} %get-tuple-element.40), channel_id=1, source_target_pairs={{0,3},{1,0},{2,1},{3,2},{4,7},{5,4},{6,5},{7,6},{8,11},{9,8},{10,9... | collective-permute-start | bytes 3932168 | tf_op jit(solution)/shard_map/ppermute | solution.py:233
  202.4 9.0 %copy-start.15 = (f32[512]{0:T(512)S(1)}, f32[512]{0:T(512)}, u32[]{:S(2)}) copy-start(f32[512]{0:T(512)} %dynamic-slice_convert_fusion) | copy-start | bytes 6148
  203.1 19.8 %copy-start.4 = (bf16[1280,512]{1,0:T(8,128)(2,1)S(1)}, bf16[1280,512]{1,0:T(8,128)(2,1)}, u32[]{:S(2)}) copy-start(bf16[1280,512]{1,0:T(8,128)(2,1)} %shard_map.163) | copy-start | bytes 3932164
  204.1 22.1 %all-to-all-start.4 = ((bf16[32,24,512]{2,1,0:T(8,128)(2,1)}), bf16[32,24,512]{2,1,0:T(8,128)(2,1)S(1)}, u32[]{:S(2)}, u32[]{:S(2)}) async-start(bf16[32,24,512]{2,1,0:T(8,128)(2,1)} %fusion.16), calls=%async_computation.4 | async-start | bytes 1572864 | tf_op jit(solution)/shard_map/all_to_all | solution.py:119
  226.2 16.7 %copy-start.9 = (s32[32,320]{1,0:T(8,128)S(1)}, s32[32,320]{1,0:T(8,128)}, u32[]{:S(2)}) copy-start(s32[32,320]{1,0:T(8,128)} %copy-done.7) | copy-start | bytes 122884
  226.2 17.4 %copy-start.14 = (s32[320]{0:T(512)S(1)}, s32[320]{0:T(512)}, u32[]{:S(2)}) copy-start(s32[320]{0:T(512)} %copy-done.13) | copy-start | bytes 3844
  226.2 28.1 %all-to-all-start.3 = ((bf16[32,40,512]{2,1,0:T(8,128)(2,1)}), bf16[32,40,512]{2,1,0:T(8,128)(2,1)S(1)}, u32[]{:S(2)}, u32[]{:S(2)}) async-start(bf16[32,40,512]{2,1,0:T(8,128)(2,1)} %bitcast.45), calls=%async_computation.3 | async-start | bytes 2621440 | tf_op jit(solution)/shard_map/all_to_all | solution.py:119
  233.9 3.8 %collective-permute-start.10 = (f32[32,40]{1,0:T(8,128)S(1)}, f32[32,40]{1,0:T(8,128)S(1)}, u32[]{:S(2)}, u32[]{:S(2)}) collective-permute-start(f32[32,40]{1,0:T(8,128)S(1)} %bitcast.146), channel_id=1, source_target_pairs={{0,1},{1,0},{2,3},{3,2},{4,5},{5,4},{6,7},{7,6},{8,9},{9,8},{10,11... | collective-permute-start | bytes 15368 | tf_op jit(solution)/shard_map/ppermute | solution.py:297
  237.7 5.2 %collective-permute-start.11 = (f32[32,40]{1,0:T(8,128)S(1)}, f32[32,40]{1,0:T(8,128)S(1)}, u32[]{:S(2)}, u32[]{:S(2)}) collective-permute-start(f32[32,40]{1,0:T(8,128)S(1)} %add.129), channel_id=1, source_target_pairs={{0,2},{1,3},{2,0},{3,1},{4,6},{5,7},{6,4},{7,5},{8,10},{9,11},{10,... | collective-permute-start | bytes 15368 | tf_op jit(solution)/shard_map/ppermute | solution.py:298
  (13 other events, 44.3 us)

commit v4 on v3

--- a/solution.py
+++ b/solution.py
@@ -43,8 +43,9 @@
 
 
 def last_parts(
-    q, gate_in, up_in, back_in, xf, yp, yf, gf, uf, dp, df, gt, ut, act_o, dgate_o, dup_o, w_o, away_o
+    q, gate_in, up_in, back_in, xf, yp, yf, gf, uf, dp, df, *more
 ):
+    turned, (act_o, dgate_o, dup_o, w_o, *parts_o) = more[:8], more[8:]
     gate_pre = gate_in[...] + mm(xf[...], gf[...])
     up_pre = up_in[...] + mm(xf[...], uf[...])
     gate_clamp = jnp.minimum(gate_pre, CLAMP_LIMIT)
@@ -60,19 +61,8 @@
     d_up = jnp.where(jnp.abs(up_pre) < CLAMP_LIMIT, back * glu, 0.0).astype(BF16)
     dgate_o[...] = d_gate
     dup_o[...] = d_up
-    away_o[...] = (mm(d_gate, gt[...]) + mm(d_up, ut[...])).astype(BF16)
-
-
-def next_parts(q, dg, du, gn, un, gp, up, top, low, ahead_o, behind_o):
-    first = pl.program_id(0) < TILES // 2
-    ahead = mm(dg[...], gn[...]) + mm(du[...], un[...])
-    behind = mm(dg[...], gp[...]) + mm(du[...], up[...])
-    ahead_o[...] = (ahead + jnp.where(first, top[...].astype(F32), 0.0)).astype(BF16)
-    behind_o[...] = (behind + jnp.where(first, 0.0, low[...].astype(F32))).astype(BF16)
-
-
-def own_part(q, dg, du, ga, ua, out):
-    out[...] = (mm(dg[...], ga[...]) + mm(du[...], ua[...])).astype(BF16)
+    for k, out in enumerate(parts_o):
+        out[...] = (mm(d_gate, turned[k][...]) + mm(d_up, turned[4 + k][...])).astype(BF16)
 
 
 def weight_grads(q, xa, xn, xp, xf, ya, yn, yp, yf, dg, du, act, gate_o, up_o, down_o):
@@ -203,44 +193,37 @@
         [wide(hid, F32)] * 3,
         8 * unit,
     )
-    act, d_gate, d_up, w_part, away = call(
+    act, d_gate, d_up, w_part, mid, ahead, behind, away = call(
         last_parts,
         TILES,
         q,
         [by_tile(a) for a in (*parts, x_far, y_prv, y_far)]
         + [by_row(gate_w, 3), by_row(up_w, 3), by_row(down_t, 2), by_row(down_t, 3)]
-        + [by_col(gate_t, 3), by_col(up_t, 3)],
-        [wide(hid, BF16)] * 3 + [wide(1, F32), wide(quarter, BF16)],
-        6 * unit,
-    )
-    half = slots // 2
-    top_in = lax.ppermute(away[:half], "tp", up)
-    low_in = lax.ppermute(away[half:], "tp", down)
-    ahead, behind = call(
-        next_parts,
-        TILES,
-        q,
-        [by_tile(d_gate), by_tile(d_up), by_col(gate_t, 1), by_col(up_t, 1)]
-        + [by_col(gate_t, 2), by_col(up_t, 2)]
-        + [
-            (top_in, pl.BlockSpec((tile, quarter), lambda t, q: (lax.min(t, TILES // 2 - 1), 0))),
-            (low_in, pl.BlockSpec((tile, quarter), lambda t, q: (lax.max(t - TILES // 2, 0), 0))),
-        ],
-        [wide(quarter, BF16)] * 2,
-        4 * unit,
+        + [by_col(gate_t, k) for k in range(4)]
+        + [by_col(up_t, k) for k in range(4)],
+        [wide(hid, BF16)] * 3 + [wide(1, F32)] + [wide(quarter, BF16)] * 4,
+        12 * unit,
     )
     ahead = lax.ppermute(ahead, "tp", up)
     behind = lax.ppermute(behind, "tp", down)
-    (mid,) = call(
-        own_part,
-        TILES,
-        q,
-        [by_tile(d_gate), by_tile(d_up), by_col(gate_t, 0), by_col(up_t, 0)],
-        [wide(quarter, BF16)],
-        2 * unit,
-    )
-    total = (mid.astype(F32) + ahead.astype(F32) + behind.astype(F32)).astype(BF16)
-    back_rows = exchange(total.reshape(n_ep, cap, quarter)).reshape(slots, quarter)
+
+    def placed(size):
+        at = lax.broadcasted_iota(jnp.int32, (n_ep, size, tok), 1)
+        return (key[:, None, :] == at).astype(BF16).reshape(n_ep * size, tok)
+
+    w_rows = w_part.reshape(n_ep, 1, cap)
+    w_high = w_rows.astype(BF16)
+    w_low = (w_rows - w_high.astype(F32)).astype(BF16)
+
+    def line(a):
+        return jnp.pad(a.astype(BF16), ((0, 0), (0, 0), (0, quarter - a.shape[2])))
+
+    lines = jnp.pad(jnp.concatenate([line(w_high), line(w_low)], axis=1), ((0, 0), (0, 6), (0, 0)))
+    p_send = jnp.concatenate([away.reshape(n_ep, cap, quarter), lines], axis=1)
+    p_got = exchange(p_send)
+    w_back = p_got[:, cap, :cap].astype(F32) + p_got[:, cap + 1, :cap].astype(F32)
+    from_far = mm(placed(cap + 8), p_got.reshape(n_ep * (cap + 8), quarter), ROWS).astype(BF16)
+    from_far = lax.ppermute(from_far, "tp", [(k, k ^ 2) for k in range(n_tp)])
 
     grad_gate, grad_up, grad_down = call(
         weight_grads,
@@ -281,19 +264,12 @@
     out_part = mm(scaled_own, dense_act, ROWS)
     gate_part = jnp.sum(tokens_own.astype(F32) * dlogit[:, None], axis=0)
     sent = jnp.concatenate([in_part, out_part], axis=1).reshape(n_ep, thin, 2 * hidden)
-    w_rows = w_part.reshape(n_ep, 1, cap)
-    w_high = w_rows.astype(BF16)
-    w_low = (w_rows - w_high.astype(F32)).astype(BF16)
-
-    def line(a):
-        return jnp.pad(a.astype(BF16), ((0, 0), (0, 0), (0, 2 * hidden - a.shape[2])))
-
-    tail = jnp.concatenate([line(gate_part.reshape(n_ep, 1, thin)), line(w_high), line(w_low)], axis=1)
-    tail = jnp.pad(tail, ((0, 0), (0, 5), (0, 0)))
+    tail = jnp.pad(line(gate_part.reshape(n_ep, 1, thin)), ((0, 0), (0, 7), (0, 0)))
     sent = jnp.concatenate([sent.astype(BF16), tail], axis=1)
-    came = exchange(sent)
-    summed = jnp.sum(came[:, : thin + 1].astype(F32), axis=0)
-    w_back = came[:, thin + 1, :cap].astype(F32) + came[:, thin + 2, :cap].astype(F32)
+    total = (mid.astype(F32) + ahead.astype(F32) + behind.astype(F32)).astype(BF16)
+    r_send = jnp.concatenate([total.reshape(n_ep, cap, quarter), sent], axis=1)
+    r_got = exchange(r_send)
+    summed = jnp.sum(r_got[:, cap:].astype(F32), axis=0)
     w_back = w_back + lax.ppermute(w_back, "tp", [(k, k ^ 1) for k in range(n_tp)])
     w_back = w_back + lax.ppermute(w_back, "tp", [(k, k ^ 2) for k in range(n_tp)])
     per_expert = jnp.sum(jnp.where(hit, w_back[:, :, None], 0.0), axis=1)
@@ -304,7 +280,9 @@
         ],
         axis=1,
     ).astype(BF16)
-    grad_tokens = (dense_dx + mm(place, back_rows, ROWS)).astype(BF16)
+    deep = r_got.shape[1]
+    from_own = mm(placed(deep), r_got.reshape(n_ep * deep, quarter), ROWS)
+    grad_tokens = (dense_dx + from_own + from_far.astype(F32)).astype(BF16)
     return (
         grad_tokens,
         grad_route_weights,

time: 258 us -> 246 us (0.953)
  Pallas kernels: 52.3 us -> 43.9 us
  waiting for transfers between devices: 74.2 us -> 65.9 us
  other arithmetic: 12 us -> 15.7 us
  matrix products: 18.5 us -> 21.5 us
    all_to_all x5, waiting for transfers between devices: 43.3 us -> 33.1 us  [exchange(): return lax.all_to_all(a, 'ep', split_axis=0, concat_axis=0, tiled=True)]
    ppermute x1, waiting for transfers between devices: 10.2 us -> 20.2 us  [shards(): ahead = lax.ppermute(ahead, 'tp', up)]
    pallas_call x5 -> x3, Pallas kernels: 52.3 us -> 43.9 us  [call(): pl.pallas_call(body, grid_spec=pltpu.PrefetchScalarGridSpec(num_scalar_pr...]
    ppermute x2 -> x1, waiting for transfers between devices: 10.1 us -> 6.05 us  [shards(): from_far = lax.ppermute(from_far, 'tp', [(k, k ^ 2) for k in range(n_tp)])]
    concatenate x2 -> x3, other arithmetic: 1.11 us -> 4.34 us  [the longest x1 2.68 us: shards(): p_send = jnp.concatenate([away.reshape(n_ep, cap, quarter), lines], axis=1)]
    dot_general x11 -> x12, matrix products: 17.4 us -> 20.4 us  [mm(): return lax.dot_general(a, b, dims, preferred_element_type=F32)]
    unnamed x46 -> x52, local copies, waits for them, and re-layouts: 16.4 us -> 17.8 us
  transfers between devices with their start and end apart: 17 -> 16, of which waited for: 10 -> 9; matrix products, arithmetic and copies ran while one was open for 27% -> 30% of each run, Pallas kernels for 18% -> 18%
where the time goes in v4:
time: 246 us; the launch traced here: 244 us
  waiting for transfers between devices  65.9 us (27%)
  starting transfers between devices  50.2 us (20%)
  local copies, waits for them, and re-layouts  45.8 us (19%)
  Pallas kernels  43.9 us (18%)
  matrix products  21.5 us (9%)
  other arithmetic  15.7 us (6%)
    pallas_call x3, Pallas kernels, call(): pl.pallas_call(body, grid_spec=pltpu.PrefetchScalarGridSpec(num_scalar_pr...  43.9 us
    all_to_all x5, waiting for transfers between devices, exchange(): return lax.all_to_all(a, 'ep', split_axis=0, concat_axis=0, tiled=True)  33.1 us
    all_to_all x5, starting transfers between devices, exchange(): return lax.all_to_all(a, 'ep', split_axis=0, concat_axis=0, tiled=True)  32.8 us
    dot_general x12, matrix products, mm(): return lax.dot_general(a, b, dims, preferred_element_type=F32)  20.4 us
    ppermute x1, waiting for transfers between devices, shards(): ahead = lax.ppermute(ahead, 'tp', up)  20.2 us
    unnamed x52, local copies, waits for them, and re-layouts  17.8 us
    ppermute x1, waiting for transfers between devices, shards(): from_far = lax.ppermute(from_far, 'tp', [(k, k ^ 2) for k in range(n_tp)])  6.05 us
    slice x2, local copies, waits for them, and re-layouts, shards(): a[:, :cap].reshape(slots, quarter)  5 us
  transfers between devices with their start and end apart: 16, of which 9 were waited for; matrix products, arithmetic and copies ran while one was open for 30% of the time, Pallas kernels for 18%

profile of v4, /device:TPU:0, one launch (start us, length us, event | category | flops | bytes accessed | tf_op | source)
XLA Modules:
  0.0 244.1 jit_solution(3211675240224843575)
XLA Ops:
  6.6 8.6 %all-to-all-start = ((bf16[32,56,512]{2,1,0:T(8,128)(2,1)}), bf16[32,56,512]{2,1,0:T(8,128)(2,1)S(1)}, u32[]{:S(2)}, u32[]{:S(2)}) async-start(bf16[32,56,512]{2,1,0:T(8,128)(2,1)} %bitcast.150), calls=%async_computation | async-start | bytes 3670016 | tf_op jit(solution)/shard_map/all_to_all | solution.py:109
  15.8 4.0 %convolution_convert_fusion = bf16[1280,1024]{1,0:T(8,128)(2,1)} fusion(bf16[1280,320]{1,0:T(8,128)(2,1)S(1)} %bitcast_select_fusion, bf16[320,512]{1,0:T(8,128)(2,1)} %get-tuple-element.59, bf16[320,512]{1,0:T(8,128)(2,1)S(1)} %get-tuple-element.58), kind=kOutput, calls=%fused_computation.2 | convolution fusion | flops 841482240 | bytes 4096000 | tf_op jit(solution)/shard_map/dot_general | solution.py:20
  19.8 22.5 %all-to-all-done = bf16[32,56,512]{2,1,0:T(8,128)(2,1)S(1)} async-done(((bf16[32,56,512]{2,1,0:T(8,128)(2,1)}), bf16[32,56,512]{2,1,0:T(8,128)(2,1)S(1)}, u32[]{:S(2)}, u32[]{:S(2)}) %all-to-all-start) | async-done | bytes 1835040 | tf_op jit(solution)/shard_map/all_to_all | solution.py:109
  43.5 4.8 %all-to-all-start.1 = ((bf16[32,40,1024]{2,1,0:T(8,128)(2,1)}), bf16[32,40,1024]{2,1,0:T(8,128)(2,1)}, u32[]{:S(2)}, u32[]{:S(2)}) async-start(bf16[32,40,1024]{2,1,0:T(8,128)(2,1)} %bitcast.146), calls=%async_computation.1 | async-start | bytes 5242880 | tf_op jit(solution)/shard_map/all_to_all | solution.py:109
  48.3 4.1 %copy.56 = bf16[1,512,2048]{1,2,0:T(8,128)(2,1)} copy(bf16[1,512,2048]{2,1,0:T(8,128)(2,1)} %param.16) | data formatting | bytes 4194304 | tf_op args[6]
  54.9 4.1 %copy.55 = bf16[1,2048,512]{1,2,0:T(8,128)(2,1)} copy(bf16[1,2048,512]{2,1,0:T(8,128)(2,1)} %param.15) | data formatting | bytes 4194304 | tf_op args[5]
  63.4 2.5 %copy.67 = bf16[320,2048]{0,1:T(8,128)(2,1)} copy(bf16[320,2048]{1,0:T(8,128)(2,1)} %param.11) | data formatting | bytes 2621440 | tf_op args[1]
  69.5 3.0 %convolution_convert_fusion.2 = bf16[1280,512]{1,0:T(8,128)(2,1)} fusion(pred[1280,320]{1,0:T(32,128)(4,1)} %bitcast_compare_fusion.1, bf16[320,2048]{1,0:T(8,128)(2,1)S(1)} %copy-done.3, s32[]{:T(128)S(6)} %select_n.91), kind=kOutput, calls=%fused_computation.8 | convolution fusion | flops 420085760 | bytes 2048004 | tf_op jit(solution)/shard_map/dot_general | solution.py:20
  74.9 9.6 %all-to-all-done.1 = bf16[32,40,1024]{2,1,0:T(8,128)(2,1)} async-done(((bf16[32,40,1024]{2,1,0:T(8,128)(2,1)}), bf16[32,40,1024]{2,1,0:T(8,128)(2,1)}, u32[]{:S(2)}, u32[]{:S(2)}) %all-to-all-start.1) | async-done | bytes 2621472 | tf_op jit(solution)/shard_map/all_to_all | solution.py:109
  84.5 4.7 %all-to-all-start.2 = ((bf16[32,40,512]{2,1,0:T(8,128)(2,1)}), bf16[32,40,512]{2,1,0:T(8,128)(2,1)}, u32[]{:S(2)}, u32[]{:S(2)}) async-start(bf16[32,40,512]{2,1,0:T(8,128)(2,1)} %bitcast.151), calls=%async_computation.2 | async-start | bytes 2621440 | tf_op jit(solution)/shard_map/all_to_all | solution.py:109
  89.2 3.4 %fusion.55 = (bf16[1280,512]{1,0:T(8,128)(2,1)}, bf16[1280,512]{1,0:T(8,128)(2,1)}) fusion(bf16[1280,1024]{1,0:T(8,128)(2,1)} %bitcast.30), kind=kLoop, calls=%fused_computation.114 | loop fusion | bytes 5242880 | tf_op jit(solution)/shard_map/slice | solution.py:163
  92.5 2.8 %collective-permute-start.5 = (bf16[1280,512]{1,0:T(8,128)(2,1)}, bf16[1280,512]{1,0:T(8,128)(2,1)}, u32[]{:S(2)}, u32[]{:S(2)}) collective-permute-start(bf16[1280,512]{1,0:T(8,128)(2,1)} %get-tuple-element.56.yb.yn), channel_id=1, source_target_pairs={{0,3},{1,0},{2,1},{3,2},{4,7},{5,4},{6,5},{7,6},{8,11},{9,8},{10,9... | collective-permute-start | bytes 3932168 | tf_op jit(solution)/shard_map/ppermute | solution.py:165
  100.4 2.8 %collective-permute-done.1 = bf16[32,56,512]{2,1,0:T(8,128)(2,1)} collective-permute-done((bf16[32,56,512]{2,1,0:T(8,128)(2,1)S(1)}, bf16[32,56,512]{2,1,0:T(8,128)(2,1)}, u32[]{:S(2)}, u32[]{:S(2)}) %collective-permute-start.1) | collective-permute-done | bytes 1835040 | tf_op jit(solution)/shard_map/ppermute | solution.py:156
  106.8 3.0 %collective-permute-start.2 = (bf16[16,16,512]{2,1,0:T(8,128)(2,1)}, bf16[16,16,512]{2,1,0:T(8,128)(2,1)}, u32[]{:S(2)}, u32[]{:S(2)}) collective-permute-start(bf16[16,16,512]{2,1,0:T(8,128)(2,1)} %slice.96), channel_id=1, source_target_pairs={{0,3},{1,0},{2,1},{3,2},{4,7},{5,4},{6,5},{7,6},{8,11},{9,8},{10,9... | collective-permute-start | bytes 786440 | tf_op jit(solution)/shard_map/ppermute | solution.py:162
  118.6 10.7 %shard_map.161 = (f32[1280,512]{1,0:T(8,128)}, f32[1280,512]{1,0:T(8,128)}, f32[1280,512]{1,0:T(8,128)}) custom-call(s32[4]{0:T(128)} %pad_add_fusion.1.q, bf16[1280,512]{1,0:T(8,128)(2,1)} %bitcast.137, bf16[1280,512]{1,0:T(8,128)(2,1)} %bitcast.141, bf16[1280,512]{1,0:T(8,128)(2,1)} %bitcast.139, bf16[1280,512]{1,0:T(8,128)(2,1)} %get-tuple-element.57.ya, ...), custom_call_target="tpu_custom_call" | custom-call | flops 5368709120 | bytes 31195136 | tf_op jit(solution)/shard_map/pallas_call | solution.py:26
  131.6 16.5 %shard_map.162 = (bf16[1280,512]{1,0:T(8,128)(2,1)}, bf16[1280,512]{1,0:T(8,128)(2,1)}, bf16[1280,512]{1,0:T(8,128)(2,1)}, f32[1280,1]{1,0:T(8,128)}, bf16[1280,...) custom-call(s32[4]{0:T(128)} %pad_add_fusion.1.q, ...), custom_call_target="tpu_custom_call" | custom-call | flops 8053063680 | bytes 46142464 | tf_op jit(solution)/shard_map/pallas_call | solution.py:26
  149.7 2.7 %fusion.5 = bf16[32,48,512]{2,1,0:T(8,128)(2,1)} fusion(bf16[32,2,512]{2,1,0:T(2,128)(2,1)S(1)} %fusion.38, bf16[32,40,512]{2,1,0:T(8,128)(2,1)} %bitcast.152), kind=kLoop, calls=%fused_computation.18 | loop fusion | flops 4718592 | bytes 2949120 | tf_op jit(solution)/shard_map/concatenate | solution.py:222
  152.3 7.3 %all-to-all-start.4 = ((bf16[32,48,512]{2,1,0:T(8,128)(2,1)}), bf16[32,48,512]{2,1,0:T(8,128)(2,1)S(1)}, u32[]{:S(2)}, u32[]{:S(2)}) async-start(bf16[32,48,512]{2,1,0:T(8,128)(2,1)} %fusion.5), calls=%async_computation.4 | async-start | bytes 3145728 | tf_op jit(solution)/shard_map/all_to_all | solution.py:109
  172.0 20.2 %collective-permute-done.6 = bf16[1280,512]{1,0:T(8,128)(2,1)} collective-permute-done((bf16[1280,512]{1,0:T(8,128)(2,1)}, bf16[1280,512]{1,0:T(8,128)(2,1)}, u32[]{:S(2)}, u32[]{:S(2)}) %collective-permute-start.6) | collective-permute-done | bytes 1310752 | tf_op jit(solution)/shard_map/ppermute | solution.py:207
  192.2 2.6 %add_convert_fusion = bf16[1280,512]{1,0:T(8,128)(2,1)S(1)} fusion(bf16[1280,512]{1,0:T(8,128)(2,1)} %collective-permute-done.7, bf16[1280,512]{1,0:T(8,128)(2,1)} %collective-permute-done.6, bf16[1280,512]{1,0:T(8,128)(2,1)} %get-tuple-element.37), kind=kLoop, calls=%fused_computation.10 | loop fusion | flops 3932160 | bytes 5242880 | tf_op jit(solution)/shard_map/convert_element_type | solution.py:269
  197.6 7.5 %all-to-all-start.3 = ((bf16[32,64,512]{2,1,0:T(8,128)(2,1)}), bf16[32,64,512]{2,1,0:T(8,128)(2,1)S(1)}, u32[]{:S(2)}, u32[]{:S(2)}) async-start(bf16[32,64,512]{2,1,0:T(8,128)(2,1)} %fusion.4), calls=%async_computation.3 | async-start | bytes 4194304 | tf_op jit(solution)/shard_map/all_to_all | solution.py:109
  205.0 16.7 %shard_map.163 = (f32[2048,512]{1,0:T(8,128)}, f32[2048,512]{1,0:T(8,128)}, f32[512,2048]{1,0:T(8,128)}) custom-call(s32[4]{0:T(128)} %pad_add_fusion.1.q, bf16[1280,512]{1,0:T(8,128)(2,1)} %bitcast.138, bf16[1280,512]{1,0:T(8,128)(2,1)} %bitcast.142, bf16[1280,512]{1,0:T(8,128)(2,1)} %bitcast.140, bf16[1280,512]{1,0:T(8,128)(2,1)} %bitcast.42.xf, ...), custom_call_target="tpu_custom_call" | custom-call | flops 8053063680 | bytes 27000832 | tf_op jit(solution)/shard_map/pallas_call | solution.py:26
  227.3 3.0 %collective-permute-start.10 = (f32[32,40]{1,0:T(8,128)S(1)}, f32[32,40]{1,0:T(8,128)S(1)}, u32[]{:S(2)}, u32[]{:S(2)}) collective-permute-start(f32[32,40]{1,0:T(8,128)S(1)} %add.135), channel_id=1, source_target_pairs={{0,2},{1,3},{2,0},{3,1},{4,6},{5,7},{6,4},{7,5},{8,10},{9,11},{10,... | collective-permute-start | bytes 15368 | tf_op jit(solution)/shard_map/ppermute | solution.py:274
  236.1 6.1 %collective-permute-done.8 = bf16[320,512]{1,0:T(8,128)(2,1)S(1)} collective-permute-done((bf16[320,512]{1,0:T(8,128)(2,1)}, bf16[320,512]{1,0:T(8,128)(2,1)S(1)}, u32[]{:S(2)}, u32[]{:S(2)}) %collective-permute-start.8) | collective-permute-done | bytes 327712 | tf_op jit(solution)/shard_map/ppermute | solution.py:226
  (129 shorter events, 70.1 us)
Async XLA Ops:
  1.5 13.8 %copy-start.16 = (s32[320]{0:T(512)}, s32[320]{0:T(512)S(1)}, u32[]{:S(2)}) copy-start(s32[320]{0:T(512)S(1)} %get-tuple-element.53) | copy-start | bytes 3844
  1.8 13.6 %copy-start.8 = (s32[32,320]{1,0:T(8,128)}, s32[32,320]{1,0:T(8,128)S(1)}, u32[]{:S(2)}) copy-start(s32[32,320]{1,0:T(8,128)S(1)} %fusion.21) | copy-start | bytes 122884
  6.6 8.7 %copy-start.15 = (bf16[320,2]{0,1:T(2,128)(2,1)S(1)}, bf16[320,2]{0,1:T(2,128)(2,1)}, u32[]{:S(2)}) copy-start(bf16[320,2]{0,1:T(2,128)(2,1)} %param.13) | copy-start | bytes 3844
  6.6 35.6 %all-to-all-start = ((bf16[32,56,512]{2,1,0:T(8,128)(2,1)}), bf16[32,56,512]{2,1,0:T(8,128)(2,1)S(1)}, u32[]{:S(2)}, u32[]{:S(2)}) async-start(bf16[32,56,512]{2,1,0:T(8,128)(2,1)} %bitcast.150), calls=%async_computation | async-start | bytes 3670016 | tf_op jit(solution)/shard_map/all_to_all | solution.py:109
  43.5 41.0 %all-to-all-start.1 = ((bf16[32,40,1024]{2,1,0:T(8,128)(2,1)}), bf16[32,40,1024]{2,1,0:T(8,128)(2,1)}, u32[]{:S(2)}, u32[]{:S(2)}) async-start(bf16[32,40,1024]{2,1,0:T(8,128)(2,1)} %bitcast.146), calls=%async_computation.1 | async-start | bytes 5242880 | tf_op jit(solution)/shard_map/all_to_all | solution.py:109
  54.9 7.3 %copy-start.9 = (s32[32,320]{1,0:T(8,128)S(1)}, s32[32,320]{1,0:T(8,128)}, u32[]{:S(2)}) copy-start(s32[32,320]{1,0:T(8,128)} %copy-done.8) | copy-start | bytes 122884
  59.0 6.9 %copy-start.3 = (bf16[320,2048]{1,0:T(8,128)(2,1)S(1)}, bf16[320,2048]{1,0:T(8,128)(2,1)}, u32[]{:S(2)}) copy-start(bf16[320,2048]{1,0:T(8,128)(2,1)} %param.10) | copy-start | bytes 3932164
  59.0 44.2 %collective-permute-start.1 = (bf16[32,56,512]{2,1,0:T(8,128)(2,1)S(1)}, bf16[32,56,512]{2,1,0:T(8,128)(2,1)}, u32[]{:S(2)}, u32[]{:S(2)}) collective-permute-start(bf16[32,56,512]{2,1,0:T(8,128)(2,1)S(1)} %copy-done.2), channel_id=1, source_target_pairs={{0,1},{1,2},{2,3},{3,0},{4,5},{5,6},{6,7},{7,4},{8,9},{9,10},{10,1... | collective-permute-start | bytes 5505032 | tf_op jit(solution)/shard_map/ppermute | solution.py:156
  60.5 44.7 %collective-permute-start = (bf16[32,56,512]{2,1,0:T(8,128)(2,1)S(1)}, bf16[32,56,512]{2,1,0:T(8,128)(2,1)}, u32[]{:S(2)}, u32[]{:S(2)}) collective-permute-start(bf16[32,56,512]{2,1,0:T(8,128)(2,1)S(1)} %copy-done.2), channel_id=1, source_target_pairs={{0,3},{1,0},{2,1},{3,2},{4,7},{5,4},{6,5},{7,6},{8,11},{9,8},{10,9... | collective-permute-start | bytes 5505032 | tf_op jit(solution)/shard_map/ppermute | solution.py:157
  84.5 44.8 %all-to-all-start.2 = ((bf16[32,40,512]{2,1,0:T(8,128)(2,1)}), bf16[32,40,512]{2,1,0:T(8,128)(2,1)}, u32[]{:S(2)}, u32[]{:S(2)}) async-start(bf16[32,40,512]{2,1,0:T(8,128)(2,1)} %bitcast.151), calls=%async_computation.2 | async-start | bytes 2621440 | tf_op jit(solution)/shard_map/all_to_all | solution.py:109
  92.5 39.0 %collective-permute-start.5 = (bf16[1280,512]{1,0:T(8,128)(2,1)}, bf16[1280,512]{1,0:T(8,128)(2,1)}, u32[]{:S(2)}, u32[]{:S(2)}) collective-permute-start(bf16[1280,512]{1,0:T(8,128)(2,1)} %get-tuple-element.56.yb.yn), channel_id=1, source_target_pairs={{0,3},{1,0},{2,1},{3,2},{4,7},{5,4},{6,5},{7,6},{8,11},{9,8},{10,9... | collective-permute-start | bytes 3932168 | tf_op jit(solution)/shard_map/ppermute | solution.py:165
  95.3 36.3 %collective-permute-start.4 = (bf16[1280,512]{1,0:T(8,128)(2,1)}, bf16[1280,512]{1,0:T(8,128)(2,1)}, u32[]{:S(2)}, u32[]{:S(2)}) collective-permute-start(bf16[1280,512]{1,0:T(8,128)(2,1)} %get-tuple-element.57.ya), channel_id=1, source_target_pairs={{0,1},{1,2},{2,3},{3,0},{4,5},{5,6},{6,7},{7,4},{8,9},{9,10},{10,1... | collective-permute-start | bytes 3932168 | tf_op jit(solution)/shard_map/ppermute | solution.py:164
  104.9 58.1 %collective-permute-start.3 = (bf16[16,16,512]{2,1,0:T(8,128)(2,1)}, bf16[16,16,512]{2,1,0:T(8,128)(2,1)}, u32[]{:S(2)}, u32[]{:S(2)}) collective-permute-start(bf16[16,16,512]{2,1,0:T(8,128)(2,1)} %slice.97), channel_id=1, source_target_pairs={{0,1},{1,2},{2,3},{3,0},{4,5},{5,6},{6,7},{7,4},{8,9},{9,10},{10,1... | collective-permute-start | bytes 786440 | tf_op jit(solution)/shard_map/ppermute | solution.py:161
  106.8 56.1 %collective-permute-start.2 = (bf16[16,16,512]{2,1,0:T(8,128)(2,1)}, bf16[16,16,512]{2,1,0:T(8,128)(2,1)}, u32[]{:S(2)}, u32[]{:S(2)}) collective-permute-start(bf16[16,16,512]{2,1,0:T(8,128)(2,1)} %slice.96), channel_id=1, source_target_pairs={{0,3},{1,0},{2,1},{3,2},{4,7},{5,4},{6,5},{7,6},{8,11},{9,8},{10,9... | collective-permute-start | bytes 786440 | tf_op jit(solution)/shard_map/ppermute | solution.py:162
  152.3 44.1 %all-to-all-start.4 = ((bf16[32,48,512]{2,1,0:T(8,128)(2,1)}), bf16[32,48,512]{2,1,0:T(8,128)(2,1)S(1)}, u32[]{:S(2)}, u32[]{:S(2)}) async-start(bf16[32,48,512]{2,1,0:T(8,128)(2,1)} %fusion.5), calls=%async_computation.4 | async-start | bytes 3145728 | tf_op jit(solution)/shard_map/all_to_all | solution.py:109
  159.6 32.6 %collective-permute-start.6 = (bf16[1280,512]{1,0:T(8,128)(2,1)}, bf16[1280,512]{1,0:T(8,128)(2,1)}, u32[]{:S(2)}, u32[]{:S(2)}) collective-permute-start(bf16[1280,512]{1,0:T(8,128)(2,1)} %get-tuple-element.38), channel_id=1, source_target_pairs={{0,1},{1,2},{2,3},{3,0},{4,5},{5,6},{6,7},{7,4},{8,9},{9,10},{10,1... | collective-permute-start | bytes 3932168 | tf_op jit(solution)/shard_map/ppermute | solution.py:207
  161.2 31.0 %collective-permute-start.7 = (bf16[1280,512]{1,0:T(8,128)(2,1)}, bf16[1280,512]{1,0:T(8,128)(2,1)}, u32[]{:S(2)}, u32[]{:S(2)}) collective-permute-start(bf16[1280,512]{1,0:T(8,128)(2,1)} %get-tuple-element.39), channel_id=1, source_target_pairs={{0,3},{1,0},{2,1},{3,2},{4,7},{5,4},{6,5},{7,6},{8,11},{9,8},{10,9... | collective-permute-start | bytes 3932168 | tf_op jit(solution)/shard_map/ppermute | solution.py:208
  197.6 37.3 %all-to-all-start.3 = ((bf16[32,64,512]{2,1,0:T(8,128)(2,1)}), bf16[32,64,512]{2,1,0:T(8,128)(2,1)S(1)}, u32[]{:S(2)}, u32[]{:S(2)}) async-start(bf16[32,64,512]{2,1,0:T(8,128)(2,1)} %fusion.4), calls=%async_computation.3 | async-start | bytes 4194304 | tf_op jit(solution)/shard_map/all_to_all | solution.py:109
  221.7 8.6 %copy-start.10 = (s32[32,320]{1,0:T(8,128)S(1)}, s32[32,320]{1,0:T(8,128)}, u32[]{:S(2)}) copy-start(s32[32,320]{1,0:T(8,128)} %copy-done.8) | copy-start | bytes 122884
  223.5 3.8 %collective-permute-start.9 = (f32[32,40]{1,0:T(8,128)S(1)}, f32[32,40]{1,0:T(8,128)S(1)}, u32[]{:S(2)}, u32[]{:S(2)}) collective-permute-start(f32[32,40]{1,0:T(8,128)S(1)} %bitcast.156), channel_id=1, source_target_pairs={{0,1},{1,0},{2,3},{3,2},{4,5},{5,4},{6,7},{7,6},{8,9},{9,8},{10,11... | collective-permute-start | bytes 15368 | tf_op jit(solution)/shard_map/ppermute | solution.py:273
  227.3 6.0 %copy-start.17 = (s32[320]{0:T(512)S(1)}, s32[320]{0:T(512)}, u32[]{:S(2)}) copy-start(s32[320]{0:T(512)} %copy-done.16) | copy-start | bytes 3844
  227.3 14.9 %copy-start.11 = (f32[320,512]{1,0:T(8,128)S(1)}, f32[320,512]{1,0:T(8,128)}, u32[]{:S(2)}) copy-start(f32[320,512]{1,0:T(8,128)} %convolution_add_fusion) | copy-start | bytes 1966084
  227.3 5.3 %collective-permute-start.10 = (f32[32,40]{1,0:T(8,128)S(1)}, f32[32,40]{1,0:T(8,128)S(1)}, u32[]{:S(2)}, u32[]{:S(2)}) collective-permute-start(f32[32,40]{1,0:T(8,128)S(1)} %add.135), channel_id=1, source_target_pairs={{0,2},{1,3},{2,0},{3,1},{4,6},{5,7},{6,4},{7,5},{8,10},{9,11},{10,... | collective-permute-start | bytes 15368 | tf_op jit(solution)/shard_map/ppermute | solution.py:274
  231.9 10.3 %collective-permute-start.8 = (bf16[320,512]{1,0:T(8,128)(2,1)}, bf16[320,512]{1,0:T(8,128)(2,1)S(1)}, u32[]{:S(2)}, u32[]{:S(2)}) collective-permute-start(bf16[320,512]{1,0:T(8,128)(2,1)} %fusion.14), channel_id=1, source_target_pairs={{0,2},{1,3},{2,0},{3,1},{4,6},{5,7},{6,4},{7,5},{8,10},{9,11},{10,... | collective-permute-start | bytes 983048 | tf_op jit(solution)/shard_map/ppermute | solution.py:226
  (15 other events, 34.9 us)

commit v5 on v4

--- a/solution.py
+++ b/solution.py
@@ -45,7 +45,7 @@
 def last_parts(
     q, gate_in, up_in, back_in, xf, yp, yf, gf, uf, dp, df, *more
 ):
-    turned, (act_o, dgate_o, dup_o, w_o, *parts_o) = more[:8], more[8:]
+    turned, (act_o, dgate_o, dup_o, w_o, *parts_o) = more[:6], more[6:]
     gate_pre = gate_in[...] + mm(xf[...], gf[...])
     up_pre = up_in[...] + mm(xf[...], uf[...])
     gate_clamp = jnp.minimum(gate_pre, CLAMP_LIMIT)
@@ -62,7 +62,11 @@
     dgate_o[...] = d_gate
     dup_o[...] = d_up
     for k, out in enumerate(parts_o):
-        out[...] = (mm(d_gate, turned[k][...]) + mm(d_up, turned[4 + k][...])).astype(BF16)
+        out[...] = (mm(d_gate, turned[k][...]) + mm(d_up, turned[3 + k][...])).astype(BF16)
+
+
+def own_part(q, dg, du, ga, ua, out):
+    out[...] = (mm(dg[...], ga[...]) + mm(du[...], ua[...])).astype(BF16)
 
 
 def weight_grads(q, xa, xn, xp, xf, ya, yn, yp, yf, dg, du, act, gate_o, up_o, down_o):
@@ -193,16 +197,16 @@
         [wide(hid, F32)] * 3,
         8 * unit,
     )
-    act, d_gate, d_up, w_part, mid, ahead, behind, away = call(
+    act, d_gate, d_up, w_part, ahead, behind, away = call(
         last_parts,
         TILES,
         q,
         [by_tile(a) for a in (*parts, x_far, y_prv, y_far)]
         + [by_row(gate_w, 3), by_row(up_w, 3), by_row(down_t, 2), by_row(down_t, 3)]
-        + [by_col(gate_t, k) for k in range(4)]
-        + [by_col(up_t, k) for k in range(4)],
-        [wide(hid, BF16)] * 3 + [wide(1, F32)] + [wide(quarter, BF16)] * 4,
-        12 * unit,
+        + [by_col(gate_t, k) for k in range(1, 4)]
+        + [by_col(up_t, k) for k in range(1, 4)],
+        [wide(hid, BF16)] * 3 + [wide(1, F32)] + [wide(quarter, BF16)] * 3,
+        10 * unit,
     )
     ahead = lax.ppermute(ahead, "tp", up)
     behind = lax.ppermute(behind, "tp", down)
@@ -266,6 +270,14 @@
     sent = jnp.concatenate([in_part, out_part], axis=1).reshape(n_ep, thin, 2 * hidden)
     tail = jnp.pad(line(gate_part.reshape(n_ep, 1, thin)), ((0, 0), (0, 7), (0, 0)))
     sent = jnp.concatenate([sent.astype(BF16), tail], axis=1)
+    (mid,) = call(
+        own_part,
+        TILES,
+        q,
+        [by_tile(d_gate), by_tile(d_up), by_col(gate_t, 0), by_col(up_t, 0)],
+        [wide(quarter, BF16)],
+        2 * unit,
+    )
     total = (mid.astype(F32) + ahead.astype(F32) + behind.astype(F32)).astype(BF16)
     r_send = jnp.concatenate([total.reshape(n_ep, cap, quarter), sent], axis=1)
     r_got = exchange(r_send)

time: 246 us -> 244 us (level)
  waiting for transfers between devices: 65.9 us -> 60 us
  Pallas kernels: 43.9 us -> 47.6 us
    ppermute x1, waiting for transfers between devices: 20.2 us -> 13.9 us  [shards(): ahead = lax.ppermute(ahead, 'tp', up)]
    pallas_call x3 -> x4, Pallas kernels: 43.9 us -> 47.6 us  [call(): pl.pallas_call(body, grid_spec=pltpu.PrefetchScalarGridSpec(num_scalar_pr...]
    unnamed x52 -> x50, local copies, waits for them, and re-layouts: 17.8 us -> 17 us
  transfers between devices with their start and end apart: 16 -> 16, of which waited for: 9 -> 7; matrix products, arithmetic and copies ran while one was open for 30% -> 30% of each run, Pallas kernels for 18% -> 20%
where the time goes in v5:
time: 244 us; the launch traced here: 243 us
  waiting for transfers between devices  60 us (25%)
  starting transfers between devices  50.6 us (21%)
  Pallas kernels  47.6 us (20%)
  local copies, waits for them, and re-layouts  44.2 us (18%)
  matrix products  22.9 us (9%)
  other arithmetic  16.2 us (7%)
    pallas_call x4, Pallas kernels, call(): pl.pallas_call(body, grid_spec=pltpu.PrefetchScalarGridSpec(num_scalar_pr...  47.6 us
    all_to_all x5, starting transfers between devices, exchange(): return lax.all_to_all(a, 'ep', split_axis=0, concat_axis=0, tiled=True)  32.9 us
    all_to_all x5, waiting for transfers between devices, exchange(): return lax.all_to_all(a, 'ep', split_axis=0, concat_axis=0, tiled=True)  32.1 us
    dot_general x12, matrix products, mm(): return lax.dot_general(a, b, dims, preferred_element_type=F32)  21.9 us
    unnamed x50, local copies, waits for them, and re-layouts  17 us
    ppermute x1, waiting for transfers between devices, shards(): ahead = lax.ppermute(ahead, 'tp', up)  13.9 us
    ppermute x1, waiting for transfers between devices, shards(): from_far = lax.ppermute(from_far, 'tp', [(k, k ^ 2) for k in range(n_tp)])  7.05 us
    slice x2, local copies, waits for them, and re-layouts, shards(): a[:, :cap].reshape(slots, quarter)  4.96 us
  transfers between devices with their start and end apart: 16, of which 7 were waited for; matrix products, arithmetic and copies ran while one was open for 30% of the time, Pallas kernels for 20%

profile of v5, /device:TPU:0, one launch (start us, length us, event | category | flops | bytes accessed | tf_op | source)
XLA Modules:
  0.0 242.6 jit_solution(15716802392339805360)
XLA Ops:
  6.6 8.6 %all-to-all-start = ((bf16[32,56,512]{2,1,0:T(8,128)(2,1)}), bf16[32,56,512]{2,1,0:T(8,128)(2,1)S(1)}, u32[]{:S(2)}, u32[]{:S(2)}) async-start(bf16[32,56,512]{2,1,0:T(8,128)(2,1)} %bitcast.150), calls=%async_computation | async-start | bytes 3670016 | tf_op jit(solution)/shard_map/all_to_all | solution.py:113
  15.8 4.0 %convolution_convert_fusion = bf16[1280,1024]{1,0:T(8,128)(2,1)} fusion(bf16[1280,320]{1,0:T(8,128)(2,1)S(1)} %bitcast_select_fusion, bf16[320,512]{1,0:T(8,128)(2,1)} %get-tuple-element.57, bf16[320,512]{1,0:T(8,128)(2,1)S(1)} %get-tuple-element.56), kind=kOutput, calls=%fused_computation.2 | convolution fusion | flops 841482240 | bytes 4096000 | tf_op jit(solution)/shard_map/dot_general | solution.py:20
  19.8 22.5 %all-to-all-done = bf16[32,56,512]{2,1,0:T(8,128)(2,1)S(1)} async-done(((bf16[32,56,512]{2,1,0:T(8,128)(2,1)}), bf16[32,56,512]{2,1,0:T(8,128)(2,1)S(1)}, u32[]{:S(2)}, u32[]{:S(2)}) %all-to-all-start) | async-done | bytes 1835040 | tf_op jit(solution)/shard_map/all_to_all | solution.py:113
  43.5 4.8 %all-to-all-start.1 = ((bf16[32,40,1024]{2,1,0:T(8,128)(2,1)}), bf16[32,40,1024]{2,1,0:T(8,128)(2,1)}, u32[]{:S(2)}, u32[]{:S(2)}) async-start(bf16[32,40,1024]{2,1,0:T(8,128)(2,1)} %bitcast.146), calls=%async_computation.1 | async-start | bytes 5242880 | tf_op jit(solution)/shard_map/all_to_all | solution.py:113
  48.3 4.1 %copy.56 = bf16[1,512,2048]{1,2,0:T(8,128)(2,1)} copy(bf16[1,512,2048]{2,1,0:T(8,128)(2,1)} %param.16) | data formatting | bytes 4194304 | tf_op args[6]
  54.9 4.1 %copy.55 = bf16[1,2048,512]{1,2,0:T(8,128)(2,1)} copy(bf16[1,2048,512]{2,1,0:T(8,128)(2,1)} %param.15) | data formatting | bytes 4194304 | tf_op args[5]
  69.5 3.0 %convolution_convert_fusion.2 = bf16[1280,512]{1,0:T(8,128)(2,1)} fusion(pred[1280,320]{1,0:T(32,128)(4,1)} %bitcast_compare_fusion.1, bf16[320,2048]{1,0:T(8,128)(2,1)S(1)} %copy-done.3, s32[]{:T(128)S(6)} %select_n.91), kind=kOutput, calls=%fused_computation.8 | convolution fusion | flops 420085760 | bytes 2048004 | tf_op jit(solution)/shard_map/dot_general | solution.py:20
  74.8 9.7 %all-to-all-done.1 = bf16[32,40,1024]{2,1,0:T(8,128)(2,1)} async-done(((bf16[32,40,1024]{2,1,0:T(8,128)(2,1)}), bf16[32,40,1024]{2,1,0:T(8,128)(2,1)}, u32[]{:S(2)}, u32[]{:S(2)}) %all-to-all-start.1) | async-done | bytes 2621472 | tf_op jit(solution)/shard_map/all_to_all | solution.py:113
  84.5 4.7 %all-to-all-start.2 = ((bf16[32,40,512]{2,1,0:T(8,128)(2,1)}), bf16[32,40,512]{2,1,0:T(8,128)(2,1)}, u32[]{:S(2)}, u32[]{:S(2)}) async-start(bf16[32,40,512]{2,1,0:T(8,128)(2,1)} %bitcast.151), calls=%async_computation.2 | async-start | bytes 2621440 | tf_op jit(solution)/shard_map/all_to_all | solution.py:113
  89.1 3.4 %fusion.55 = (bf16[1280,512]{1,0:T(8,128)(2,1)}, bf16[1280,512]{1,0:T(8,128)(2,1)}) fusion(bf16[1280,1024]{1,0:T(8,128)(2,1)} %bitcast.30), kind=kLoop, calls=%fused_computation.114 | loop fusion | bytes 5242880 | tf_op jit(solution)/shard_map/slice | solution.py:167
  92.5 2.8 %collective-permute-start.5 = (bf16[1280,512]{1,0:T(8,128)(2,1)}, bf16[1280,512]{1,0:T(8,128)(2,1)}, u32[]{:S(2)}, u32[]{:S(2)}) collective-permute-start(bf16[1280,512]{1,0:T(8,128)(2,1)} %get-tuple-element.54.yb.yn), channel_id=1, source_target_pairs={{0,3},{1,0},{2,1},{3,2},{4,7},{5,4},{6,5},{7,6},{8,11},{9,8},{10,9... | collective-permute-start | bytes 3932168 | tf_op jit(solution)/shard_map/ppermute | solution.py:169
  100.5 2.7 %collective-permute-done.1 = bf16[32,56,512]{2,1,0:T(8,128)(2,1)} collective-permute-done((bf16[32,56,512]{2,1,0:T(8,128)(2,1)S(1)}, bf16[32,56,512]{2,1,0:T(8,128)(2,1)}, u32[]{:S(2)}, u32[]{:S(2)}) %collective-permute-start.1) | collective-permute-done | bytes 1835040 | tf_op jit(solution)/shard_map/ppermute | solution.py:160
  106.1 3.2 %collective-permute-start.2 = (bf16[16,16,512]{2,1,0:T(8,128)(2,1)S(1)}, bf16[16,16,512]{2,1,0:T(8,128)(2,1)S(1)}, u32[]{:S(2)}, u32[]{:S(2)}) collective-permute-start(bf16[16,16,512]{2,1,0:T(8,128)(2,1)S(1)} %slice.96), channel_id=1, source_target_pairs={{0,3},{1,0},{2,1},{3,2},{4,7},{5,4},{6,5},{7,6},{8,11},{9,8},{10,9... | collective-permute-start | bytes 786440 | tf_op jit(solution)/shard_map/ppermute | solution.py:166
  118.1 10.7 %shard_map.161 = (f32[1280,512]{1,0:T(8,128)}, f32[1280,512]{1,0:T(8,128)}, f32[1280,512]{1,0:T(8,128)}) custom-call(s32[4]{0:T(128)} %pad_add_fusion.1.q, bf16[1280,512]{1,0:T(8,128)(2,1)} %bitcast.137, bf16[1280,512]{1,0:T(8,128)(2,1)} %bitcast.141, bf16[1280,512]{1,0:T(8,128)(2,1)} %bitcast.139, bf16[1280,512]{1,0:T(8,128)(2,1)} %get-tuple-element.55.ya, ...), custom_call_target="tpu_custom_call" | custom-call | flops 5368709120 | bytes 31195136 | tf_op jit(solution)/shard_map/pallas_call | solution.py:26
  128.8 2.8 %collective-permute-done.5.yf = bf16[1280,512]{1,0:T(8,128)(2,1)} collective-permute-done((bf16[1280,512]{1,0:T(8,128)(2,1)}, bf16[1280,512]{1,0:T(8,128)(2,1)}, u32[]{:S(2)}, u32[]{:S(2)}) %collective-permute-start.5) | collective-permute-done | bytes 1310752 | tf_op jit(solution)/shard_map/ppermute | solution.py:169
  131.5 14.4 %shard_map.162 = (bf16[1280,512]{1,0:T(8,128)(2,1)}, bf16[1280,512]{1,0:T(8,128)(2,1)}, bf16[1280,512]{1,0:T(8,128)(2,1)}, f32[1280,1]{1,0:T(8,128)}, bf16[1280,...) custom-call(s32[4]{0:T(128)} %pad_add_fusion.1.q, f32[1280,512]{1,0:T(8,128)} %get-tuple-element.30.gate_in, ...), custom_call_target="tpu_custom_call" | custom-call | flops 6710886400 | bytes 40637440 | tf_op jit(solution)/shard_map/pallas_call | solution.py:26
  150.2 7.4 %all-to-all-start.4 = ((bf16[32,48,512]{2,1,0:T(8,128)(2,1)}), bf16[32,48,512]{2,1,0:T(8,128)(2,1)}, u32[]{:S(2)}, u32[]{:S(2)}) async-start(bf16[32,48,512]{2,1,0:T(8,128)(2,1)} %fusion.5), calls=%async_computation.4 | async-start | bytes 3145728 | tf_op jit(solution)/shard_map/all_to_all | solution.py:113
  160.9 5.7 %shard_map.163 = bf16[1280,512]{1,0:T(8,128)(2,1)} custom-call(s32[4]{0:T(128)} %pad_add_fusion.1.q, bf16[1280,512]{1,0:T(8,128)(2,1)} %get-tuple-element.36.dg, bf16[1280,512]{1,0:T(8,128)(2,1)} %get-tuple-element.37.du, bf16[512,2048]{1,0:T(8,128)(2,1)} %bitcast.132, bf16[512,2048]{1,0:T(8,128)(2,1)} %bitcast.136), custom_call_target="tpu_custom_call" | custom-call | flops 1342177280 | bytes 8126464 | tf_op jit(solution)/shard_map/pallas_call | solution.py:26
  176.2 13.9 %collective-permute-done.6 = bf16[1280,512]{1,0:T(8,128)(2,1)} collective-permute-done((bf16[1280,512]{1,0:T(8,128)(2,1)}, bf16[1280,512]{1,0:T(8,128)(2,1)}, u32[]{:S(2)}, u32[]{:S(2)}) %collective-permute-start.6) | collective-permute-done | bytes 1310752 | tf_op jit(solution)/shard_map/ppermute | solution.py:211
  193.9 7.4 %all-to-all-start.3 = ((bf16[32,64,512]{2,1,0:T(8,128)(2,1)}), bf16[32,64,512]{2,1,0:T(8,128)(2,1)S(1)}, u32[]{:S(2)}, u32[]{:S(2)}) async-start(bf16[32,64,512]{2,1,0:T(8,128)(2,1)} %fusion.4), calls=%async_computation.3 | async-start | bytes 4194304 | tf_op jit(solution)/shard_map/all_to_all | solution.py:113
  201.4 16.8 %shard_map.164 = (f32[2048,512]{1,0:T(8,128)}, f32[2048,512]{1,0:T(8,128)}, f32[512,2048]{1,0:T(8,128)}) custom-call(s32[4]{0:T(128)} %pad_add_fusion.1.q, bf16[1280,512]{1,0:T(8,128)(2,1)} %bitcast.138, bf16[1280,512]{1,0:T(8,128)(2,1)} %bitcast.142, bf16[1280,512]{1,0:T(8,128)(2,1)} %bitcast.140, bf16[1280,512]{1,0:T(8,128)(2,1)} %bitcast.42.xf, ...), custom_call_target="tpu_custom_call" | custom-call | flops 8053063680 | bytes 27000832 | tf_op jit(solution)/shard_map/pallas_call | solution.py:26
  224.3 3.0 %collective-permute-start.10 = (f32[32,40]{1,0:T(8,128)S(1)}, f32[32,40]{1,0:T(8,128)S(1)}, u32[]{:S(2)}, u32[]{:S(2)}) collective-permute-start(f32[32,40]{1,0:T(8,128)S(1)} %add.135), channel_id=1, source_target_pairs={{0,2},{1,3},{2,0},{3,1},{4,6},{5,7},{6,4},{7,5},{8,10},{9,11},{10,... | collective-permute-start | bytes 15368 | tf_op jit(solution)/shard_map/ppermute | solution.py:286
  227.3 3.1 %fusion.14 = bf16[320,512]{1,0:T(8,128)(2,1)} fusion(bf16[32,48,512]{2,1,0:T(8,128)(2,1)} %all-to-all-done.4, s32[32,320]{1,0:T(8,128)S(1)} %copy-done.9), kind=kOutput, calls=%fused_computation.29 | convolution fusion | flops 503971840 | bytes 1941504 | tf_op jit(solution)/shard_map/dot_general | solution.py:20
  233.6 7.0 %collective-permute-done.8 = bf16[320,512]{1,0:T(8,128)(2,1)S(1)} collective-permute-done((bf16[320,512]{1,0:T(8,128)(2,1)}, bf16[320,512]{1,0:T(8,128)(2,1)S(1)}, u32[]{:S(2)}, u32[]{:S(2)}) %collective-permute-start.8) | collective-permute-done | bytes 327712 | tf_op jit(solution)/shard_map/ppermute | solution.py:230
  (128 shorter events, 71.9 us)
Async XLA Ops:
  1.5 13.8 %copy-start.15 = (s32[320]{0:T(512)}, s32[320]{0:T(512)S(1)}, u32[]{:S(2)}) copy-start(s32[320]{0:T(512)S(1)} %get-tuple-element.51) | copy-start | bytes 3844
  1.8 13.6 %copy-start.7 = (s32[32,320]{1,0:T(8,128)}, s32[32,320]{1,0:T(8,128)S(1)}, u32[]{:S(2)}) copy-start(s32[32,320]{1,0:T(8,128)S(1)} %fusion.21) | copy-start | bytes 122884
  6.6 8.7 %copy-start.14 = (bf16[320,2]{0,1:T(2,128)(2,1)S(1)}, bf16[320,2]{0,1:T(2,128)(2,1)}, u32[]{:S(2)}) copy-start(bf16[320,2]{0,1:T(2,128)(2,1)} %param.13) | copy-start | bytes 3844
  6.6 35.6 %all-to-all-start = ((bf16[32,56,512]{2,1,0:T(8,128)(2,1)}), bf16[32,56,512]{2,1,0:T(8,128)(2,1)S(1)}, u32[]{:S(2)}, u32[]{:S(2)}) async-start(bf16[32,56,512]{2,1,0:T(8,128)(2,1)} %bitcast.150), calls=%async_computation | async-start | bytes 3670016 | tf_op jit(solution)/shard_map/all_to_all | solution.py:113
  43.5 41.0 %all-to-all-start.1 = ((bf16[32,40,1024]{2,1,0:T(8,128)(2,1)}), bf16[32,40,1024]{2,1,0:T(8,128)(2,1)}, u32[]{:S(2)}, u32[]{:S(2)}) async-start(bf16[32,40,1024]{2,1,0:T(8,128)(2,1)} %bitcast.146), calls=%async_computation.1 | async-start | bytes 5242880 | tf_op jit(solution)/shard_map/all_to_all | solution.py:113
  54.9 7.3 %copy-start.8 = (s32[32,320]{1,0:T(8,128)S(1)}, s32[32,320]{1,0:T(8,128)}, u32[]{:S(2)}) copy-start(s32[32,320]{1,0:T(8,128)} %copy-done.7) | copy-start | bytes 122884
  59.0 44.2 %collective-permute-start.1 = (bf16[32,56,512]{2,1,0:T(8,128)(2,1)S(1)}, bf16[32,56,512]{2,1,0:T(8,128)(2,1)}, u32[]{:S(2)}, u32[]{:S(2)}) collective-permute-start(bf16[32,56,512]{2,1,0:T(8,128)(2,1)S(1)} %copy-done.2), channel_id=1, source_target_pairs={{0,1},{1,2},{2,3},{3,0},{4,5},{5,6},{6,7},{7,4},{8,9},{9,10},{10,1... | collective-permute-start | bytes 5505032 | tf_op jit(solution)/shard_map/ppermute | solution.py:160
  60.5 44.7 %collective-permute-start = (bf16[32,56,512]{2,1,0:T(8,128)(2,1)S(1)}, bf16[32,56,512]{2,1,0:T(8,128)(2,1)}, u32[]{:S(2)}, u32[]{:S(2)}) collective-permute-start(bf16[32,56,512]{2,1,0:T(8,128)(2,1)S(1)} %copy-done.2), channel_id=1, source_target_pairs={{0,3},{1,0},{2,1},{3,2},{4,7},{5,4},{6,5},{7,6},{8,11},{9,8},{10,9... | collective-permute-start | bytes 5505032 | tf_op jit(solution)/shard_map/ppermute | solution.py:161
  84.5 44.3 %all-to-all-start.2 = ((bf16[32,40,512]{2,1,0:T(8,128)(2,1)}), bf16[32,40,512]{2,1,0:T(8,128)(2,1)}, u32[]{:S(2)}, u32[]{:S(2)}) async-start(bf16[32,40,512]{2,1,0:T(8,128)(2,1)} %bitcast.151), calls=%async_computation.2 | async-start | bytes 2621440 | tf_op jit(solution)/shard_map/all_to_all | solution.py:113
  92.5 39.0 %collective-permute-start.5 = (bf16[1280,512]{1,0:T(8,128)(2,1)}, bf16[1280,512]{1,0:T(8,128)(2,1)}, u32[]{:S(2)}, u32[]{:S(2)}) collective-permute-start(bf16[1280,512]{1,0:T(8,128)(2,1)} %get-tuple-element.54.yb.yn), channel_id=1, source_target_pairs={{0,3},{1,0},{2,1},{3,2},{4,7},{5,4},{6,5},{7,6},{8,11},{9,8},{10,9... | collective-permute-start | bytes 3932168 | tf_op jit(solution)/shard_map/ppermute | solution.py:169
  95.3 36.3 %collective-permute-start.4 = (bf16[1280,512]{1,0:T(8,128)(2,1)}, bf16[1280,512]{1,0:T(8,128)(2,1)}, u32[]{:S(2)}, u32[]{:S(2)}) collective-permute-start(bf16[1280,512]{1,0:T(8,128)(2,1)} %get-tuple-element.55.ya), channel_id=1, source_target_pairs={{0,1},{1,2},{2,3},{3,0},{4,5},{5,6},{6,7},{7,4},{8,9},{9,10},{10,1... | collective-permute-start | bytes 3932168 | tf_op jit(solution)/shard_map/ppermute | solution.py:168
  104.9 61.7 %collective-permute-start.3 = (bf16[16,16,512]{2,1,0:T(8,128)(2,1)}, bf16[16,16,512]{2,1,0:T(8,128)(2,1)}, u32[]{:S(2)}, u32[]{:S(2)}) collective-permute-start(bf16[16,16,512]{2,1,0:T(8,128)(2,1)} %slice.97), channel_id=1, source_target_pairs={{0,1},{1,2},{2,3},{3,0},{4,5},{5,6},{6,7},{7,4},{8,9},{9,10},{10,1... | collective-permute-start | bytes 786440 | tf_op jit(solution)/shard_map/ppermute | solution.py:165
  106.1 60.5 %collective-permute-start.2 = (bf16[16,16,512]{2,1,0:T(8,128)(2,1)S(1)}, bf16[16,16,512]{2,1,0:T(8,128)(2,1)S(1)}, u32[]{:S(2)}, u32[]{:S(2)}) collective-permute-start(bf16[16,16,512]{2,1,0:T(8,128)(2,1)S(1)} %slice.96), channel_id=1, source_target_pairs={{0,3},{1,0},{2,1},{3,2},{4,7},{5,4},{6,5},{7,6},{8,11},{9,8},{10,9... | collective-permute-start | bytes 786440 | tf_op jit(solution)/shard_map/ppermute | solution.py:166
  150.2 43.8 %all-to-all-start.4 = ((bf16[32,48,512]{2,1,0:T(8,128)(2,1)}), bf16[32,48,512]{2,1,0:T(8,128)(2,1)}, u32[]{:S(2)}, u32[]{:S(2)}) async-start(bf16[32,48,512]{2,1,0:T(8,128)(2,1)} %fusion.5), calls=%async_computation.4 | async-start | bytes 3145728 | tf_op jit(solution)/shard_map/all_to_all | solution.py:113
  157.6 32.5 %collective-permute-start.6 = (bf16[1280,512]{1,0:T(8,128)(2,1)}, bf16[1280,512]{1,0:T(8,128)(2,1)}, u32[]{:S(2)}, u32[]{:S(2)}) collective-permute-start(bf16[1280,512]{1,0:T(8,128)(2,1)} %get-tuple-element.38), channel_id=1, source_target_pairs={{0,1},{1,2},{2,3},{3,0},{4,5},{5,6},{6,7},{7,4},{8,9},{9,10},{10,1... | collective-permute-start | bytes 3932168 | tf_op jit(solution)/shard_map/ppermute | solution.py:211
  159.2 30.9 %collective-permute-start.7 = (bf16[1280,512]{1,0:T(8,128)(2,1)}, bf16[1280,512]{1,0:T(8,128)(2,1)}, u32[]{:S(2)}, u32[]{:S(2)}) collective-permute-start(bf16[1280,512]{1,0:T(8,128)(2,1)} %get-tuple-element.39), channel_id=1, source_target_pairs={{0,3},{1,0},{2,1},{3,2},{4,7},{5,4},{6,5},{7,6},{8,11},{9,8},{10,9... | collective-permute-start | bytes 3932168 | tf_op jit(solution)/shard_map/ppermute | solution.py:212
  175.0 15.1 %copy-start.4 = (bf16[1280,512]{1,0:T(8,128)(2,1)S(1)}, bf16[1280,512]{1,0:T(8,128)(2,1)}, u32[]{:S(2)}) copy-start(bf16[1280,512]{1,0:T(8,128)(2,1)} %shard_map.163) | copy-start | bytes 3932164
  193.9 38.4 %all-to-all-start.3 = ((bf16[32,64,512]{2,1,0:T(8,128)(2,1)}), bf16[32,64,512]{2,1,0:T(8,128)(2,1)S(1)}, u32[]{:S(2)}, u32[]{:S(2)}) async-start(bf16[32,64,512]{2,1,0:T(8,128)(2,1)} %fusion.4), calls=%async_computation.3 | async-start | bytes 4194304 | tf_op jit(solution)/shard_map/all_to_all | solution.py:113
  218.2 9.1 %copy-start.9 = (s32[32,320]{1,0:T(8,128)S(1)}, s32[32,320]{1,0:T(8,128)}, u32[]{:S(2)}) copy-start(s32[32,320]{1,0:T(8,128)} %copy-done.7) | copy-start | bytes 122884
  220.5 3.8 %collective-permute-start.9 = (f32[32,40]{1,0:T(8,128)S(1)}, f32[32,40]{1,0:T(8,128)S(1)}, u32[]{:S(2)}, u32[]{:S(2)}) collective-permute-start(f32[32,40]{1,0:T(8,128)S(1)} %bitcast.156), channel_id=1, source_target_pairs={{0,1},{1,0},{2,3},{3,2},{4,5},{5,4},{6,7},{7,6},{8,9},{9,8},{10,11... | collective-permute-start | bytes 15368 | tf_op jit(solution)/shard_map/ppermute | solution.py:285
  224.3 7.4 %copy-start.16 = (s32[320]{0:T(512)S(1)}, s32[320]{0:T(512)}, u32[]{:S(2)}) copy-start(s32[320]{0:T(512)} %copy-done.15) | copy-start | bytes 3844
  224.3 16.3 %copy-start.10 = (f32[320,512]{1,0:T(8,128)S(1)}, f32[320,512]{1,0:T(8,128)}, u32[]{:S(2)}) copy-start(f32[320,512]{1,0:T(8,128)} %convolution_add_fusion) | copy-start | bytes 1966084
  224.3 6.7 %collective-permute-start.10 = (f32[32,40]{1,0:T(8,128)S(1)}, f32[32,40]{1,0:T(8,128)S(1)}, u32[]{:S(2)}, u32[]{:S(2)}) collective-permute-start(f32[32,40]{1,0:T(8,128)S(1)} %add.135), channel_id=1, source_target_pairs={{0,2},{1,3},{2,0},{3,1},{4,6},{5,7},{6,4},{7,5},{8,10},{9,11},{10,... | collective-permute-start | bytes 15368 | tf_op jit(solution)/shard_map/ppermute | solution.py:286
  230.4 10.3 %collective-permute-start.8 = (bf16[320,512]{1,0:T(8,128)(2,1)}, bf16[320,512]{1,0:T(8,128)(2,1)S(1)}, u32[]{:S(2)}, u32[]{:S(2)}) collective-permute-start(bf16[320,512]{1,0:T(8,128)(2,1)} %fusion.14), channel_id=1, source_target_pairs={{0,2},{1,3},{2,0},{3,1},{4,6},{5,7},{6,4},{7,5},{8,10},{9,11},{10,... | collective-permute-start | bytes 983048 | tf_op jit(solution)/shard_map/ppermute | solution.py:230
  (14 other events, 40.5 us)
